TPU v7x, 512 devices: a whole 4x8x8 slice. The times are simulated.
512 devices in a mesh: sp: 64 (over z, y), tp: 8 (over x, core).
Axes of the slice: x: 4, y: 8, z: 8, core: 2. Of those that a mesh axis runs over, the one named last changes fastest.
Arguments:
- resid: bfloat16 [12288, 2048], P('sp'), may hold values from -6 to 6
- query: bfloat16 [12288, 2048], P('sp', 'tp'), may hold values from -6 to 6
- key: bfloat16 [12288, 1024], P('sp', 'tp'), may hold values from -6 to 6
- value: bfloat16 [12288, 1024], P('sp', 'tp'), may hold values from -6 to 6
- q_gain: float32 [128], replicated, may hold values from 0.3 to 5, as said below
- k_gain: float32 [128], replicated, may hold values from 0.3 to 5, as said below
- out_weight: bfloat16 [2048, 2048], P('tp'), may hold values from -0.125 to 0.125
- norm_gain: float32 [2048], replicated, may hold values from 0.1 to 1.9
- gate_weight: bfloat16 [2048, 5632], P('sp', 'tp'), may hold values from -0.125 to 0.125
- up_weight: bfloat16 [2048, 5632], P('sp', 'tp'), may hold values from -0.125 to 0.125
- down_weight: bfloat16 [5632, 2048], P('tp', 'sp'), may hold values from -0.078125 to 0.078125
Outputs:
- mixed: bfloat16 [12288, 2048], P(('sp', 'tp'))
Inputs may be any that keep to these rules, and one draw needn't show every extreme that they name: `q_gain`: positive gains. `k_gain`: positive gains.
All inputs are finite; a program needn't handle non-finite values.
Results may differ from a plain program's by a relative error of at most 0.012.
The roundings to bfloat16 on the way count: a program that leaves them out, or rounds other values in their place, can miss the bound.
Values may be sent and summed in bfloat16 or wider, within the bound.
No kernel may reach another device: no remote copies, remote signals or barrier semaphores. Data moves between devices by JAX's collectives and lax.ppermute only.
A program may use at most 64 MiB of HBM per device.

v0:
```python
import jax
import jax.numpy as jnp
from jax import lax
from jax.sharding import Mesh
from jax.sharding import PartitionSpec as P

GRID_W = 64
SP = ("sp_0", "sp_1")
SP_TP = ("sp_0", "sp_1", "tp")


EPSILON = 1e-06


def sent_together(arrays, axis, dim, along):
    widths = [a.shape[along] for a in arrays]
    both = jnp.concatenate(arrays, axis=along)
    whole = lax.all_gather(both, axis, axis=dim, tiled=True)
    return tuple(jnp.split(whole, [sum(widths[:k]) for k in range(1, len(widths))], axis=along))


def split_up(x, dim, count):
    before, after = (x.shape[:dim], x.shape[dim + 1 :])
    return jnp.moveaxis(x.reshape(*before, count, -1, *after), dim, 0)


def sent_and_summed(x, axis, dim):
    count = lax.axis_size(axis)
    blocks = lax.all_to_all(split_up(x, dim, count), axis, 0, 0, tiled=True)
    return jnp.sum(blocks.astype(jnp.float32), axis=0)


def laid_out(blocks, dim):
    shape = list(blocks.shape[1:])
    shape[dim] *= blocks.shape[0]
    return jnp.moveaxis(blocks, 0, dim).reshape(shape)


def sent_to_all(x, axis):
    copies = jnp.broadcast_to(x, (lax.axis_size(axis), *x.shape))
    return lax.all_to_all(copies, axis, split_axis=0, concat_axis=0, tiled=True)


def gathered_copies(x, axis, dim):
    return laid_out(sent_to_all(x, axis), dim)


def all_blocks(x, axes, order):
    blocks = x
    for k in order:
        blocks = lax.all_gather(blocks, axes[k])
    done = order[::-1]
    back = [done.index(k) for k in range(len(axes))]
    blocks = blocks.transpose(*back, *range(len(axes), blocks.ndim))
    return blocks.reshape(-1, *x.shape)


def gather_axes(x, axes, order, dim):
    return laid_out(all_blocks(x, axes, order), dim)


def rotate(values, positions):
    dim_size = values.shape[-1]
    half_dim = dim_size // 2
    quarter = half_dim // 2
    inverse = 10000.0 ** (-jnp.arange(quarter, dtype=jnp.float32) / quarter)
    outputs = []
    for axis_pos, coords in enumerate((positions // GRID_W, positions % GRID_W)):
        angles = coords.astype(jnp.float32)[:, None] * inverse[None, :]
        cosine = jnp.cos(angles)[:, None, :]
        sine = jnp.sin(angles)[:, None, :]
        section = values[..., axis_pos * half_dim : (axis_pos + 1) * half_dim]
        first_half = section[..., :quarter]
        second_half = section[..., quarter:]
        outputs += [
            first_half * cosine - second_half * sine,
            second_half * cosine + first_half * sine,
        ]
    return jnp.concatenate(outputs, axis=-1)


def prepare(projected, gain, positions):
    values = projected.astype(jnp.float32)
    normed = values * lax.rsqrt(jnp.mean(values * values, axis=-1, keepdims=True) + EPSILON) * gain
    return rotate(normed, positions).astype(jnp.bfloat16)


def normalize(stream, gain):
    values = stream.astype(jnp.float32)
    return (
        values * lax.rsqrt(jnp.mean(values * values, axis=-1, keepdims=True) + EPSILON) * gain
    ).astype(jnp.bfloat16)


def body(
    resid,
    query,
    key,
    value,
    q_gain,
    k_gain,
    out_weight,
    norm_gain,
    gate_weight,
    up_weight,
    down_weight,
):
    rows_here = query.shape[0]
    head_dim = q_gain.shape[0]
    heads_here = query.shape[1] // head_dim
    kv_here = key.shape[1] // head_dim
    group_size = heads_here // kv_here
    score_scale = head_dim ** (-0.5)
    positions = lax.axis_index(SP) * rows_here + jnp.arange(rows_here, dtype=jnp.int32)
    q_rot = prepare(query.reshape(rows_here, heads_here, head_dim), q_gain, positions)
    k_rot = prepare(key.reshape(rows_here, kv_here, head_dim), k_gain, positions)
    val_rows = value.reshape(rows_here, kv_here, head_dim)
    grouped = q_rot.reshape(rows_here, kv_here, group_size, head_dim)

    def key_block(carry, block):
        maxima, totals, accum = carry
        block_keys, block_vals = block
        scores = (
            jnp.einsum("qkgd,skd->kgqs", grouped, block_keys, preferred_element_type=jnp.float32)
            * score_scale
        )
        new_max = jnp.maximum(maxima, jnp.max(scores, axis=-1))
        shrink = jnp.exp(maxima - new_max)
        weights = jnp.exp(scores - new_max[..., None])
        totals = totals * shrink + jnp.sum(weights, axis=-1)
        accum = accum * shrink[..., None] + jnp.einsum(
            "kgqs,skd->kgqd",
            weights.astype(jnp.bfloat16),
            block_vals,
            preferred_element_type=jnp.float32,
        )
        return ((new_max, totals, accum), None)

    start_max = jnp.full((kv_here, group_size, rows_here), -1e30, jnp.float32)
    start_total = jnp.zeros((kv_here, group_size, rows_here), jnp.float32)
    start_accum = jnp.zeros((kv_here, group_size, rows_here, head_dim), jnp.float32)
    carry = (start_max, start_total, start_accum)
    key_part, val_part = sent_together((k_rot, val_rows), SP, 0, 1)
    length = key_part.shape[0]
    factor = 4
    span = rows_here * factor
    turns = length // span
    key_blocks = key_part.reshape(turns, span, kv_here, head_dim)
    val_blocks = val_part.reshape(turns, span, kv_here, head_dim)
    carry, _ = lax.scan(key_block, carry, (key_blocks, val_blocks))
    maxima, totals, accum = carry
    attn = (
        jnp.transpose(accum / totals[..., None], (2, 0, 1, 3))
        .reshape(rows_here, heads_here * head_dim)
        .astype(jnp.bfloat16)
    )
    share = rows_here // lax.axis_size("tp")
    my_first = lax.axis_index("tp") * share
    proj = sent_and_summed(
        jnp.dot(attn, out_weight, preferred_element_type=jnp.float32).astype(jnp.bfloat16), "tp", 0
    )
    my_resid = lax.dynamic_slice_in_dim(resid, my_first, share, 0)
    my_stream = (my_resid.astype(jnp.float32) + proj).astype(jnp.bfloat16)
    mixer_rows = gathered_copies(normalize(my_stream, norm_gain), "tp", 0)

    def add_rows(shard_rows):
        return jnp.dot(mixer_rows, shard_rows, preferred_element_type=jnp.float32)

    shard_pair = sent_together((gate_weight, up_weight), SP, 0, 1)
    gate = add_rows(shard_pair[0])
    up_part = add_rows(shard_pair[1])
    hidden = (jax.nn.silu(gate) * up_part).astype(jnp.bfloat16)
    down_whole = gather_axes(down_weight, SP, (0, 1), 1)
    down = sent_and_summed(
        jnp.dot(hidden, down_whole, preferred_element_type=jnp.float32).astype(jnp.bfloat16),
        "tp",
        0,
    )
    return (my_stream.astype(jnp.float32) + 0.5 * down).astype(jnp.bfloat16)


def solution(mesh):
    torus = Mesh(mesh.devices.reshape(8, 8, mesh.shape["tp"]), ("sp_0", "sp_1", "tp"))
    return jax.shard_map(
        body,
        mesh=torus,
        in_specs=(
            P(SP, None),
            P(SP, "tp"),
            P(SP, "tp"),
            P(SP, "tp"),
            P(),
            P(),
            P("tp", None),
            P(),
            P(SP, "tp"),
            P(SP, "tp"),
            P("tp", SP),
        ),
        out_specs=P(SP_TP, None),
        check_vma=False,
    )
```

profile of v0, /device:TPU:1, one launch (start us, length us, event | category | flops | bytes accessed | tf_op | source)
XLA Modules:
  0.0 276.4 jit_solution(4359281037432150624)
XLA Ops:
  6.6 1.0 copy.38
  7.6 0.9 copy.39
  8.5 0.7 fusion.39
  9.6 0.8 copy.40
  10.5 28.5 %all-gather.2 = bf16[8,704,32]{1,2,0:T(8,128)(2,1)} all-gather(bf16[1,704,32]{1,2,0:T(8,128)(2,1)} %bitcast.106), channel_id=2, replica_groups=mesh['sp_0'=8,'sp_1'=8,'tp'=8] {'sp_0'}, dimensions={0}, use_global_device_ids=true | all-gather | bytes 405504 | tf_op jit(solution)/shard_map/all_gather | solution.py:51
  39.1 1.5 pad_maximum_fusion.2
  40.7 0.8 multiply_cosine_fusion.1
  41.4 1.0 reshape.443
  43.0 0.7 fusion.43
  43.7 0.6 pad_maximum_fusion.1
  44.4 61.1 %all-gather.7.cloned.1.call-done = bf16[12288,2,128]{2,1,0:T(2,128)(2,1)} async-done(((bf16[192,2,128]{2,1,0:T(2,128)(2,1)}), bf16[12288,2,128]{2,1,0:T(2,128)(2,1)}) %all-gather.7.cloned.1.call-update) | async-done | bytes 6291472 | tf_op jit(solution)/shard_map/all_gather | solution.py:18
  105.4 12.6 %fusion.68 = (bf16[12288,1,128]{2,1,0:T(2,128)(2,1)S(1)}, bf16[12288,1,128]{2,1,0:T(2,128)(2,1)S(1)}) fusion(bf16[12288,2,128]{2,1,0:T(2,128)(2,1)} %all-gather.7.cloned.1.call-done), kind=kLoop, calls=%fused_computation.109 | loop fusion | bytes 12582912 | tf_op jit(solution)/shard_map/split | solution.py:19
  118.0 4.6 %copy.50 = bf16[12288,1,128]{2,0,1:T(8,128)(2,1)} copy(bf16[12288,1,128]{2,1,0:T(2,128)(2,1)S(1)} %get-tuple-element.132) | data formatting | bytes 6291456
  122.6 4.6 %copy.51 = bf16[12288,1,128]{2,0,1:T(8,128)(2,1)} copy(bf16[12288,1,128]{2,1,0:T(2,128)(2,1)S(1)} %get-tuple-element.131) | data formatting | bytes 6291456
  127.2 50.6 %while.15 = (s32[]{:T(128)}, f32[1,2,192]{2,1,0:T(2,128)S(1)}, f32[1,2,192]{2,1,0:T(2,128)S(1)}, f32[1,2,192,128]{3,2,1,0:T(8,128)S(1)}, bf16[16,768,1,128]{3,1,...) while((s32[]{:T(128)}, f32[1,2,192]{2,1,0:T(2,128)S(1)}, ...), condition=%wide.region_5.6_spmd.clone, body=%wide.region_2.5_spmd.clone.sunk | while | flops 152914176 | bytes 4449385 | solution.py:150
  127.2 1.3 fusion.81
  128.6 1.4 fusion.84
  130.4 1.3 fusion.81
  131.8 1.4 fusion.84
  133.2 0.3 fusion.83
  133.6 1.3 fusion.81
  134.9 1.4 fusion.84
  136.4 0.3 fusion.83
  136.7 1.3 fusion.81
  138.1 1.4 fusion.84
  139.5 0.3 fusion.83
  139.9 1.3 fusion.81
  141.3 1.4 fusion.84
  142.7 0.3 fusion.83
  143.1 1.3 fusion.81
  144.4 1.4 fusion.84
  146.2 1.3 fusion.81
  147.6 1.4 fusion.84
  149.0 0.4 fusion.83
  149.4 1.3 fusion.81
  150.8 1.4 fusion.84
  152.6 1.3 fusion.81
  153.9 1.4 fusion.84
  155.7 1.3 fusion.81
  157.1 1.4 fusion.84
  158.9 1.3 fusion.81
  160.3 1.4 fusion.84
  162.1 1.3 fusion.81
  163.4 1.4 fusion.84
  165.2 1.3 fusion.81
  166.6 1.4 fusion.84
  168.4 1.3 fusion.81
  169.7 1.4 fusion.84
  171.5 1.3 fusion.81
  172.9 1.4 fusion.84
  174.7 1.3 fusion.81
  176.1 1.4 fusion.84
  178.1 1.3 convolution_convert_fusion.1
  179.4 6.1 %all-to-all-start = ((bf16[8,24,2048]{2,1,0:T(8,128)(2,1)}), bf16[8,24,2048]{2,1,0:T(8,128)(2,1)S(1)}, u32[]{:S(2)}, u32[]{:S(2)}) async-start(bf16[8,24,2048]{2,1,0:T(8,128)(2,1)} %bitcast.12), calls=%async_computation | async-start | bytes 1572864 | tf_op jit(solution)/shard_map/all_to_all | solution.py:29
  185.5 12.2 %all-to-all-done = bf16[8,24,2048]{2,1,0:T(8,128)(2,1)S(1)} async-done(((bf16[8,24,2048]{2,1,0:T(8,128)(2,1)}), bf16[8,24,2048]{2,1,0:T(8,128)(2,1)S(1)}, u32[]{:S(2)}, u32[]{:S(2)}) %all-to-all-start) | async-done | bytes 786464 | tf_op jit(solution)/shard_map/all_to_all | solution.py:29
  197.8 1.0 fusion.33
  198.9 1.0 broadcast_in_dim.11
  199.9 4.4 %all-to-all-start.1 = ((bf16[8,24,2048]{2,1,0:T(8,128)(2,1)}), bf16[8,24,2048]{2,1,0:T(8,128)(2,1)S(1)}, u32[]{:S(2)}, u32[]{:S(2)}) async-start(bf16[8,24,2048]{2,1,0:T(8,128)(2,1)} %broadcast_in_dim.11), calls=%async_computation.1 | async-start | bytes 1572864 | tf_op jit(solution)/shard_map/all_to_all | solution.py:41
  204.3 3.8 %copy.49 = bf16[8,8,704,32]{2,3,1,0:T(8,128)(2,1)} copy(bf16[8,8,704,32]{2,3,0,1:T(8,128)(2,1)} %bitcast.96) | data formatting | bytes 5767168 | tf_op jit(solution)/shard_map/transpose | solution.py:54
  208.1 33.0 %all-gather.9.cloned.1.call-done = bf16[2048,1408]{1,0:T(8,128)(2,1)} async-done(((bf16[32,1408]{1,0:T(8,128)(2,1)}), bf16[2048,1408]{1,0:T(8,128)(2,1)}) %all-gather.9.cloned.1.call-update) | async-done | bytes 5767184 | tf_op jit(solution)/shard_map/all_gather | solution.py:18
  241.1 2.7 fusion.17
  243.8 5.0 %convolution_convert_fusion = bf16[192,2048]{1,0:T(8,128)(2,1)S(1)} fusion(bf16[704,2048]{0,1:T(8,128)(2,1)} %bitcast.97, bf16[192,2048]{1,0:T(8,128)(2,1)S(1)} %bitcast.101, bf16[2048,1408]{1,0:T(8,128)(2,1)} %all-gather.9.cloned.1.call-done, f32[192,704]{1,0:T(8,128)S(1)} %fusion.17), kind=kOutput, calls=%fused_computation.27 | convolution fusion | flops 1108500480 | bytes 8404992 | tf_op jit(solution)/shard_map/dot_general | solution.py:175
  248.9 20.2 %all_to_all.15 = bf16[8,24,2048]{2,1,0:T(8,128)(2,1)S(1)} all-to-all(bf16[8,24,2048]{2,1,0:T(8,128)(2,1)S(1)} %bitcast.102), channel_id=1, replica_groups=mesh['sp_0'=8,'sp_1'=8,'tp'=8] {'tp'}, dimensions={0} | all-to-all | bytes 1572864 | tf_op jit(solution)/shard_map/all_to_all | solution.py:29
  269.2 0.7 fusion.36
  (92 shorter events, 6.0 us)
Async XLA Ops:
  6.5 171.6 %copy-start = (bf16[256,2048]{1,0:T(8,128)(2,1)S(1)}, bf16[256,2048]{1,0:T(8,128)(2,1)}, u32[]{:S(2)}) copy-start(bf16[256,2048]{1,0:T(8,128)(2,1)} %param.19) | copy-start | bytes 3145732
  6.5 36.2 %copy-start.2 = (f32[128]{0:T(128)S(1)}, f32[128]{0:T(128)}, u32[]{:S(2)}) copy-start(f32[128]{0:T(128)} %param.17) | copy-start | bytes 1540
  6.5 98.9 %all-gather.7.cloned.1.call-start = ((), (), s32[]{:S(2)}) async-start(), calls=%async_computation.3 | async-start | bytes 6389760 | tf_op jit(solution)/shard_map/all_gather | solution.py:18
  10.4 193.9 %all-gather.11.cloned.1.call-start = ((), (), s32[]{:S(2)}) async-start(), calls=%async_computation.5 | async-start | bytes 3538944 | tf_op jit(solution)/shard_map/all_gather | solution.py:51
  39.0 202.1 %all-gather.9.cloned.1.call-start = ((), (), s32[]{:S(2)}) async-start(), calls=%async_computation.4 | async-start | bytes 5857280 | tf_op jit(solution)/shard_map/all_gather | solution.py:18
  177.9 20.9 %copy-start.1 = (f32[2048]{0:T(1024)S(1)}, f32[2048]{0:T(1024)}, u32[]{:S(2)}) copy-start(f32[2048]{0:T(1024)} %param.20) | copy-start | bytes 24580
  179.4 18.2 %all-to-all-start = ((bf16[8,24,2048]{2,1,0:T(8,128)(2,1)}), bf16[8,24,2048]{2,1,0:T(8,128)(2,1)S(1)}, u32[]{:S(2)}, u32[]{:S(2)}) async-start(bf16[8,24,2048]{2,1,0:T(8,128)(2,1)} %bitcast.12), calls=%async_computation | async-start | bytes 1572864 | tf_op jit(solution)/shard_map/all_to_all | solution.py:29
  199.9 41.3 %all-to-all-start.1 = ((bf16[8,24,2048]{2,1,0:T(8,128)(2,1)}), bf16[8,24,2048]{2,1,0:T(8,128)(2,1)S(1)}, u32[]{:S(2)}, u32[]{:S(2)}) async-start(bf16[8,24,2048]{2,1,0:T(8,128)(2,1)} %broadcast_in_dim.11), calls=%async_computation.1 | async-start | bytes 1572864 | tf_op jit(solution)/shard_map/all_to_all | solution.py:41
Sparse Core Ops, SparseCore 0:
  10.5 94.8 all-gather.6
  107.5 44.2 all-gather.10
  154.9 86.2 all-gather.8
where the time goes:
time: 278 us; the launch traced here: 276 us
  waiting for transfers between devices  106 us (38%)
  matrix products  52.9 us (19%)
  blocking collectives  48.7 us (18%)
  local copies, waits for them, and re-layouts  30.4 us (11%)
  other arithmetic  13.5 us (5%)
  between operations  13.3 us (5%)
  starting transfers between devices  10.6 us (4%)
    all_gather x2, waiting for transfers between devices, sent_together(): whole = lax.all_gather(both, axis, axis=dim, tiled=True)  94.1 us
    all_gather x1, blocking collectives, all_blocks(): blocks = lax.all_gather(blocks, axes[k])  28.5 us
    dot_general x16, matrix products, key_block(): jnp.einsum('kgqs,skd->kgqd', weights.astype(jnp.bfloat16), block_vals, pr...  22.4 us
    dot_general x16, matrix products, key_block(): jnp.einsum('qkgd,skd->kgqs', grouped, block_keys, preferred_element_type=...  21.5 us
    all_to_all x1, blocking collectives, sent_and_summed(): blocks = lax.all_to_all(split_up(x, dim, count), axis, 0, 0, tiled=True)  20.2 us
    split x1, local copies, waits for them, and re-layouts, sent_together(): jnp.split(whole, [sum(widths[:k]) for k in range(1, len(widths))], axis=a...  12.6 us
    all_to_all x1, waiting for transfers between devices, sent_and_summed(): blocks = lax.all_to_all(split_up(x, dim, count), axis, 0, 0, tiled=True)  12.2 us
    unnamed x11, local copies, waits for them, and re-layouts  11.1 us
  transfers between devices with their start and end apart: 5, of which 3 were waited for; matrix products, arithmetic and copies ran while one was open for 31% of the time, Pallas kernels for 0%

commit v1 on v0

v1 whole, which is shorter than its diff:
```python
import functools

import jax
import jax.numpy as jnp
import numpy as np
from jax import lax
from jax.experimental import pallas as pl
from jax.experimental.pallas import tpu as pltpu
from jax.sharding import Mesh
from jax.sharding import PartitionSpec as P

GRID_W = 64
SP = ("sp_0", "sp_1")
SP_TP = ("sp_0", "sp_1", "tp")
EPSILON = 1e-06
BF16 = jnp.bfloat16
F32 = jnp.float32
ROPE_BASE = 10000.0
STAT_ROWS = 16
LOG2E = 1.4426950408889634


def rope_tables(head_dim):
    quarter = head_dim // 4
    lane = np.arange(head_dim)
    inverse = np.power(np.float32(ROPE_BASE), -(lane % quarter).astype(np.float32) / np.float32(quarter))
    inverse = inverse.astype(np.float32)
    angles = np.arange(GRID_W, dtype=np.float32)[:, None] * inverse[None, :]
    sign = np.where((lane // quarter) % 2 == 0, -1.0, 1.0).astype(np.float32)
    cosine = np.cos(angles.astype(np.float64)).astype(np.float32)
    sine = np.sin(angles.astype(np.float64)).astype(np.float32) * sign
    return inverse[None, :], sign[None, :], cosine, sine


def prep_kernel(q_ref, k_ref, v_ref, qg_ref, kg_ref, inv_ref, sign_ref, cos_ref, sin_ref, qo_ref, kvo_ref):
    rows, head_dim = k_ref.shape
    heads = q_ref.shape[1] // head_dim
    quarter = head_dim // 4
    spans = rows // GRID_W
    sp = lax.axis_index("sp_0") * lax.axis_size("sp_1") + lax.axis_index("sp_1")
    first_row = (sp * spans).astype(F32)
    line = first_row + lax.broadcasted_iota(jnp.int32, (8, head_dim), 0).astype(F32)
    angle = line * inv_ref[...]
    row_cos = jnp.cos(angle)
    row_sin = jnp.sin(angle) * sign_ref[...]
    lane = lax.broadcasted_iota(jnp.int32, (GRID_W, head_dim), 1)
    by_row = lane < 2 * quarter
    is_first = (lane // quarter) % 2 == 0

    def turned(x, gain, cosine, sine):
        x = x.astype(F32)
        x = x * lax.rsqrt(jnp.mean(x * x, axis=-1, keepdims=True) + EPSILON) * gain
        other = jnp.where(
            is_first,
            pltpu.roll(x, head_dim - quarter, 1),
            pltpu.roll(x, quarter, 1),
        )
        return (x * cosine + other * sine).astype(BF16)

    for j in range(spans):
        at = pl.ds(j * GRID_W, GRID_W)
        cosine = jnp.where(by_row, row_cos[j : j + 1, :], cos_ref[...])
        sine = jnp.where(by_row, row_sin[j : j + 1, :], sin_ref[...])
        for h in range(heads):
            cols = slice(h * head_dim, (h + 1) * head_dim)
            qo_ref[at, cols] = turned(q_ref[at, cols], qg_ref[...], cosine, sine)
        kvo_ref[at, 0:head_dim] = turned(k_ref[at, :], kg_ref[...], cosine, sine)
    kvo_ref[:, head_dim:] = v_ref[...]


def prep(query, key, value, q_gain, k_gain):
    rows, head_dim = key.shape
    inverse, sign, cosine, sine = rope_tables(head_dim)
    return pl.pallas_call(
        prep_kernel,
        out_shape=(
            jax.ShapeDtypeStruct(query.shape, BF16),
            jax.ShapeDtypeStruct((rows, 2 * head_dim), BF16),
        ),
        name="prep",
    )(
        query,
        key,
        value,
        q_gain.reshape(1, -1),
        k_gain.reshape(1, -1),
        jnp.asarray(inverse),
        jnp.asarray(sign),
        jnp.asarray(cosine),
        jnp.asarray(sine),
    )


def split3(x):
    a = x.astype(BF16)
    rest = x - a.astype(F32)
    b = rest.astype(BF16)
    c = (rest - b.astype(F32)).astype(BF16)
    return a, b, c


def attend_kernel(q_ref, kv_ref, o_ref, s_ref, *, chunk):
    rows, width = q_ref.shape[1:]
    keys = kv_ref.shape[0]
    head_dim = kv_ref.shape[1] // 2
    heads = width // head_dim
    factor = head_dim ** (-0.5) * LOG2E
    nt = (((1,), (1,)), ((), ()))
    eye = (
        lax.broadcasted_iota(jnp.int32, (128, 128), 0)
        == lax.broadcasted_iota(jnp.int32, (128, 128), 1)
    )
    stat = jnp.zeros((STAT_ROWS, 128), F32)
    srow = lax.broadcasted_iota(jnp.int32, (STAT_ROWS, 128), 0)
    for h in range(heads):
        cols = slice(h * head_dim, (h + 1) * head_dim)
        q = q_ref[0, :, cols]
        peak = jnp.full((rows, 128), -jnp.inf, F32)
        for c in range(keys // chunk):
            at = pl.ds(c * chunk, chunk)
            s = lax.dot_general(q, kv_ref[at, 0:head_dim], nt, preferred_element_type=F32)
            s_ref[h, :, at] = s
            for u in range(chunk // 128):
                peak = jnp.maximum(peak, s[:, u * 128 : (u + 1) * 128])
        top = jnp.max(peak, axis=-1, keepdims=True)
        total = jnp.zeros((rows, 128), F32)
        accum = jnp.zeros((rows, head_dim), F32)
        for c in range(keys // chunk):
            at = pl.ds(c * chunk, chunk)
            w = jnp.exp2((s_ref[h, :, at] - top) * factor)
            for u in range(chunk // 128):
                total = total + w[:, u * 128 : (u + 1) * 128]
            accum = accum + jnp.dot(
                w.astype(BF16), kv_ref[at, head_dim:], preferred_element_type=F32
            )
        whole = jnp.sum(total, axis=-1, keepdims=True)
        o_ref[0, 0:rows, cols] = (accum / whole).astype(BF16)
        level = top * factor + jnp.log2(whole)
        out = jnp.zeros((STAT_ROWS, 128), F32)
        for t in range(-(-rows // 128)):
            n = min(128, rows - t * 128)
            spread = jnp.broadcast_to(level[t * 128 : t * 128 + n], (n, 128))
            flat = jnp.sum(jnp.where(eye[:n], spread, 0.0), axis=0, keepdims=True)
            a, b, c = split3(flat)
            for k, piece in enumerate((a, b, c)):
                out = jnp.where(srow == 3 * t + k, piece.astype(F32), out)
        o_ref[0, rows:, cols] = out.astype(BF16)


def attend(queries, keys_values):
    parts, rows, width = queries.shape
    keys = keys_values.shape[0]
    head_dim = keys_values.shape[1] // 2
    heads = width // head_dim
    work = parts * heads * rows * keys
    return pl.pallas_call(
        functools.partial(attend_kernel, chunk=256),
        grid=(parts,),
        in_specs=[
            pl.BlockSpec((1, rows, width), lambda i: (i, 0, 0)),
            pl.BlockSpec((keys, 2 * head_dim), lambda i: (0, 0)),
        ],
        out_specs=pl.BlockSpec((1, rows + STAT_ROWS, width), lambda i: (i, 0, 0)),
        out_shape=jax.ShapeDtypeStruct((parts, rows + STAT_ROWS, width), BF16),
        scratch_shapes=[pltpu.VMEM((heads, rows, keys), F32)],
        compiler_params=pltpu.CompilerParams(
            dimension_semantics=("arbitrary",), vmem_limit_bytes=32 * 2**20
        ),
        cost_estimate=pl.CostEstimate(
            flops=4 * work * head_dim, bytes_accessed=4 * 2**20, transcendentals=work
        ),
        name="attend",
    )(queries, keys_values)


def project_kernel(part_ref, w_ref, o_ref):
    parts, all_rows, width = part_ref.shape
    rows = all_rows - STAT_ROWS
    head_dim = 128
    eye = (
        lax.broadcasted_iota(jnp.int32, (128, 128), 0)
        == lax.broadcasted_iota(jnp.int32, (128, 128), 1)
    )
    pieces = []
    for h in range(width // head_dim):
        cols = slice(h * head_dim, (h + 1) * head_dim)
        outs = []
        stats = [part_ref[p, rows:, cols].astype(F32) for p in range(parts)]
        for t in range(-(-rows // 128)):
            n = min(128, rows - t * 128)
            levels = [
                s[3 * t : 3 * t + 1] + s[3 * t + 1 : 3 * t + 2] + s[3 * t + 2 : 3 * t + 3]
                for s in stats
            ]
            top = functools.reduce(jnp.maximum, levels)
            shares = [jnp.exp2(v - top) for v in levels]
            whole = functools.reduce(jnp.add, shares)
            total = jnp.zeros((n, head_dim), F32)
            for p in range(parts):
                flat = jnp.broadcast_to(shares[p] / whole, (n, 128))
                share = jnp.sum(jnp.where(eye[:n], flat, 0.0), axis=1, keepdims=True)
                total = total + share * part_ref[p, t * 128 : t * 128 + n, cols].astype(F32)
            outs.append(total.astype(BF16))
        pieces.append(jnp.concatenate(outs, axis=0))
    attn = jnp.concatenate(pieces, axis=1)
    for c in range(w_ref.shape[1] // 512):
        at = pl.ds(c * 512, 512)
        o_ref[:, at] = jnp.dot(attn, w_ref[:, at], preferred_element_type=F32).astype(BF16)


def project(parts, weight):
    rows = parts.shape[1] - STAT_ROWS
    return pl.pallas_call(
        project_kernel,
        out_shape=jax.ShapeDtypeStruct((rows, weight.shape[1]), BF16),
        cost_estimate=pl.CostEstimate(
            flops=2 * rows * weight.size, bytes_accessed=3 * 2**20, transcendentals=0
        ),
        name="project",
    )(parts, weight)


def feed_kernel(x_ref, w_ref, o_ref, acc_ref, down_ref, *, units):
    step = pl.program_id(0)
    block = w_ref.shape[0]
    both = 2 * units

    @pl.when(step == 0)
    def _():
        acc_ref[...] = jnp.zeros_like(acc_ref)

    acc_ref[...] += jnp.dot(x_ref[...], w_ref[:, 0:both], preferred_element_type=F32)
    down_ref[pl.ds(pl.multiple_of(step * block, block), block), :] = w_ref[:, both:]

    @pl.when(step == pl.num_programs(0) - 1)
    def _():
        gate = acc_ref[:, 0:units]
        up = acc_ref[:, units:both]
        hidden = (gate / (1.0 + jnp.exp(-gate)) * up).astype(BF16)
        spare = down_ref.shape[1] - units
        if spare:
            hidden = jnp.concatenate([hidden, jnp.zeros((hidden.shape[0], spare), BF16)], axis=1)
        nt = (((1,), (1,)), ((), ()))
        for c in range(o_ref.shape[1] // 256):
            at = pl.ds(c * 256, 256)
            o_ref[:, at] = lax.dot_general(
                hidden, down_ref[at, :], nt, preferred_element_type=F32
            ).astype(BF16)


def feed(x, weights, units):
    rows, depth = x.shape
    width = weights.shape[1]
    block = 256
    return pl.pallas_call(
        functools.partial(feed_kernel, units=units),
        grid=(depth // block,),
        in_specs=[
            pl.BlockSpec((rows, block), lambda i: (0, i)),
            pl.BlockSpec((block, width), lambda i: (i, 0)),
        ],
        out_specs=pl.BlockSpec((rows, depth), lambda i: (0, 0)),
        out_shape=jax.ShapeDtypeStruct((rows, depth), BF16),
        scratch_shapes=[
            pltpu.VMEM((rows, 2 * units), F32),
            pltpu.VMEM((depth, width - 2 * units), BF16),
        ],
        compiler_params=pltpu.CompilerParams(
            dimension_semantics=("arbitrary",), vmem_limit_bytes=60 * 2**20
        ),
        cost_estimate=pl.CostEstimate(
            flops=6 * rows * depth * units, bytes_accessed=10 * 2**20, transcendentals=0
        ),
        name="feed",
    )(x, weights)


def normalize(stream, gain):
    values = stream.astype(F32)
    return (
        values * lax.rsqrt(jnp.mean(values * values, axis=-1, keepdims=True) + EPSILON) * gain
    ).astype(BF16)


def summed_over_tp(x):
    share = x.shape[0] // lax.axis_size("tp")
    blocks = lax.all_to_all(x.reshape(-1, share, x.shape[1]), "tp", 0, 0, tiled=True)
    return jnp.sum(blocks.astype(F32), axis=0)


def body(
    resid,
    query,
    key,
    value,
    q_gain,
    k_gain,
    out_weight,
    norm_gain,
    gate_weight,
    up_weight,
    down_weight,
):
    rows = query.shape[0]
    units = gate_weight.shape[1]
    shard = [gate_weight, up_weight, down_weight.T]
    spare = -(3 * units) % 128
    if spare:
        shard.append(jnp.zeros((gate_weight.shape[0], spare), BF16))
    weights = lax.all_gather(jnp.concatenate(shard, axis=1), SP, axis=0, tiled=True)

    q_rot, keys_values = prep(query, key, value, q_gain, k_gain)
    queries = lax.all_gather(q_rot, "sp_1", axis=0)
    keys_values = lax.all_gather(keys_values, "sp_0", axis=0, tiled=True)
    partial = attend(queries, keys_values)
    partial = lax.all_to_all(partial, "sp_1", 0, 0, tiled=True)
    proj = summed_over_tp(project(partial, out_weight))
    share = rows // lax.axis_size("tp")
    my_resid = lax.dynamic_slice_in_dim(resid, lax.axis_index("tp") * share, share, 0)
    my_stream = (my_resid.astype(F32) + proj).astype(BF16)
    normed = lax.all_gather(normalize(my_stream, norm_gain), "tp", axis=0, tiled=True)
    down = summed_over_tp(feed(normed, weights, units))
    return (my_stream.astype(F32) + 0.5 * down).astype(BF16)


def solution(mesh):
    torus = Mesh(mesh.devices.reshape(8, 8, mesh.shape["tp"]), ("sp_0", "sp_1", "tp"))
    return jax.shard_map(
        body,
        mesh=torus,
        in_specs=(
            P(SP, None),
            P(SP, "tp"),
            P(SP, "tp"),
            P(SP, "tp"),
            P(),
            P(),
            P("tp", None),
            P(),
            P(SP, "tp"),
            P(SP, "tp"),
            P("tp", SP),
        ),
        out_specs=P(SP_TP, None),
        check_vma=False,
    )
```

time: 278 us -> 188 us (0.68)
  waiting for transfers between devices: 106 us -> 12.2 us
  blocking collectives: 48.7 us -> 118 us
  matrix products: 52.9 us -> 0 us
  local copies, waits for them, and re-layouts: 30.4 us -> 1.61 us
  Pallas kernels: 0 us -> 25.1 us
  other arithmetic: 13.5 us -> 2.02 us
  starting transfers between devices: 10.6 us -> 15.8 us
    all_gather x3 -> x1, waiting for transfers between devices: 94.1 us -> 0.01 us  [body(): lax.all_gather(jnp.concatenate(shard, axis=1), SP, axis=0, tiled=True)]
    dot_general x35 -> x0, matrix products: 52.9 us -> none  [the longest x16 22.4 us: key_block(): jnp.einsum('kgqs,skd->kgqd', weights.astype(jnp.bfloat16), block_vals, pr...]
    all_gather x1 -> x3, blocking collectives: 28.5 us -> 68.6 us  [the longest x1 28.7 us: body(): keys_values = lax.all_gather(keys_values, 'sp_0', axis=0, tiled=True)]
    all_to_all x1 -> x2, blocking collectives: 20.2 us -> 49.1 us  [the longest x1 33.4 us: body(): partial = lax.all_to_all(partial, 'sp_1', 0, 0, tiled=True)]
    pallas_call x0 -> x4, Pallas kernels: none -> 25.1 us  [the longest x1 10.1 us: attend(): pl.pallas_call(functools.partial(attend_kernel, chunk=256), grid=(parts,)...]
    split x1 -> x0, local copies, waits for them, and re-layouts: 12.6 us -> none  [sent_together(): jnp.split(whole, [sum(widths[:k]) for k in range(1, len(widths))], axis=a...]
    unnamed x11 -> x2, local copies, waits for them, and re-layouts: 11.1 us -> 0.01 us
    reduce_sum x20 -> x2, other arithmetic: 6.1 us -> 0.22 us  [summed_over_tp(): return jnp.sum(blocks.astype(F32), axis=0)]
  transfers between devices with their start and end apart: 5 -> 2, of which waited for: 3 -> 1; matrix products, arithmetic and copies ran while one was open for 31% -> 1% of each run, Pallas kernels for 0% -> 8%
where the time goes in v1:
time: 188 us
  blocking collectives  118 us (63%)
  Pallas kernels  25.1 us (13%)
  starting transfers between devices  15.8 us (8%)
  between operations  13.4 us (7%)
  waiting for transfers between devices  12.2 us (6%)
  other arithmetic  2.02 us (1%)
    all_to_all x1, blocking collectives, body(): partial = lax.all_to_all(partial, 'sp_1', 0, 0, tiled=True)  33.4 us
    all_gather x1, blocking collectives, body(): keys_values = lax.all_gather(keys_values, 'sp_0', axis=0, tiled=True)  28.7 us
    all_gather x1, blocking collectives, body(): queries = lax.all_gather(q_rot, 'sp_1', axis=0)  24.7 us
    all_to_all x1, starting transfers between devices, summed_over_tp(): lax.all_to_all(x.reshape(-1, share, x.shape[1]), 'tp', 0, 0, tiled=True)  15.8 us
    all_to_all x1, blocking collectives, summed_over_tp(): lax.all_to_all(x.reshape(-1, share, x.shape[1]), 'tp', 0, 0, tiled=True)  15.7 us
    all_gather x1, blocking collectives, body(): lax.all_gather(normalize(my_stream, norm_gain), 'tp', axis=0, tiled=True)  15.3 us
    all_to_all x1, waiting for transfers between devices, summed_over_tp(): lax.all_to_all(x.reshape(-1, share, x.shape[1]), 'tp', 0, 0, tiled=True)  12.2 us
    pallas_call x1, Pallas kernels, attend(): pl.pallas_call(functools.partial(attend_kernel, chunk=256), grid=(parts,)...  10.1 us
  transfers between devices with their start and end apart: 2, of which 1 were waited for; matrix products, arithmetic and copies ran while one was open for 1% of the time, Pallas kernels for 8%

profile of v1, /device:TPU:1, one launch (start us, length us, event | category | flops | bytes accessed | tf_op | source)
XLA Modules:
  0.0 187.9 jit_solution(4754706826510709257)
XLA Ops:
  6.5 0.0 all-gather.3.cloned.1.call-start
  6.5 1.6 concatenate.3
  8.1 0.0 all-gather.3.cloned.1.call-update
  8.2 2.6 %prep.1 = (bf16[192,256]{1,0:T(8,128)(2,1)}, bf16[192,256]{1,0:T(8,128)(2,1)}) custom-call(bf16[192,256]{1,0:T(8,128)(2,1)} %q_ref.1, bf16[192,128]{1,0:T(8,128)(2,1)} %k_ref.1, bf16[192,128]{1,0:T(8,128)(2,1)} %v_ref.1, f32[1,128]{1,0:T(1,128)} %bitcast.10, f32[1,128]{1,0:T(1,128)} %bitcast.11, f32[1,128]{1,0:T(1,128)} %constant.29.clone.inv_ref, ...), custom_call_target="tpu_custom_call" | custom-call | tf_op jit(solution)/shard_map/prep/pallas_call | solution.py:74
  10.7 28.7 %all_gather.17.kv_ref = bf16[1536,256]{1,0:T(8,128)(2,1)S(1)} all-gather(bf16[192,256]{1,0:T(8,128)(2,1)} %get-tuple-element.8), channel_id=1, replica_groups=mesh['sp_0'=8,'sp_1'=8,'tp'=8] {'sp_0'}, dimensions={0}, use_global_device_ids=true | all-gather | bytes 884736 | tf_op jit(solution)/shard_map/all_gather | solution.py:314
  39.4 24.7 %all-gather = bf16[1536,256]{1,0:T(8,128)(2,1)S(1)} all-gather(bf16[192,256]{1,0:T(8,128)(2,1)} %get-tuple-element.7), channel_id=2, replica_groups=mesh['sp_0'=8,'sp_1'=8,'tp'=8] {'sp_1'}, dimensions={0}, use_global_device_ids=true | all-gather | bytes 884736 | tf_op jit(solution)/shard_map/all_gather | solution.py:313
  64.1 10.1 %attend.1 = bf16[8,208,256]{2,1,0:T(8,128)(2,1)S(1)} custom-call(bf16[8,192,256]{2,1,0:T(8,128)(2,1)S(1)} %bitcast.6, bf16[1536,256]{1,0:T(8,128)(2,1)S(1)} %all_gather.17.kv_ref), custom_call_target="tpu_custom_call" | custom-call | flops 2415919104 | bytes 4194304 | tf_op jit(solution)/shard_map/attend/pallas_call | solution.py:156
  74.2 33.4 %all_to_all.15.part_ref = bf16[8,208,256]{2,1,0:T(8,128)(2,1)} all-to-all(bf16[8,208,256]{2,1,0:T(8,128)(2,1)S(1)} %attend.1), channel_id=1, replica_groups=mesh['sp_0'=8,'sp_1'=8,'tp'=8] {'sp_1'}, dimensions={0} | all-to-all | bytes 1703936 | tf_op jit(solution)/shard_map/all_to_all | solution.py:316
  107.5 3.2 %project.1 = bf16[192,2048]{1,0:T(8,128)(2,1)} custom-call(bf16[8,208,256]{2,1,0:T(8,128)(2,1)} %all_to_all.15.part_ref, bf16[256,2048]{1,0:T(8,128)(2,1)} %w_ref.1), custom_call_target="tpu_custom_call" | custom-call | flops 201326592 | bytes 3145728 | tf_op jit(solution)/shard_map/project/pallas_call | solution.py:213
  110.7 0.0 copy-start
  110.7 15.8 %all-to-all-start.1 = ((bf16[8,24,2048]{2,1,0:T(8,128)(2,1)}), bf16[8,24,2048]{2,1,0:T(8,128)(2,1)S(1)}, u32[]{:S(2)}, u32[]{:S(2)}) async-start(bf16[8,24,2048]{2,1,0:T(8,128)(2,1)} %bitcast.8), calls=%async_computation.1 | async-start | bytes 1572864 | tf_op jit(solution)/shard_map/all_to_all | solution.py:287
  126.5 12.2 %all-to-all-done.1 = bf16[8,24,2048]{2,1,0:T(8,128)(2,1)S(1)} async-done(((bf16[8,24,2048]{2,1,0:T(8,128)(2,1)}), bf16[8,24,2048]{2,1,0:T(8,128)(2,1)S(1)}, u32[]{:S(2)}, u32[]{:S(2)}) %all-to-all-start.1) | async-done | bytes 786464 | tf_op jit(solution)/shard_map/all_to_all | solution.py:287
  138.7 0.1 convert_reduce_fusion.1
  138.8 1.0 fusion
  139.8 0.0 copy-done
  139.8 0.1 fusion.2
  139.9 15.3 %all_gather.18.x_ref = bf16[192,2048]{1,0:T(8,128)(2,1)} all-gather(bf16[24,2048]{1,0:T(8,128)(2,1)S(1)} %fusion.2), channel_id=1, replica_groups=mesh['sp_0'=8,'sp_1'=8,'tp'=8] {'tp'}, dimensions={0}, use_global_device_ids=true | all-gather | bytes 884736 | tf_op jit(solution)/shard_map/all_gather | solution.py:321
  155.2 0.0 all-gather.3.cloned.1.call-done.w_ref
  155.2 9.3 %feed.1 = bf16[192,2048]{1,0:T(8,128)(2,1)} custom-call(bf16[192,2048]{1,0:T(8,128)(2,1)} %all_gather.18.x_ref, bf16[2048,2176]{1,0:T(8,128)(2,1)} %all-gather.3.cloned.1.call-done.w_ref), custom_call_target="tpu_custom_call" | custom-call | flops 1660944384 | bytes 10485760 | tf_op jit(solution)/shard_map/feed/pallas_call | solution.py:255
  164.5 15.7 %all_to_all.16 = bf16[8,24,2048]{2,1,0:T(8,128)(2,1)S(1)} all-to-all(bf16[8,24,2048]{2,1,0:T(8,128)(2,1)} %bitcast.7), channel_id=1, replica_groups=mesh['sp_0'=8,'sp_1'=8,'tp'=8] {'tp'}, dimensions={0} | all-to-all | bytes 1572864 | tf_op jit(solution)/shard_map/all_to_all | solution.py:287
  180.2 0.1 convert_reduce_fusion
  180.4 0.7 fusion.3
  (2 shorter events, 0.0 us)
Async XLA Ops:
  6.5 148.7 %all-gather.3.cloned.1.call-start = ((), (), s32[]{:S(2)}) async-start(), calls=%async_computation.3 | async-start | bytes 9052160 | tf_op jit(solution)/shard_map/all_gather | solution.py:310
  110.7 29.1 %copy-start = (f32[2048]{0:T(1024)S(1)}, f32[2048]{0:T(1024)}, u32[]{:S(2)}) copy-start(f32[2048]{0:T(1024)} %param.22) | copy-start | bytes 24580
  110.7 28.0 %all-to-all-start.1 = ((bf16[8,24,2048]{2,1,0:T(8,128)(2,1)}), bf16[8,24,2048]{2,1,0:T(8,128)(2,1)S(1)}, u32[]{:S(2)}, u32[]{:S(2)}) async-start(bf16[8,24,2048]{2,1,0:T(8,128)(2,1)} %bitcast.8), calls=%async_computation.1 | async-start | bytes 1572864 | tf_op jit(solution)/shard_map/all_to_all | solution.py:287
Sparse Core Ops, SparseCore 0:
  10.3 125.0 all-gather.2

commit v2 on v1

--- a/solution.py
+++ b/solution.py
@@ -63,18 +63,20 @@
         sine = jnp.where(by_row, row_sin[j : j + 1, :], sin_ref[...])
         for h in range(heads):
             cols = slice(h * head_dim, (h + 1) * head_dim)
-            qo_ref[at, cols] = turned(q_ref[at, cols], qg_ref[...], cosine, sine)
+            made = turned(q_ref[at, cols], qg_ref[...], cosine, sine)
+            for n in range(qo_ref.shape[0]):
+                qo_ref[n, at, cols] = made
         kvo_ref[at, 0:head_dim] = turned(k_ref[at, :], kg_ref[...], cosine, sine)
     kvo_ref[:, head_dim:] = v_ref[...]
 
 
-def prep(query, key, value, q_gain, k_gain):
+def prep(query, key, value, q_gain, k_gain, copies):
     rows, head_dim = key.shape
     inverse, sign, cosine, sine = rope_tables(head_dim)
     return pl.pallas_call(
         prep_kernel,
         out_shape=(
-            jax.ShapeDtypeStruct(query.shape, BF16),
+            jax.ShapeDtypeStruct((copies, *query.shape), BF16),
             jax.ShapeDtypeStruct((rows, 2 * head_dim), BF16),
         ),
         name="prep",
@@ -220,59 +222,16 @@
     )(parts, weight)
 
 
-def feed_kernel(x_ref, w_ref, o_ref, acc_ref, down_ref, *, units):
-    step = pl.program_id(0)
-    block = w_ref.shape[0]
-    both = 2 * units
-
-    @pl.when(step == 0)
-    def _():
-        acc_ref[...] = jnp.zeros_like(acc_ref)
-
-    acc_ref[...] += jnp.dot(x_ref[...], w_ref[:, 0:both], preferred_element_type=F32)
-    down_ref[pl.ds(pl.multiple_of(step * block, block), block), :] = w_ref[:, both:]
-
-    @pl.when(step == pl.num_programs(0) - 1)
-    def _():
-        gate = acc_ref[:, 0:units]
-        up = acc_ref[:, units:both]
-        hidden = (gate / (1.0 + jnp.exp(-gate)) * up).astype(BF16)
-        spare = down_ref.shape[1] - units
-        if spare:
-            hidden = jnp.concatenate([hidden, jnp.zeros((hidden.shape[0], spare), BF16)], axis=1)
-        nt = (((1,), (1,)), ((), ()))
-        for c in range(o_ref.shape[1] // 256):
-            at = pl.ds(c * 256, 256)
-            o_ref[:, at] = lax.dot_general(
-                hidden, down_ref[at, :], nt, preferred_element_type=F32
-            ).astype(BF16)
-
-
 def feed(x, weights, units):
-    rows, depth = x.shape
-    width = weights.shape[1]
-    block = 256
-    return pl.pallas_call(
-        functools.partial(feed_kernel, units=units),
-        grid=(depth // block,),
-        in_specs=[
-            pl.BlockSpec((rows, block), lambda i: (0, i)),
-            pl.BlockSpec((block, width), lambda i: (i, 0)),
-        ],
-        out_specs=pl.BlockSpec((rows, depth), lambda i: (0, 0)),
-        out_shape=jax.ShapeDtypeStruct((rows, depth), BF16),
-        scratch_shapes=[
-            pltpu.VMEM((rows, 2 * units), F32),
-            pltpu.VMEM((depth, width - 2 * units), BF16),
-        ],
-        compiler_params=pltpu.CompilerParams(
-            dimension_semantics=("arbitrary",), vmem_limit_bytes=60 * 2**20
-        ),
-        cost_estimate=pl.CostEstimate(
-            flops=6 * rows * depth * units, bytes_accessed=10 * 2**20, transcendentals=0
-        ),
-        name="feed",
-    )(x, weights)
+    gate = jnp.dot(x, weights[:, 0:units], preferred_element_type=F32)
+    up = jnp.dot(x, weights[:, units : 2 * units], preferred_element_type=F32)
+    hidden = (jax.nn.silu(gate) * up).astype(BF16)
+    return lax.dot_general(
+        hidden,
+        weights[:, 2 * units : 3 * units],
+        (((1,), (1,)), ((), ())),
+        preferred_element_type=F32,
+    ).astype(BF16)
 
 
 def normalize(stream, gain):
@@ -304,13 +263,10 @@
     rows = query.shape[0]
     units = gate_weight.shape[1]
     shard = [gate_weight, up_weight, down_weight.T]
-    spare = -(3 * units) % 128
-    if spare:
-        shard.append(jnp.zeros((gate_weight.shape[0], spare), BF16))
     weights = lax.all_gather(jnp.concatenate(shard, axis=1), SP, axis=0, tiled=True)
 
-    q_rot, keys_values = prep(query, key, value, q_gain, k_gain)
-    queries = lax.all_gather(q_rot, "sp_1", axis=0)
+    copies, keys_values = prep(query, key, value, q_gain, k_gain, lax.axis_size("sp_1"))
+    queries = lax.all_to_all(copies, "sp_1", 0, 0, tiled=True)
     keys_values = lax.all_gather(keys_values, "sp_0", axis=0, tiled=True)
     partial = attend(queries, keys_values)
     partial = lax.all_to_all(partial, "sp_1", 0, 0, tiled=True)

time: 188 us -> 164 us (0.87)
  blocking collectives: 118 us -> 84 us
  starting transfers between devices: 15.8 us -> 26 us
  Pallas kernels: 25.1 us -> 16.1 us
  matrix products: 0 us -> 7.97 us
    all_gather x1 -> x0, blocking collectives: 24.7 us -> none  [body(): queries = lax.all_gather(q_rot, 'sp_1', axis=0)]
    pallas_call x2 -> x1, Pallas kernels: 11.9 us -> 2.84 us  [prep(): pl.pallas_call(prep_kernel, out_shape=(jax.ShapeDtypeStruct((copies, *que...]
    dot_general x0 -> x2, matrix products: none -> 7.97 us  [the longest x1 5.27 us: feed(): lax.dot_general(hidden, weights[:, 2 * units:3 * units], (((1,), (1,)), (...]
    all_to_all x0 -> x1, starting transfers between devices: none -> 7.64 us  [body(): queries = lax.all_to_all(copies, 'sp_1', 0, 0, tiled=True)]
    all_to_all x1, blocking collectives: 33.4 us -> 26.1 us  [body(): partial = lax.all_to_all(partial, 'sp_1', 0, 0, tiled=True)]
    all_to_all x1, starting transfers between devices: 15.8 us -> 18.3 us  [summed_over_tp(): lax.all_to_all(x.reshape(-1, share, x.shape[1]), 'tp', 0, 0, tiled=True)]
  transfers between devices with their start and end apart: 2 -> 3, of which waited for: 1 -> 1; matrix products, arithmetic and copies ran while one was open for 1% -> 1% of each run, Pallas kernels for 8% -> 10%
where the time goes in v2:
time: 164 us; the launch traced here: 163 us
  blocking collectives  84 us (51%)
  starting transfers between devices  26 us (16%)
  Pallas kernels  16.1 us (10%)
  between operations  13.4 us (8%)
  waiting for transfers between devices  12.2 us (7%)
  matrix products  7.97 us (5%)
  other arithmetic  2.04 us (1%)
    all_gather x1, blocking collectives, body(): keys_values = lax.all_gather(keys_values, 'sp_0', axis=0, tiled=True)  28.9 us
    all_to_all x1, blocking collectives, body(): partial = lax.all_to_all(partial, 'sp_1', 0, 0, tiled=True)  26.1 us
    all_to_all x1, starting transfers between devices, summed_over_tp(): lax.all_to_all(x.reshape(-1, share, x.shape[1]), 'tp', 0, 0, tiled=True)  18.3 us
    all_to_all x1, blocking collectives, summed_over_tp(): lax.all_to_all(x.reshape(-1, share, x.shape[1]), 'tp', 0, 0, tiled=True)  14.8 us
    all_gather x1, blocking collectives, body(): lax.all_gather(normalize(my_stream, norm_gain), 'tp', axis=0, tiled=True)  14.2 us
    all_to_all x1, waiting for transfers between devices, summed_over_tp(): lax.all_to_all(x.reshape(-1, share, x.shape[1]), 'tp', 0, 0, tiled=True)  12.2 us
    pallas_call x1, Pallas kernels, attend(): pl.pallas_call(functools.partial(attend_kernel, chunk=256), grid=(parts,)...  10.1 us
    all_to_all x1, starting transfers between devices, body(): queries = lax.all_to_all(copies, 'sp_1', 0, 0, tiled=True)  7.64 us
  transfers between devices with their start and end apart: 3, of which 1 were waited for; matrix products, arithmetic and copies ran while one was open for 1% of the time, Pallas kernels for 10%

profile of v2, /device:TPU:1, one launch (start us, length us, event | category | flops | bytes accessed | tf_op | source)
XLA Modules:
  0.0 163.3 jit_solution(5693358035113802008)
XLA Ops:
  6.5 0.0 all-gather.2.cloned.1.call-start
  6.5 1.6 concatenate.3
  8.1 0.0 all-gather.2.cloned.1.call-update
  8.2 2.8 %prep.1 = (bf16[8,192,256]{2,1,0:T(8,128)(2,1)}, bf16[192,256]{1,0:T(8,128)(2,1)}) custom-call(bf16[192,256]{1,0:T(8,128)(2,1)} %q_ref.1, bf16[192,128]{1,0:T(8,128)(2,1)} %k_ref.1, bf16[192,128]{1,0:T(8,128)(2,1)} %v_ref.1, f32[1,128]{1,0:T(1,128)} %bitcast.10, f32[1,128]{1,0:T(1,128)} %bitcast.11, f32[1,128]{1,0:T(1,128)} %constant.30.clone.inv_ref, ...), custom_call_target="tpu_custom_call" | custom-call | tf_op jit(solution)/shard_map/prep/pallas_call | solution.py:76
  11.0 7.6 %all-to-all-start = ((bf16[8,192,256]{2,1,0:T(8,128)(2,1)}), bf16[8,192,256]{2,1,0:T(8,128)(2,1)S(1)}, u32[]{:S(2)}, u32[]{:S(2)}) async-start(bf16[8,192,256]{2,1,0:T(8,128)(2,1)} %get-tuple-element.7), calls=%async_computation | async-start | bytes 1572864 | tf_op jit(solution)/shard_map/all_to_all | solution.py:269
  18.6 28.9 %all_gather.9.kv_ref = bf16[1536,256]{1,0:T(8,128)(2,1)S(1)} all-gather(bf16[192,256]{1,0:T(8,128)(2,1)} %get-tuple-element.8), channel_id=1, replica_groups=mesh['sp_0'=8,'sp_1'=8,'tp'=8] {'sp_0'}, dimensions={0}, use_global_device_ids=true | all-gather | bytes 884736 | tf_op jit(solution)/shard_map/all_gather | solution.py:270
  47.5 0.0 all-to-all-done.q_ref
  47.6 10.1 %attend.1 = bf16[8,208,256]{2,1,0:T(8,128)(2,1)S(1)} custom-call(bf16[8,192,256]{2,1,0:T(8,128)(2,1)S(1)} %all-to-all-done.q_ref, bf16[1536,256]{1,0:T(8,128)(2,1)S(1)} %all_gather.9.kv_ref), custom_call_target="tpu_custom_call" | custom-call | flops 2415919104 | bytes 4194304 | tf_op jit(solution)/shard_map/attend/pallas_call | solution.py:158
  57.6 26.1 %all_to_all.20.part_ref = bf16[8,208,256]{2,1,0:T(8,128)(2,1)} all-to-all(bf16[8,208,256]{2,1,0:T(8,128)(2,1)S(1)} %attend.1), channel_id=1, replica_groups=mesh['sp_0'=8,'sp_1'=8,'tp'=8] {'sp_1'}, dimensions={0} | all-to-all | bytes 1703936 | tf_op jit(solution)/shard_map/all_to_all | solution.py:272
  83.7 0.0 copy-start
  83.7 3.2 %project.1 = bf16[192,2048]{1,0:T(8,128)(2,1)} custom-call(bf16[8,208,256]{2,1,0:T(8,128)(2,1)} %all_to_all.20.part_ref, bf16[256,2048]{1,0:T(8,128)(2,1)} %w_ref.1), custom_call_target="tpu_custom_call" | custom-call | flops 201326592 | bytes 3145728 | tf_op jit(solution)/shard_map/project/pallas_call | solution.py:215
  86.9 18.3 %all-to-all-start.2 = ((bf16[8,24,2048]{2,1,0:T(8,128)(2,1)}), bf16[8,24,2048]{2,1,0:T(8,128)(2,1)S(1)}, u32[]{:S(2)}, u32[]{:S(2)}) async-start(bf16[8,24,2048]{2,1,0:T(8,128)(2,1)} %bitcast.7), calls=%async_computation.2 | async-start | bytes 1572864 | tf_op jit(solution)/shard_map/all_to_all | solution.py:246
  105.2 12.2 %all-to-all-done.2 = bf16[8,24,2048]{2,1,0:T(8,128)(2,1)S(1)} async-done(((bf16[8,24,2048]{2,1,0:T(8,128)(2,1)}), bf16[8,24,2048]{2,1,0:T(8,128)(2,1)S(1)}, u32[]{:S(2)}, u32[]{:S(2)}) %all-to-all-start.2) | async-done | bytes 786464 | tf_op jit(solution)/shard_map/all_to_all | solution.py:246
  117.4 0.1 convert_reduce_fusion.1
  117.5 1.0 fusion.23
  118.6 0.0 copy-done
  118.6 0.1 fusion.25
  118.7 14.2 %all_gather.10 = bf16[192,2048]{1,0:T(8,128)(2,1)S(1)} all-gather(bf16[24,2048]{1,0:T(8,128)(2,1)S(1)} %fusion.25), channel_id=1, replica_groups=mesh['sp_0'=8,'sp_1'=8,'tp'=8] {'tp'}, dimensions={0}, use_global_device_ids=true | all-gather | bytes 884736 | tf_op jit(solution)/shard_map/all_gather | solution.py:277
  132.9 0.0 all-gather.2.cloned.1.call-done
  132.9 2.7 %fusion.4 = f32[192,704]{1,0:T(8,128)S(1)} fusion(bf16[192,2048]{1,0:T(8,128)(2,1)S(1)} %all_gather.10, bf16[2048,2112]{1,0:T(8,128)(2,1)} %all-gather.2.cloned.1.call-done), kind=kOutput, calls=%fused_computation.4 | convolution fusion | flops 553648128 | bytes 4472832 | tf_op jit(solution)/shard_map/dot_general | solution.py:226
  135.6 5.3 %fusion.6 = bf16[192,2048]{1,0:T(8,128)(2,1)S(1)} fusion(bf16[2048,2112]{1,0:T(8,128)(2,1)} %all-gather.2.cloned.1.call-done, bf16[192,2048]{1,0:T(8,128)(2,1)S(1)} %all_gather.10, f32[192,704]{1,0:T(8,128)S(1)} %fusion.4), kind=kOutput, calls=%fused_computation.6 | convolution fusion | flops 1108500480 | bytes 8404992 | tf_op jit(solution)/shard_map/dot_general | solution.py:229
  140.8 14.8 %all_to_all.21 = bf16[8,24,2048]{2,1,0:T(8,128)(2,1)S(1)} all-to-all(bf16[8,24,2048]{2,1,0:T(8,128)(2,1)S(1)} %bitcast.8), channel_id=1, replica_groups=mesh['sp_0'=8,'sp_1'=8,'tp'=8] {'tp'}, dimensions={0} | all-to-all | bytes 1572864 | tf_op jit(solution)/shard_map/all_to_all | solution.py:246
  155.7 0.1 convert_reduce_fusion
  155.8 0.7 fusion.26
  (1 shorter events, 0.0 us)
Async XLA Ops:
  6.5 126.3 %all-gather.2.cloned.1.call-start = ((), (), s32[]{:S(2)}) async-start(), calls=%async_computation.4 | async-start | bytes 9052160 | tf_op jit(solution)/shard_map/all_gather | solution.py:266
  11.0 36.5 %all-to-all-start = ((bf16[8,192,256]{2,1,0:T(8,128)(2,1)}), bf16[8,192,256]{2,1,0:T(8,128)(2,1)S(1)}, u32[]{:S(2)}, u32[]{:S(2)}) async-start(bf16[8,192,256]{2,1,0:T(8,128)(2,1)} %get-tuple-element.7), calls=%async_computation | async-start | bytes 1572864 | tf_op jit(solution)/shard_map/all_to_all | solution.py:269
  83.7 34.8 %copy-start = (f32[2048]{0:T(1024)S(1)}, f32[2048]{0:T(1024)}, u32[]{:S(2)}) copy-start(f32[2048]{0:T(1024)} %param.22) | copy-start | bytes 24580
  86.9 30.5 %all-to-all-start.2 = ((bf16[8,24,2048]{2,1,0:T(8,128)(2,1)}), bf16[8,24,2048]{2,1,0:T(8,128)(2,1)S(1)}, u32[]{:S(2)}, u32[]{:S(2)}) async-start(bf16[8,24,2048]{2,1,0:T(8,128)(2,1)} %bitcast.7), calls=%async_computation.2 | async-start | bytes 1572864 | tf_op jit(solution)/shard_map/all_to_all | solution.py:246
Sparse Core Ops, SparseCore 0:
  10.3 117.8 all-gather.1

commit v3 on v2

--- a/solution.py
+++ b/solution.py
@@ -101,93 +101,118 @@
     return a, b, c
 
 
-def attend_kernel(q_ref, kv_ref, o_ref, s_ref, *, chunk):
-    rows, width = q_ref.shape[1:]
-    keys = kv_ref.shape[0]
-    head_dim = kv_ref.shape[1] // 2
-    heads = width // head_dim
-    factor = head_dim ** (-0.5) * LOG2E
-    nt = (((1,), (1,)), ((), ()))
+def packed_stats(level):
+    rows = level.shape[0]
     eye = (
         lax.broadcasted_iota(jnp.int32, (128, 128), 0)
         == lax.broadcasted_iota(jnp.int32, (128, 128), 1)
     )
-    stat = jnp.zeros((STAT_ROWS, 128), F32)
-    srow = lax.broadcasted_iota(jnp.int32, (STAT_ROWS, 128), 0)
-    for h in range(heads):
-        cols = slice(h * head_dim, (h + 1) * head_dim)
-        q = q_ref[0, :, cols]
-        peak = jnp.full((rows, 128), -jnp.inf, F32)
-        for c in range(keys // chunk):
-            at = pl.ds(c * chunk, chunk)
-            s = lax.dot_general(q, kv_ref[at, 0:head_dim], nt, preferred_element_type=F32)
-            s_ref[h, :, at] = s
-            for u in range(chunk // 128):
-                peak = jnp.maximum(peak, s[:, u * 128 : (u + 1) * 128])
+    place = lax.broadcasted_iota(jnp.int32, (STAT_ROWS, 128), 0)
+    out = jnp.zeros((STAT_ROWS, 128), F32)
+    for t in range(-(-rows // 128)):
+        n = min(128, rows - t * 128)
+        spread = jnp.broadcast_to(level[t * 128 : t * 128 + n], (n, 128))
+        flat = jnp.sum(jnp.where(eye[:n], spread, 0.0), axis=0, keepdims=True)
+        for k, piece in enumerate(split3(flat)):
+            out = jnp.where(place == 3 * t + k, piece.astype(F32), out)
+    return out.astype(BF16)
+
+
+def attend_kernel(q_ref, next_ref, kv_ref, o_ref, even_ref, odd_ref, top_ref, *, chunk):
+    rows, head_dim = q_ref.shape[1:]
+    count = kv_ref.shape[0] // chunk
+    factor = head_dim ** (-0.5) * LOG2E
+
+    def score(q, s_ref, c, peak):
+        at = pl.ds(c * chunk, chunk)
+        s = lax.dot_general(
+            q, kv_ref[at, 0:head_dim], (((1,), (1,)), ((), ())), preferred_element_type=F32
+        )
+        s_ref[:, at] = s
+        for u in range(chunk // 128):
+            x = s[:, u * 128 : (u + 1) * 128]
+            peak = x if peak is None else jnp.maximum(peak, x)
+        return peak
+
+    def weigh(s_ref, top, c, total, accum):
+        at = pl.ds(c * chunk, chunk)
+        w = jnp.exp2((s_ref[:, at] - top) * factor)
+        for u in range(chunk // 128):
+            x = w[:, u * 128 : (u + 1) * 128]
+            total = x if total is None else total + x
+        d = jnp.dot(w.astype(BF16), kv_ref[at, head_dim:], preferred_element_type=F32)
+        return total, d if accum is None else accum + d
+
+    def finish(b, top, total, accum):
+        whole = jnp.sum(total, axis=-1, keepdims=True)
+        o_ref[b, 0:rows, :] = (accum / whole).astype(BF16)
+        o_ref[b, rows:, :] = packed_stats(top * factor + jnp.log2(whole))
+
+    @pl.when(pl.program_id(0) == 0)
+    def _():
+        peak = None
+        for c in range(count):
+            peak = score(q_ref[0], even_ref, c, peak)
+        top_ref[...] = jnp.broadcast_to(jnp.max(peak, axis=-1, keepdims=True), top_ref.shape)
+
+    top = top_ref[:, 0:1]
+    for b, (q, s_ref, done_ref) in enumerate(
+        ((q_ref[1], odd_ref, even_ref), (next_ref[0], even_ref, odd_ref))
+    ):
+        peak = total = accum = None
+        for c in range(count):
+            peak = score(q, s_ref, c, peak)
+            total, accum = weigh(done_ref, top, c, total, accum)
+        finish(b, top, total, accum)
         top = jnp.max(peak, axis=-1, keepdims=True)
-        total = jnp.zeros((rows, 128), F32)
-        accum = jnp.zeros((rows, head_dim), F32)
-        for c in range(keys // chunk):
-            at = pl.ds(c * chunk, chunk)
-            w = jnp.exp2((s_ref[h, :, at] - top) * factor)
-            for u in range(chunk // 128):
-                total = total + w[:, u * 128 : (u + 1) * 128]
-            accum = accum + jnp.dot(
-                w.astype(BF16), kv_ref[at, head_dim:], preferred_element_type=F32
-            )
-        whole = jnp.sum(total, axis=-1, keepdims=True)
-        o_ref[0, 0:rows, cols] = (accum / whole).astype(BF16)
-        level = top * factor + jnp.log2(whole)
-        out = jnp.zeros((STAT_ROWS, 128), F32)
-        for t in range(-(-rows // 128)):
-            n = min(128, rows - t * 128)
-            spread = jnp.broadcast_to(level[t * 128 : t * 128 + n], (n, 128))
-            flat = jnp.sum(jnp.where(eye[:n], spread, 0.0), axis=0, keepdims=True)
-            a, b, c = split3(flat)
-            for k, piece in enumerate((a, b, c)):
-                out = jnp.where(srow == 3 * t + k, piece.astype(F32), out)
-        o_ref[0, rows:, cols] = out.astype(BF16)
-
-
-def attend(queries, keys_values):
-    parts, rows, width = queries.shape
+    top_ref[...] = jnp.broadcast_to(top, top_ref.shape)
+
+
+def attend(queries, keys_values, head):
+    parts, rows, _ = queries.shape
     keys = keys_values.shape[0]
     head_dim = keys_values.shape[1] // 2
-    heads = width // head_dim
-    work = parts * heads * rows * keys
+    steps = parts // 2
+    work = parts * rows * keys
     return pl.pallas_call(
-        functools.partial(attend_kernel, chunk=256),
-        grid=(parts,),
+        functools.partial(attend_kernel, chunk=next(n for n in (512, 384, 256, 128) if keys % n == 0)),
+        grid=(steps,),
         in_specs=[
-            pl.BlockSpec((1, rows, width), lambda i: (i, 0, 0)),
+            pl.BlockSpec((2, rows, head_dim), lambda i: (i, 0, head)),
+            pl.BlockSpec(
+                (2, rows, head_dim), lambda i: (jnp.minimum(i + 1, steps - 1), 0, head)
+            ),
             pl.BlockSpec((keys, 2 * head_dim), lambda i: (0, 0)),
         ],
-        out_specs=pl.BlockSpec((1, rows + STAT_ROWS, width), lambda i: (i, 0, 0)),
-        out_shape=jax.ShapeDtypeStruct((parts, rows + STAT_ROWS, width), BF16),
-        scratch_shapes=[pltpu.VMEM((heads, rows, keys), F32)],
+        out_specs=pl.BlockSpec((2, rows + STAT_ROWS, head_dim), lambda i: (i, 0, 0)),
+        out_shape=jax.ShapeDtypeStruct((parts, rows + STAT_ROWS, head_dim), BF16),
+        scratch_shapes=[
+            pltpu.VMEM((rows, keys), F32),
+            pltpu.VMEM((rows, keys), F32),
+            pltpu.VMEM((rows, 128), F32),
+        ],
         compiler_params=pltpu.CompilerParams(
             dimension_semantics=("arbitrary",), vmem_limit_bytes=32 * 2**20
         ),
         cost_estimate=pl.CostEstimate(
-            flops=4 * work * head_dim, bytes_accessed=4 * 2**20, transcendentals=work
-        ),
-        name="attend",
-    )(queries, keys_values)
-
-
-def project_kernel(part_ref, w_ref, o_ref):
-    parts, all_rows, width = part_ref.shape
+            flops=4 * work * head_dim, bytes_accessed=2 * 2**20, transcendentals=work
+        ),
+        name=f"attend{head}",
+    )(queries, queries, keys_values)
+
+
+def project_kernel(*refs):
+    *part_refs, w_ref, o_ref = refs
+    parts, all_rows, head_dim = part_refs[0].shape
     rows = all_rows - STAT_ROWS
-    head_dim = 128
     eye = (
         lax.broadcasted_iota(jnp.int32, (128, 128), 0)
         == lax.broadcasted_iota(jnp.int32, (128, 128), 1)
     )
     pieces = []
-    for h in range(width // head_dim):
-        cols = slice(h * head_dim, (h + 1) * head_dim)
+    for part_ref in part_refs:
         outs = []
-        stats = [part_ref[p, rows:, cols].astype(F32) for p in range(parts)]
+        stats = [part_ref[p, rows:, :].astype(F32) for p in range(parts)]
         for t in range(-(-rows // 128)):
             n = min(128, rows - t * 128)
             levels = [
@@ -201,7 +226,7 @@
             for p in range(parts):
                 flat = jnp.broadcast_to(shares[p] / whole, (n, 128))
                 share = jnp.sum(jnp.where(eye[:n], flat, 0.0), axis=1, keepdims=True)
-                total = total + share * part_ref[p, t * 128 : t * 128 + n, cols].astype(F32)
+                total = total + share * part_ref[p, t * 128 : t * 128 + n, :].astype(F32)
             outs.append(total.astype(BF16))
         pieces.append(jnp.concatenate(outs, axis=0))
     attn = jnp.concatenate(pieces, axis=1)
@@ -211,7 +236,7 @@
 
 
 def project(parts, weight):
-    rows = parts.shape[1] - STAT_ROWS
+    rows = parts[0].shape[1] - STAT_ROWS
     return pl.pallas_call(
         project_kernel,
         out_shape=jax.ShapeDtypeStruct((rows, weight.shape[1]), BF16),
@@ -219,19 +244,59 @@
             flops=2 * rows * weight.size, bytes_accessed=3 * 2**20, transcendentals=0
         ),
         name="project",
-    )(parts, weight)
+    )(*parts, weight)
+
+
+def feed_kernel(x_ref, w_hbm, o_ref, w_ref, acc_ref, sems, *, units):
+    depth, width = w_ref.shape
+    pieces = sems.shape[0]
+    block = depth // pieces
+    both = 2 * units
+    spare = width - 3 * units
+    copies = []
+    for i in range(pieces):
+        at = pl.ds(i * block, block)
+        copies.append(pltpu.make_async_copy(w_hbm.at[at], w_ref.at[at], sems.at[i]))
+        copies[-1].start()
+    for i in range(pieces):
+        at = pl.ds(i * block, block)
+        copies[i].wait()
+        part = jnp.dot(x_ref[:, at], w_ref[at, 0:both], preferred_element_type=F32)
+        acc_ref[...] = part if i == 0 else acc_ref[...] + part
+    gate = acc_ref[:, 0:units]
+    up = acc_ref[:, units:both]
+    hidden = (gate / (1.0 + jnp.exp(-gate)) * up).astype(BF16)
+    if spare:
+        hidden = jnp.concatenate([hidden, jnp.zeros((hidden.shape[0], spare), BF16)], axis=1)
+    nt = (((1,), (1,)), ((), ()))
+    for i in range(depth // 256):
+        at = pl.ds(i * 256, 256)
+        o_ref[:, at] = lax.dot_general(
+            hidden, w_ref[at, both:], nt, preferred_element_type=F32
+        ).astype(BF16)
 
 
 def feed(x, weights, units):
-    gate = jnp.dot(x, weights[:, 0:units], preferred_element_type=F32)
-    up = jnp.dot(x, weights[:, units : 2 * units], preferred_element_type=F32)
-    hidden = (jax.nn.silu(gate) * up).astype(BF16)
-    return lax.dot_general(
-        hidden,
-        weights[:, 2 * units : 3 * units],
-        (((1,), (1,)), ((), ())),
-        preferred_element_type=F32,
-    ).astype(BF16)
+    rows, depth = x.shape
+    width = weights.shape[1]
+    pieces = 8
+    vmem = pl.BlockSpec(memory_space=pltpu.VMEM)
+    return pl.pallas_call(
+        functools.partial(feed_kernel, units=units),
+        in_specs=[vmem, pl.BlockSpec(memory_space=pl.ANY)],
+        out_specs=vmem,
+        out_shape=jax.ShapeDtypeStruct((rows, depth), BF16),
+        scratch_shapes=[
+            pltpu.VMEM((depth, width), BF16),
+            pltpu.VMEM((rows, 2 * units), F32),
+            pltpu.SemaphoreType.DMA((pieces,)),
+        ],
+        compiler_params=pltpu.CompilerParams(vmem_limit_bytes=60 * 2**20),
+        cost_estimate=pl.CostEstimate(
+            flops=6 * rows * depth * units, bytes_accessed=10 * 2**20, transcendentals=0
+        ),
+        name="feed",
+    )(x, weights)
 
 
 def normalize(stream, gain):
@@ -263,14 +328,19 @@
     rows = query.shape[0]
     units = gate_weight.shape[1]
     shard = [gate_weight, up_weight, down_weight.T]
+    spare = -(3 * units) % 128
+    if spare:
+        shard.append(jnp.zeros((gate_weight.shape[0], spare), BF16))
     weights = lax.all_gather(jnp.concatenate(shard, axis=1), SP, axis=0, tiled=True)
 
     copies, keys_values = prep(query, key, value, q_gain, k_gain, lax.axis_size("sp_1"))
     queries = lax.all_to_all(copies, "sp_1", 0, 0, tiled=True)
     keys_values = lax.all_gather(keys_values, "sp_0", axis=0, tiled=True)
-    partial = attend(queries, keys_values)
-    partial = lax.all_to_all(partial, "sp_1", 0, 0, tiled=True)
-    proj = summed_over_tp(project(partial, out_weight))
+    partials = [
+        lax.all_to_all(attend(queries, keys_values, h), "sp_1", 0, 0, tiled=True)
+        for h in range(query.shape[1] // key.shape[1])
+    ]
+    proj = summed_over_tp(project(partials, out_weight))
     share = rows // lax.axis_size("tp")
     my_resid = lax.dynamic_slice_in_dim(resid, lax.axis_index("tp") * share, share, 0)
     my_stream = (my_resid.astype(F32) + proj).astype(BF16)

time: 164 us -> 165 us (level)
  matrix products: 7.97 us -> 0 us
  Pallas kernels: 16.1 us -> 22.8 us
  waiting for transfers between devices: 12.2 us -> 18.9 us
  blocking collectives: 84 us -> 78.9 us
    dot_general x2 -> x0, matrix products: 7.97 us -> none  [the longest x1 5.27 us: feed(): lax.dot_general(hidden, weights[:, 2 * units:3 * units], (((1,), (1,)), (...]
    all_to_all x0 -> x1, waiting for transfers between devices: none -> 6.71 us  [body(): lax.all_to_all(attend(queries, keys_values, h), 'sp_1', 0, 0, tiled=True)]
    pallas_call x1 -> x3, Pallas kernels: 10.1 us -> 16.7 us  [the longest x2 9.62 us: attend(): pl.pallas_call(functools.partial(attend_kernel, chunk=next((n for n in (5...]
    all_to_all x1, blocking collectives: 26.1 us -> 19.6 us  [body(): lax.all_to_all(attend(queries, keys_values, h), 'sp_1', 0, 0, tiled=True)]
    all_to_all x0 -> x1, starting transfers between devices: none -> 6.41 us  [body(): lax.all_to_all(attend(queries, keys_values, h), 'sp_1', 0, 0, tiled=True)]
    all_to_all x1, starting transfers between devices: 18.3 us -> 12.6 us  [summed_over_tp(): lax.all_to_all(x.reshape(-1, share, x.shape[1]), 'tp', 0, 0, tiled=True)]
  transfers between devices with their start and end apart: 3 -> 4, of which waited for: 1 -> 2; matrix products, arithmetic and copies ran while one was open for 1% -> 1% of each run, Pallas kernels for 10% -> 10%
where the time goes in v3:
time: 165 us
  blocking collectives  78.9 us (48%)
  starting transfers between devices  26.8 us (16%)
  Pallas kernels  22.8 us (14%)
  waiting for transfers between devices  18.9 us (11%)
  between operations  13.4 us (8%)
  other arithmetic  2.02 us (1%)
    all_gather x1, blocking collectives, body(): keys_values = lax.all_gather(keys_values, 'sp_0', axis=0, tiled=True)  28.3 us
    all_to_all x1, blocking collectives, body(): lax.all_to_all(attend(queries, keys_values, h), 'sp_1', 0, 0, tiled=True)  19.6 us
    all_to_all x1, blocking collectives, summed_over_tp(): lax.all_to_all(x.reshape(-1, share, x.shape[1]), 'tp', 0, 0, tiled=True)  15.7 us
    all_gather x1, blocking collectives, body(): lax.all_gather(normalize(my_stream, norm_gain), 'tp', axis=0, tiled=True)  15.3 us
    all_to_all x1, starting transfers between devices, summed_over_tp(): lax.all_to_all(x.reshape(-1, share, x.shape[1]), 'tp', 0, 0, tiled=True)  12.6 us
    all_to_all x1, waiting for transfers between devices, summed_over_tp(): lax.all_to_all(x.reshape(-1, share, x.shape[1]), 'tp', 0, 0, tiled=True)  12.2 us
    pallas_call x2, Pallas kernels, attend(): pl.pallas_call(functools.partial(attend_kernel, chunk=next((n for n in (5...  9.62 us
    all_to_all x1, starting transfers between devices, body(): queries = lax.all_to_all(copies, 'sp_1', 0, 0, tiled=True)  7.77 us
  transfers between devices with their start and end apart: 4, of which 2 were waited for; matrix products, arithmetic and copies ran while one was open for 1% of the time, Pallas kernels for 10%

profile of v3, /device:TPU:1, one launch (start us, length us, event | category | flops | bytes accessed | tf_op | source)
XLA Modules:
  0.0 164.5 jit_solution(1013673395677743238)
XLA Ops:
  6.5 0.0 all-gather.2.cloned.1.call-start
  6.5 1.6 concatenate.3
  8.2 0.0 all-gather.2.cloned.1.call-update
  8.2 2.8 %prep.1 = (bf16[8,192,256]{2,1,0:T(8,128)(2,1)}, bf16[192,256]{1,0:T(8,128)(2,1)}) custom-call(bf16[192,256]{1,0:T(8,128)(2,1)} %q_ref.1, bf16[192,128]{1,0:T(8,128)(2,1)} %k_ref.1, bf16[192,128]{1,0:T(8,128)(2,1)} %v_ref.1, f32[1,128]{1,0:T(1,128)} %bitcast.8, f32[1,128]{1,0:T(1,128)} %bitcast.9, f32[1,128]{1,0:T(1,128)} %constant.29.clone.inv_ref, ...), custom_call_target="tpu_custom_call" | custom-call | tf_op jit(solution)/shard_map/prep/pallas_call | solution.py:76
  11.0 0.0 copy-start.1
  11.0 7.8 %all-to-all-start = ((bf16[8,192,256]{2,1,0:T(8,128)(2,1)}), bf16[8,192,256]{2,1,0:T(8,128)(2,1)S(1)}, u32[]{:S(2)}, u32[]{:S(2)}) async-start(bf16[8,192,256]{2,1,0:T(8,128)(2,1)} %get-tuple-element.7), calls=%async_computation | async-start | bytes 1572864 | tf_op jit(solution)/shard_map/all_to_all | solution.py:337
  18.8 0.0 copy-done.1
  18.8 28.3 %all_gather.9.kv_ref = bf16[1536,256]{1,0:T(8,128)(2,1)S(1)} all-gather(bf16[192,256]{1,0:T(8,128)(2,1)S(1)} %copy-done.1), channel_id=1, replica_groups=mesh['sp_0'=8,'sp_1'=8,'tp'=8] {'sp_0'}, dimensions={0}, use_global_device_ids=true | all-gather | bytes 884736 | tf_op jit(solution)/shard_map/all_gather | solution.py:338
  47.1 0.0 all-to-all-done.q_ref.next_ref
  47.1 5.2 %attend1.1 = bf16[8,208,128]{2,1,0:T(8,128)(2,1)} custom-call(bf16[8,192,256]{2,1,0:T(8,128)(2,1)S(1)} %all-to-all-done.q_ref.next_ref, bf16[8,192,256]{2,1,0:T(8,128)(2,1)S(1)} %all-to-all-done.q_ref.next_ref, bf16[1536,256]{1,0:T(8,128)(2,1)S(1)} %all_gather.9.kv_ref), custom_call_target="tpu_custom_call" | custom-call | flops 1207959552 | bytes 2097152 | tf_op jit(solution)/shard_map/attend1/pallas_call | solution.py:177
  52.3 6.4 %all-to-all-start.2 = ((bf16[8,208,128]{2,1,0:T(8,128)(2,1)}), bf16[8,208,128]{2,1,0:T(8,128)(2,1)S(1)}, u32[]{:S(2)}, u32[]{:S(2)}) async-start(bf16[8,208,128]{2,1,0:T(8,128)(2,1)} %attend1.1), calls=%async_computation.2 | async-start | bytes 851968 | tf_op jit(solution)/shard_map/all_to_all | solution.py:340
  58.7 4.5 %attend0.1 = bf16[8,208,128]{2,1,0:T(8,128)(2,1)S(1)} custom-call(bf16[8,192,256]{2,1,0:T(8,128)(2,1)S(1)} %all-to-all-done.q_ref.next_ref, bf16[8,192,256]{2,1,0:T(8,128)(2,1)S(1)} %all-to-all-done.q_ref.next_ref, bf16[1536,256]{1,0:T(8,128)(2,1)S(1)} %all_gather.9.kv_ref), custom_call_target="tpu_custom_call" | custom-call | flops 1207959552 | bytes 2097152 | tf_op jit(solution)/shard_map/attend0/pallas_call | solution.py:177
  63.1 6.7 %all-to-all-done.2.refs_1_ = bf16[8,208,128]{2,1,0:T(8,128)(2,1)S(1)} async-done(((bf16[8,208,128]{2,1,0:T(8,128)(2,1)}), bf16[8,208,128]{2,1,0:T(8,128)(2,1)S(1)}, u32[]{:S(2)}, u32[]{:S(2)}) %all-to-all-start.2) | async-done | bytes 426016 | tf_op jit(solution)/shard_map/all_to_all | solution.py:340
  69.9 0.0 copy-start
  69.9 19.6 %all_to_all.25.refs_0_ = bf16[8,208,128]{2,1,0:T(8,128)(2,1)} all-to-all(bf16[8,208,128]{2,1,0:T(8,128)(2,1)S(1)} %attend0.1), channel_id=1, replica_groups=mesh['sp_0'=8,'sp_1'=8,'tp'=8] {'sp_1'}, dimensions={0} | all-to-all | bytes 851968 | tf_op jit(solution)/shard_map/all_to_all | solution.py:340
  89.4 0.0 copy-done
  89.4 3.3 %project.1 = bf16[192,2048]{1,0:T(8,128)(2,1)} custom-call(bf16[8,208,128]{2,1,0:T(8,128)(2,1)} %all_to_all.25.refs_0_, bf16[8,208,128]{2,1,0:T(8,128)(2,1)} %copy-done, bf16[256,2048]{1,0:T(8,128)(2,1)} %refs_2_.1), custom_call_target="tpu_custom_call" | custom-call | flops 201326592 | bytes 3145728 | tf_op jit(solution)/shard_map/project/pallas_call | solution.py:240
  92.8 0.0 copy-start.2
  92.8 12.6 %all-to-all-start.3 = ((bf16[8,24,2048]{2,1,0:T(8,128)(2,1)}), bf16[8,24,2048]{2,1,0:T(8,128)(2,1)S(1)}, u32[]{:S(2)}, u32[]{:S(2)}) async-start(bf16[8,24,2048]{2,1,0:T(8,128)(2,1)} %bitcast.6), calls=%async_computation.3 | async-start | bytes 1572864 | tf_op jit(solution)/shard_map/all_to_all | solution.py:311
  105.4 12.2 %all-to-all-done.3 = bf16[8,24,2048]{2,1,0:T(8,128)(2,1)S(1)} async-done(((bf16[8,24,2048]{2,1,0:T(8,128)(2,1)}), bf16[8,24,2048]{2,1,0:T(8,128)(2,1)S(1)}, u32[]{:S(2)}, u32[]{:S(2)}) %all-to-all-start.3) | async-done | bytes 786464 | tf_op jit(solution)/shard_map/all_to_all | solution.py:311
  117.6 0.1 convert_reduce_fusion.1
  117.7 1.0 fusion
  118.7 0.0 copy-done.2
  118.7 0.1 fusion.2
  118.8 15.3 %all_gather.10.x_ref = bf16[192,2048]{1,0:T(8,128)(2,1)} all-gather(bf16[24,2048]{1,0:T(8,128)(2,1)S(1)} %fusion.2), channel_id=1, replica_groups=mesh['sp_0'=8,'sp_1'=8,'tp'=8] {'tp'}, dimensions={0}, use_global_device_ids=true | all-gather | bytes 884736 | tf_op jit(solution)/shard_map/all_gather | solution.py:347
  134.1 0.0 all-gather.2.cloned.1.call-done.w_hbm
  134.1 7.0 %feed.1 = bf16[192,2048]{1,0:T(8,128)(2,1)} custom-call(bf16[192,2048]{1,0:T(8,128)(2,1)} %all_gather.10.x_ref, bf16[2048,2176]{1,0:T(8,128)(2,1)} %all-gather.2.cloned.1.call-done.w_hbm), custom_call_target="tpu_custom_call" | custom-call | flops 1660944384 | bytes 10485760 | tf_op jit(solution)/shard_map/feed/pallas_call | solution.py:284
  141.2 15.7 %all_to_all.26 = bf16[8,24,2048]{2,1,0:T(8,128)(2,1)S(1)} all-to-all(bf16[8,24,2048]{2,1,0:T(8,128)(2,1)} %bitcast.5), channel_id=1, replica_groups=mesh['sp_0'=8,'sp_1'=8,'tp'=8] {'tp'}, dimensions={0} | all-to-all | bytes 1572864 | tf_op jit(solution)/shard_map/all_to_all | solution.py:311
  156.9 0.1 convert_reduce_fusion
  157.0 0.7 fusion.3
  (2 shorter events, 0.0 us)
Async XLA Ops:
  6.5 127.6 %all-gather.2.cloned.1.call-start = ((), (), s32[]{:S(2)}) async-start(), calls=%async_computation.5 | async-start | bytes 9052160 | tf_op jit(solution)/shard_map/all_gather | solution.py:334
  11.0 7.8 %copy-start.1 = (bf16[192,256]{1,0:T(8,128)(2,1)S(1)}, bf16[192,256]{1,0:T(8,128)(2,1)}, u32[]{:S(2)}) copy-start(bf16[192,256]{1,0:T(8,128)(2,1)} %get-tuple-element.8) | copy-start | bytes 294916
  11.0 36.1 %all-to-all-start = ((bf16[8,192,256]{2,1,0:T(8,128)(2,1)}), bf16[8,192,256]{2,1,0:T(8,128)(2,1)S(1)}, u32[]{:S(2)}, u32[]{:S(2)}) async-start(bf16[8,192,256]{2,1,0:T(8,128)(2,1)} %get-tuple-element.7), calls=%async_computation | async-start | bytes 1572864 | tf_op jit(solution)/shard_map/all_to_all | solution.py:337
  52.3 17.6 %all-to-all-start.2 = ((bf16[8,208,128]{2,1,0:T(8,128)(2,1)}), bf16[8,208,128]{2,1,0:T(8,128)(2,1)S(1)}, u32[]{:S(2)}, u32[]{:S(2)}) async-start(bf16[8,208,128]{2,1,0:T(8,128)(2,1)} %attend1.1), calls=%async_computation.2 | async-start | bytes 851968 | tf_op jit(solution)/shard_map/all_to_all | solution.py:340
  69.9 19.6 %copy-start = (bf16[8,208,128]{2,1,0:T(8,128)(2,1)}, bf16[8,208,128]{2,1,0:T(8,128)(2,1)S(1)}, u32[]{:S(2)}) copy-start(bf16[8,208,128]{2,1,0:T(8,128)(2,1)S(1)} %all-to-all-done.2.refs_1_) | copy-start | bytes 1277956
  92.8 26.0 %copy-start.2 = (f32[2048]{0:T(1024)S(1)}, f32[2048]{0:T(1024)}, u32[]{:S(2)}) copy-start(f32[2048]{0:T(1024)} %param.22) | copy-start | bytes 24580
  92.8 24.8 %all-to-all-start.3 = ((bf16[8,24,2048]{2,1,0:T(8,128)(2,1)}), bf16[8,24,2048]{2,1,0:T(8,128)(2,1)S(1)}, u32[]{:S(2)}, u32[]{:S(2)}) async-start(bf16[8,24,2048]{2,1,0:T(8,128)(2,1)} %bitcast.6), calls=%async_computation.3 | async-start | bytes 1572864 | tf_op jit(solution)/shard_map/all_to_all | solution.py:311
Sparse Core Ops, SparseCore 0:
  10.3 117.8 all-gather.1

commit v4 on v3

--- a/solution.py
+++ b/solution.py
@@ -11,7 +11,7 @@
 
 GRID_W = 64
 SP = ("sp_0", "sp_1")
-SP_TP = ("sp_0", "sp_1", "tp")
+TP = ("x", "c")
 EPSILON = 1e-06
 BF16 = jnp.bfloat16
 F32 = jnp.float32
@@ -119,7 +119,8 @@
 
 
 def attend_kernel(q_ref, next_ref, kv_ref, o_ref, even_ref, odd_ref, top_ref, *, chunk):
-    rows, head_dim = q_ref.shape[1:]
+    rows = q_ref.shape[1]
+    head_dim = q_ref.shape[2] // 2
     count = kv_ref.shape[0] // chunk
     factor = head_dim ** (-0.5) * LOG2E
 
@@ -145,19 +146,20 @@
 
     def finish(b, top, total, accum):
         whole = jnp.sum(total, axis=-1, keepdims=True)
-        o_ref[b, 0:rows, :] = (accum / whole).astype(BF16)
-        o_ref[b, rows:, :] = packed_stats(top * factor + jnp.log2(whole))
+        cols = slice(b * head_dim, (b + 1) * head_dim)
+        o_ref[0, 0:rows, cols] = (accum / whole).astype(BF16)
+        o_ref[0, rows:, cols] = packed_stats(top * factor + jnp.log2(whole))
 
     @pl.when(pl.program_id(0) == 0)
     def _():
         peak = None
         for c in range(count):
-            peak = score(q_ref[0], even_ref, c, peak)
+            peak = score(q_ref[0, :, 0:head_dim], even_ref, c, peak)
         top_ref[...] = jnp.broadcast_to(jnp.max(peak, axis=-1, keepdims=True), top_ref.shape)
 
     top = top_ref[:, 0:1]
     for b, (q, s_ref, done_ref) in enumerate(
-        ((q_ref[1], odd_ref, even_ref), (next_ref[0], even_ref, odd_ref))
+        ((q_ref[0, :, head_dim:], odd_ref, even_ref), (next_ref[0, :, 0:head_dim], even_ref, odd_ref))
     ):
         peak = total = accum = None
         for c in range(count):
@@ -168,24 +170,23 @@
     top_ref[...] = jnp.broadcast_to(top, top_ref.shape)
 
 
-def attend(queries, keys_values, head):
-    parts, rows, _ = queries.shape
+def attend(queries, keys_values):
+    parts, rows, width = queries.shape
     keys = keys_values.shape[0]
-    head_dim = keys_values.shape[1] // 2
-    steps = parts // 2
-    work = parts * rows * keys
+    head_dim = width // 2
+    work = parts * 2 * rows * keys
     return pl.pallas_call(
-        functools.partial(attend_kernel, chunk=next(n for n in (512, 384, 256, 128) if keys % n == 0)),
-        grid=(steps,),
+        functools.partial(
+            attend_kernel, chunk=next(n for n in (512, 384, 256, 128) if keys % n == 0)
+        ),
+        grid=(parts,),
         in_specs=[
-            pl.BlockSpec((2, rows, head_dim), lambda i: (i, 0, head)),
-            pl.BlockSpec(
-                (2, rows, head_dim), lambda i: (jnp.minimum(i + 1, steps - 1), 0, head)
-            ),
+            pl.BlockSpec((1, rows, width), lambda i: (i, 0, 0)),
+            pl.BlockSpec((1, rows, width), lambda i: (jnp.minimum(i + 1, parts - 1), 0, 0)),
             pl.BlockSpec((keys, 2 * head_dim), lambda i: (0, 0)),
         ],
-        out_specs=pl.BlockSpec((2, rows + STAT_ROWS, head_dim), lambda i: (i, 0, 0)),
-        out_shape=jax.ShapeDtypeStruct((parts, rows + STAT_ROWS, head_dim), BF16),
+        out_specs=pl.BlockSpec((1, rows + STAT_ROWS, width), lambda i: (i, 0, 0)),
+        out_shape=jax.ShapeDtypeStruct((parts, rows + STAT_ROWS, width), BF16),
         scratch_shapes=[
             pltpu.VMEM((rows, keys), F32),
             pltpu.VMEM((rows, keys), F32),
@@ -195,24 +196,25 @@
             dimension_semantics=("arbitrary",), vmem_limit_bytes=32 * 2**20
         ),
         cost_estimate=pl.CostEstimate(
-            flops=4 * work * head_dim, bytes_accessed=2 * 2**20, transcendentals=work
-        ),
-        name=f"attend{head}",
+            flops=4 * work * head_dim, bytes_accessed=4 * 2**20, transcendentals=work
+        ),
+        name="attend",
     )(queries, queries, keys_values)
 
 
-def project_kernel(*refs):
-    *part_refs, w_ref, o_ref = refs
-    parts, all_rows, head_dim = part_refs[0].shape
+def combine_kernel(part_ref, o_ref):
+    parts, all_rows, width = part_ref.shape
     rows = all_rows - STAT_ROWS
+    cores, held = o_ref.shape[:2]
+    share = rows // lax.axis_size(TP)
     eye = (
         lax.broadcasted_iota(jnp.int32, (128, 128), 0)
         == lax.broadcasted_iota(jnp.int32, (128, 128), 1)
     )
-    pieces = []
-    for part_ref in part_refs:
+    for h in range(width // 128):
+        cols = slice(h * 128, (h + 1) * 128)
+        stats = [part_ref[p, rows:, cols].astype(F32) for p in range(parts)]
         outs = []
-        stats = [part_ref[p, rows:, :].astype(F32) for p in range(parts)]
         for t in range(-(-rows // 128)):
             n = min(128, rows - t * 128)
             levels = [
@@ -222,29 +224,55 @@
             top = functools.reduce(jnp.maximum, levels)
             shares = [jnp.exp2(v - top) for v in levels]
             whole = functools.reduce(jnp.add, shares)
-            total = jnp.zeros((n, head_dim), F32)
+            total = jnp.zeros((n, 128), F32)
             for p in range(parts):
                 flat = jnp.broadcast_to(shares[p] / whole, (n, 128))
-                share = jnp.sum(jnp.where(eye[:n], flat, 0.0), axis=1, keepdims=True)
-                total = total + share * part_ref[p, t * 128 : t * 128 + n, :].astype(F32)
-            outs.append(total.astype(BF16))
-        pieces.append(jnp.concatenate(outs, axis=0))
-    attn = jnp.concatenate(pieces, axis=1)
-    for c in range(w_ref.shape[1] // 512):
+                portion = jnp.sum(jnp.where(eye[:n], flat, 0.0), axis=1, keepdims=True)
+                total = total + portion * part_ref[p, t * 128 : t * 128 + n, cols].astype(F32)
+            outs.append(total)
+        attn = jnp.concatenate(outs, axis=0)
+        for k in range(rows // share):
+            at = pl.ds(k // cores * share, share)
+            o_ref[k % cores, at, cols] = attn[k * share : (k + 1) * share].astype(BF16)
+
+
+def combine(parts):
+    rows = parts.shape[1] - STAT_ROWS
+    cores = lax.axis_size("c")
+    return pl.pallas_call(
+        combine_kernel,
+        out_shape=jax.ShapeDtypeStruct((cores, rows // cores, parts.shape[2]), BF16),
+        compiler_params=pltpu.CompilerParams(vmem_limit_bytes=16 * 2**20),
+        cost_estimate=pl.CostEstimate(
+            flops=2 * parts.size, bytes_accessed=2**20, transcendentals=0
+        ),
+        name="combine",
+    )(parts)
+
+
+def project_kernel(x_ref, own_ref, other_ref, o_ref):
+    me = lax.axis_index("c")
+    mine = x_ref[me, me]
+    others = x_ref[1 - me, me]
+    for c in range(own_ref.shape[1] // 512):
         at = pl.ds(c * 512, 512)
-        o_ref[:, at] = jnp.dot(attn, w_ref[:, at], preferred_element_type=F32).astype(BF16)
-
-
-def project(parts, weight):
-    rows = parts[0].shape[1] - STAT_ROWS
+        o_ref[:, at] = (
+            jnp.dot(mine, own_ref[:, at], preferred_element_type=F32)
+            + jnp.dot(others, other_ref[:, at], preferred_element_type=F32)
+        ).astype(BF16)
+
+
+def project(attn, own, other):
+    rows = attn.shape[2]
     return pl.pallas_call(
         project_kernel,
-        out_shape=jax.ShapeDtypeStruct((rows, weight.shape[1]), BF16),
+        out_shape=jax.ShapeDtypeStruct((rows, own.shape[1]), BF16),
+        compiler_params=pltpu.CompilerParams(vmem_limit_bytes=16 * 2**20),
         cost_estimate=pl.CostEstimate(
-            flops=2 * rows * weight.size, bytes_accessed=3 * 2**20, transcendentals=0
+            flops=4 * rows * own.size, bytes_accessed=3 * 2**20, transcendentals=0
         ),
         name="project",
-    )(*parts, weight)
+    )(attn, own, other)
 
 
 def feed_kernel(x_ref, w_hbm, o_ref, w_ref, acc_ref, sems, *, units):
@@ -306,9 +334,9 @@
     ).astype(BF16)
 
 
-def summed_over_tp(x):
-    share = x.shape[0] // lax.axis_size("tp")
-    blocks = lax.all_to_all(x.reshape(-1, share, x.shape[1]), "tp", 0, 0, tiled=True)
+def summed_over(x, axis):
+    count = lax.axis_size(axis)
+    blocks = lax.all_to_all(x.reshape(count, -1, x.shape[1]), axis, 0, 0, tiled=True)
     return jnp.sum(blocks.astype(F32), axis=0)
 
 
@@ -336,37 +364,38 @@
     copies, keys_values = prep(query, key, value, q_gain, k_gain, lax.axis_size("sp_1"))
     queries = lax.all_to_all(copies, "sp_1", 0, 0, tiled=True)
     keys_values = lax.all_gather(keys_values, "sp_0", axis=0, tiled=True)
-    partials = [
-        lax.all_to_all(attend(queries, keys_values, h), "sp_1", 0, 0, tiled=True)
-        for h in range(query.shape[1] // key.shape[1])
-    ]
-    proj = summed_over_tp(project(partials, out_weight))
-    share = rows // lax.axis_size("tp")
-    my_resid = lax.dynamic_slice_in_dim(resid, lax.axis_index("tp") * share, share, 0)
+    other_weight = lax.ppermute(out_weight, "c", [(0, 1), (1, 0)])
+    partial = lax.all_to_all(attend(queries, keys_values), "sp_1", 0, 0, tiled=True)
+    attn = lax.all_gather(combine(partial), "c", axis=0)
+    proj = summed_over(project(attn, out_weight, other_weight), "x")
+    share = rows // lax.axis_size(TP)
+    my_resid = lax.dynamic_slice_in_dim(resid, lax.axis_index(TP) * share, share, 0)
     my_stream = (my_resid.astype(F32) + proj).astype(BF16)
-    normed = lax.all_gather(normalize(my_stream, norm_gain), "tp", axis=0, tiled=True)
-    down = summed_over_tp(feed(normed, weights, units))
+    normed = lax.all_gather(normalize(my_stream, norm_gain), TP, axis=0, tiled=True)
+    down = summed_over(feed(normed, weights, units), TP)
     return (my_stream.astype(F32) + 0.5 * down).astype(BF16)
 
 
 def solution(mesh):
-    torus = Mesh(mesh.devices.reshape(8, 8, mesh.shape["tp"]), ("sp_0", "sp_1", "tp"))
+    torus = Mesh(
+        mesh.devices.reshape(8, 8, mesh.shape["tp"] // 2, 2), ("sp_0", "sp_1", "x", "c")
+    )
     return jax.shard_map(
         body,
         mesh=torus,
         in_specs=(
             P(SP, None),
-            P(SP, "tp"),
-            P(SP, "tp"),
-            P(SP, "tp"),
+            P(SP, TP),
+            P(SP, TP),
+            P(SP, TP),
             P(),
             P(),
-            P("tp", None),
+            P(TP, None),
             P(),
-            P(SP, "tp"),
-            P(SP, "tp"),
-            P("tp", SP),
-        ),
-        out_specs=P(SP_TP, None),
+            P(SP, TP),
+            P(SP, TP),
+            P(TP, SP),
+        ),
+        out_specs=P(SP + TP, None),
         check_vma=False,
     )

time: 165 us -> 160 us (0.970)
  blocking collectives: 78.9 us -> 76 us
  Pallas kernels: 22.8 us -> 20.4 us
    all_to_all x2 -> x1, blocking collectives: 35.3 us -> 17.3 us  [summed_over(): lax.all_to_all(x.reshape(count, -1, x.shape[1]), axis, 0, 0, tiled=True)]
    all_gather x1 -> x2, blocking collectives: 15.3 us -> 30 us  [the longest x1 16 us: body(): lax.all_gather(normalize(my_stream, norm_gain), TP, axis=0, tiled=True)]
    all_to_all x2, starting transfers between devices: 19 us -> 10.6 us  [the longest x1 6.38 us: body(): lax.all_to_all(attend(queries, keys_values), 'sp_1', 0, 0, tiled=True)]
    ppermute x0 -> x1, starting transfers between devices: none -> 8.08 us  [body(): other_weight = lax.ppermute(out_weight, 'c', [(0, 1), (1, 0)])]
    pallas_call x1 -> x2, Pallas kernels: 3.33 us -> 1.79 us  [the longest x1 1.27 us: project(): pl.pallas_call(project_kernel, out_shape=jax.ShapeDtypeStruct((rows, own....]
    pallas_call x2 -> x1, Pallas kernels: 9.62 us -> 8.75 us  [attend(): pl.pallas_call(functools.partial(attend_kernel, chunk=next((n for n in (5...]
  transfers between devices with their start and end apart: 4 -> 5, of which waited for: 2 -> 2; matrix products, arithmetic and copies ran while one was open for 1% -> 1% of each run, Pallas kernels for 10% -> 8%
where the time goes in v4:
time: 160 us; the launch traced here: 159 us
  blocking collectives  76 us (48%)
  starting transfers between devices  26.3 us (16%)
  Pallas kernels  20.4 us (13%)
  waiting for transfers between devices  19.7 us (12%)
  between operations  13.4 us (8%)
  other arithmetic  1.96 us (1%)
  local copies, waits for them, and re-layouts  1.71 us (1%)
    all_gather x1, blocking collectives, body(): keys_values = lax.all_gather(keys_values, 'sp_0', axis=0, tiled=True)  28.7 us
    all_to_all x1, blocking collectives, summed_over(): lax.all_to_all(x.reshape(count, -1, x.shape[1]), axis, 0, 0, tiled=True)  17.3 us
    all_gather x1, blocking collectives, body(): lax.all_gather(normalize(my_stream, norm_gain), TP, axis=0, tiled=True)  16 us
    all_gather x1, blocking collectives, body(): attn = lax.all_gather(combine(partial), 'c', axis=0)  13.9 us
    all_to_all x1, waiting for transfers between devices, body(): lax.all_to_all(attend(queries, keys_values), 'sp_1', 0, 0, tiled=True)  12.3 us
    pallas_call x1, Pallas kernels, attend(): pl.pallas_call(functools.partial(attend_kernel, chunk=next((n for n in (5...  8.75 us
    ppermute x1, starting transfers between devices, body(): other_weight = lax.ppermute(out_weight, 'c', [(0, 1), (1, 0)])  8.08 us
    all_to_all x1, starting transfers between devices, body(): queries = lax.all_to_all(copies, 'sp_1', 0, 0, tiled=True)  7.64 us
  transfers between devices with their start and end apart: 5, of which 2 were waited for; matrix products, arithmetic and copies ran while one was open for 1% of the time, Pallas kernels for 8%

profile of v4, /device:TPU:1, one launch (start us, length us, event | category | flops | bytes accessed | tf_op | source)
XLA Modules:
  0.0 159.4 jit_solution(4831389915879149853)
XLA Ops:
  6.5 0.0 copy-start
  6.5 0.0 all-gather.3.cloned.1.call-start
  6.5 1.7 %concatenate.3 = bf16[32,2176]{1,0:T(8,128)(2,1)} concatenate(bf16[32,704]{1,0:T(8,128)(2,1)} %param.23, bf16[32,704]{1,0:T(8,128)(2,1)} %param.24, bf16[32,704]{1,0:T(8,128)(2,1)} %bitcast.8, bf16[32,64]{1,0:T(8,128)(2,1)S(1)} %broadcast_in_dim.2), dimensions={1} | concatenate | bytes 278528 | tf_op jit(solution)/shard_map/concatenate | solution.py:362
  8.2 0.0 all-gather.3.cloned.1.call-update
  8.3 2.8 %prep.1 = (bf16[8,192,256]{2,1,0:T(8,128)(2,1)}, bf16[192,256]{1,0:T(8,128)(2,1)}) custom-call(bf16[192,256]{1,0:T(8,128)(2,1)} %q_ref.1, bf16[192,128]{1,0:T(8,128)(2,1)} %k_ref.1, bf16[192,128]{1,0:T(8,128)(2,1)} %v_ref.1, f32[1,128]{1,0:T(1,128)} %bitcast.9, f32[1,128]{1,0:T(1,128)} %bitcast.10, f32[1,128]{1,0:T(1,128)} %constant.35.clone.inv_ref, ...), custom_call_target="tpu_custom_call" | custom-call | tf_op jit(solution)/shard_map/prep/pallas_call | solution.py:76
  11.1 7.6 %all-to-all-start = ((bf16[8,192,256]{2,1,0:T(8,128)(2,1)}), bf16[8,192,256]{2,1,0:T(8,128)(2,1)S(1)}, u32[]{:S(2)}, u32[]{:S(2)}) async-start(bf16[8,192,256]{2,1,0:T(8,128)(2,1)} %get-tuple-element.7), calls=%async_computation | async-start | bytes 1572864 | tf_op jit(solution)/shard_map/all_to_all | solution.py:365
  18.8 0.0 copy-start.1
  18.8 28.7 %all_gather.15.kv_ref = bf16[1536,256]{1,0:T(8,128)(2,1)S(1)} all-gather(bf16[192,256]{1,0:T(8,128)(2,1)} %get-tuple-element.8), channel_id=1, replica_groups=mesh['sp_0'=8,'sp_1'=8,'x'=4,'c'=2] {'sp_0'}, dimensions={0}, use_global_device_ids=true | all-gather | bytes 884736 | tf_op jit(solution)/shard_map/all_gather | solution.py:366
  47.5 0.0 all-to-all-done.q_ref.next_ref
  47.5 8.7 %attend.1 = bf16[8,208,256]{2,1,0:T(8,128)(2,1)} custom-call(bf16[8,192,256]{2,1,0:T(8,128)(2,1)S(1)} %all-to-all-done.q_ref.next_ref, bf16[8,192,256]{2,1,0:T(8,128)(2,1)S(1)} %all-to-all-done.q_ref.next_ref, bf16[1536,256]{1,0:T(8,128)(2,1)S(1)} %all_gather.15.kv_ref), custom_call_target="tpu_custom_call" | custom-call | flops 2415919104 | bytes 4194304 | tf_op jit(solution)/shard_map/attend/pallas_call | solution.py:178
  56.2 6.4 %all-to-all-start.1 = ((bf16[8,208,256]{2,1,0:T(8,128)(2,1)}), bf16[8,208,256]{2,1,0:T(8,128)(2,1)S(1)}, u32[]{:S(2)}, u32[]{:S(2)}) async-start(bf16[8,208,256]{2,1,0:T(8,128)(2,1)} %attend.1), calls=%async_computation.1 | async-start | bytes 1703936 | tf_op jit(solution)/shard_map/all_to_all | solution.py:368
  62.6 0.0 copy-done
  62.6 8.1 %collective-permute-start = (bf16[256,2048]{1,0:T(8,128)(2,1)S(1)}, bf16[256,2048]{1,0:T(8,128)(2,1)S(1)}, u32[]{:S(2)}, u32[]{:S(2)}) collective-permute-start(bf16[256,2048]{1,0:T(8,128)(2,1)S(1)} %copy-done), channel_id=1, source_target_pairs={{0,1},{1,0},{2,3},{3,2},{4,5},{5,4},{6,7},{7,6},{8,9},{9,8},{10,11... | collective-permute-start | bytes 3145736 | tf_op jit(solution)/shard_map/ppermute | solution.py:367
  70.7 12.3 %all-to-all-done.1.part_ref = bf16[8,208,256]{2,1,0:T(8,128)(2,1)S(1)} async-done(((bf16[8,208,256]{2,1,0:T(8,128)(2,1)}), bf16[8,208,256]{2,1,0:T(8,128)(2,1)S(1)}, u32[]{:S(2)}, u32[]{:S(2)}) %all-to-all-start.1) | async-done | bytes 852000 | tf_op jit(solution)/shard_map/all_to_all | solution.py:368
  83.1 0.5 combine.1
  83.6 13.9 %all-gather = bf16[4,96,256]{2,1,0:T(8,128)(2,1)S(1)} all-gather(bf16[2,96,256]{2,1,0:T(8,128)(2,1)S(1)} %combine.1), channel_id=2, replica_groups=mesh['sp_0'=8,'sp_1'=8,'x'=4,'c'=2] {'c'}, dimensions={0}, use_global_device_ids=true | all-gather | bytes 294912 | tf_op jit(solution)/shard_map/all_gather | solution.py:369
  97.5 0.0 collective-permute-done.other_ref
  97.5 1.3 project.1
  98.8 4.2 %all-to-all-start.2 = ((bf16[4,24,2048]{2,1,0:T(8,128)(2,1)}), bf16[4,24,2048]{2,1,0:T(8,128)(2,1)S(1)}, u32[]{:S(2)}, u32[]{:S(2)}) async-start(bf16[4,24,2048]{2,1,0:T(8,128)(2,1)} %bitcast.3), calls=%async_computation.2 | async-start | bytes 786432 | tf_op jit(solution)/shard_map/all_to_all | solution.py:339
  103.0 7.3 %all-to-all-done.2 = bf16[4,24,2048]{2,1,0:T(8,128)(2,1)S(1)} async-done(((bf16[4,24,2048]{2,1,0:T(8,128)(2,1)}), bf16[4,24,2048]{2,1,0:T(8,128)(2,1)S(1)}, u32[]{:S(2)}, u32[]{:S(2)}) %all-to-all-start.2) | async-done | bytes 393248 | tf_op jit(solution)/shard_map/all_to_all | solution.py:339
  110.3 1.0 fusion
  111.4 0.0 copy-done.1
  111.4 0.1 fusion.2
  111.5 16.0 %all_gather.18.x_ref = bf16[192,2048]{1,0:T(8,128)(2,1)} all-gather(bf16[24,2048]{1,0:T(8,128)(2,1)S(1)} %fusion.2), channel_id=1, replica_groups=mesh['sp_0'=8,'sp_1'=8,'x'=4,'c'=2] {'x','c'}, dimensions={0}, use_global_device_ids=true | all-gather | bytes 884736 | tf_op jit(solution)/shard_map/all_gather | solution.py:374
  127.5 0.0 all-gather.3.cloned.1.call-done.w_hbm
  127.5 7.0 %feed.1 = bf16[192,2048]{1,0:T(8,128)(2,1)} custom-call(bf16[192,2048]{1,0:T(8,128)(2,1)} %all_gather.18.x_ref, bf16[2048,2176]{1,0:T(8,128)(2,1)} %all-gather.3.cloned.1.call-done.w_hbm), custom_call_target="tpu_custom_call" | custom-call | flops 1660944384 | bytes 10485760 | tf_op jit(solution)/shard_map/feed/pallas_call | solution.py:312
  134.5 17.3 %all_to_all.20 = bf16[8,24,2048]{2,1,0:T(8,128)(2,1)S(1)} all-to-all(bf16[8,24,2048]{2,1,0:T(8,128)(2,1)} %bitcast.7), channel_id=1, replica_groups=mesh['sp_0'=8,'sp_1'=8,'x'=4,'c'=2] {'x','c'}, dimensions={0} | all-to-all | bytes 1572864 | tf_op jit(solution)/shard_map/all_to_all | solution.py:339
  151.8 0.1 convert_reduce_fusion
  151.9 0.7 fusion.3
  (3 shorter events, 0.1 us)
Async XLA Ops:
  6.5 56.1 %copy-start = (bf16[256,2048]{1,0:T(8,128)(2,1)S(1)}, bf16[256,2048]{1,0:T(8,128)(2,1)}, u32[]{:S(2)}) copy-start(bf16[256,2048]{1,0:T(8,128)(2,1)} %own_ref.1) | copy-start | bytes 3145732
  6.5 121.0 %all-gather.3.cloned.1.call-start = ((), (), s32[]{:S(2)}) async-start(), calls=%async_computation.4 | async-start | bytes 9052160 | tf_op jit(solution)/shard_map/all_gather | solution.py:362
  11.1 36.4 %all-to-all-start = ((bf16[8,192,256]{2,1,0:T(8,128)(2,1)}), bf16[8,192,256]{2,1,0:T(8,128)(2,1)S(1)}, u32[]{:S(2)}, u32[]{:S(2)}) async-start(bf16[8,192,256]{2,1,0:T(8,128)(2,1)} %get-tuple-element.7), calls=%async_computation | async-start | bytes 1572864 | tf_op jit(solution)/shard_map/all_to_all | solution.py:365
  18.8 92.6 %copy-start.1 = (f32[2048]{0:T(1024)S(1)}, f32[2048]{0:T(1024)}, u32[]{:S(2)}) copy-start(f32[2048]{0:T(1024)} %param.22) | copy-start | bytes 24580
  56.2 26.8 %all-to-all-start.1 = ((bf16[8,208,256]{2,1,0:T(8,128)(2,1)}), bf16[8,208,256]{2,1,0:T(8,128)(2,1)S(1)}, u32[]{:S(2)}, u32[]{:S(2)}) async-start(bf16[8,208,256]{2,1,0:T(8,128)(2,1)} %attend.1), calls=%async_computation.1 | async-start | bytes 1703936 | tf_op jit(solution)/shard_map/all_to_all | solution.py:368
  62.6 34.9 %collective-permute-start = (bf16[256,2048]{1,0:T(8,128)(2,1)S(1)}, bf16[256,2048]{1,0:T(8,128)(2,1)S(1)}, u32[]{:S(2)}, u32[]{:S(2)}) collective-permute-start(bf16[256,2048]{1,0:T(8,128)(2,1)S(1)} %copy-done), channel_id=1, source_target_pairs={{0,1},{1,0},{2,3},{3,2},{4,5},{5,4},{6,7},{7,6},{8,9},{9,8},{10,11... | collective-permute-start | bytes 3145736 | tf_op jit(solution)/shard_map/ppermute | solution.py:367
  98.8 11.5 %all-to-all-start.2 = ((bf16[4,24,2048]{2,1,0:T(8,128)(2,1)}), bf16[4,24,2048]{2,1,0:T(8,128)(2,1)S(1)}, u32[]{:S(2)}, u32[]{:S(2)}) async-start(bf16[4,24,2048]{2,1,0:T(8,128)(2,1)} %bitcast.3), calls=%async_computation.2 | async-start | bytes 786432 | tf_op jit(solution)/shard_map/all_to_all | solution.py:339
Sparse Core Ops, SparseCore 0:
  10.3 117.0 all-gather.2

commit v5 on v4

--- a/solution.py
+++ b/solution.py
@@ -9,8 +9,12 @@
 from jax.sharding import Mesh
 from jax.sharding import PartitionSpec as P
 
+
 GRID_W = 64
-SP = ("sp_0", "sp_1")
+SP = ("sp_0", "ya", "yb")
+ROW = ("ya", "yb")
+FEED = ("x", "yb")
+WEIGHTS = ("sp_0", "ya", "c")
 TP = ("x", "c")
 EPSILON = 1e-06
 BF16 = jnp.bfloat16
@@ -37,7 +41,9 @@
     heads = q_ref.shape[1] // head_dim
     quarter = head_dim // 4
     spans = rows // GRID_W
-    sp = lax.axis_index("sp_0") * lax.axis_size("sp_1") + lax.axis_index("sp_1")
+    sp = lax.axis_index("sp_0")
+    for axis in ROW:
+        sp = sp * lax.axis_size(axis) + lax.axis_index(axis)
     first_row = (sp * spans).astype(F32)
     line = first_row + lax.broadcasted_iota(jnp.int32, (8, head_dim), 0).astype(F32)
     angle = line * inv_ref[...]
@@ -78,6 +84,9 @@
         out_shape=(
             jax.ShapeDtypeStruct((copies, *query.shape), BF16),
             jax.ShapeDtypeStruct((rows, 2 * head_dim), BF16),
+        ),
+        cost_estimate=pl.CostEstimate(
+            flops=4 * 10**9, bytes_accessed=2 * 2**20, transcendentals=0
         ),
         name="prep",
     )(
@@ -205,7 +214,7 @@
 def combine_kernel(part_ref, o_ref):
     parts, all_rows, width = part_ref.shape
     rows = all_rows - STAT_ROWS
-    cores, held = o_ref.shape[:2]
+    cores, _ = o_ref.shape[:2]
     share = rows // lax.axis_size(TP)
     eye = (
         lax.broadcasted_iota(jnp.int32, (128, 128), 0)
@@ -275,22 +284,11 @@
     )(attn, own, other)
 
 
-def feed_kernel(x_ref, w_hbm, o_ref, w_ref, acc_ref, sems, *, units):
+def feed_kernel(x_ref, w_ref, o_ref, acc_ref, *, units):
     depth, width = w_ref.shape
-    pieces = sems.shape[0]
-    block = depth // pieces
     both = 2 * units
     spare = width - 3 * units
-    copies = []
-    for i in range(pieces):
-        at = pl.ds(i * block, block)
-        copies.append(pltpu.make_async_copy(w_hbm.at[at], w_ref.at[at], sems.at[i]))
-        copies[-1].start()
-    for i in range(pieces):
-        at = pl.ds(i * block, block)
-        copies[i].wait()
-        part = jnp.dot(x_ref[:, at], w_ref[at, 0:both], preferred_element_type=F32)
-        acc_ref[...] = part if i == 0 else acc_ref[...] + part
+    acc_ref[...] = jnp.dot(x_ref[...], w_ref[:, 0:both], preferred_element_type=F32)
     gate = acc_ref[:, 0:units]
     up = acc_ref[:, units:both]
     hidden = (gate / (1.0 + jnp.exp(-gate)) * up).astype(BF16)
@@ -306,20 +304,14 @@
 
 def feed(x, weights, units):
     rows, depth = x.shape
-    width = weights.shape[1]
-    pieces = 8
     vmem = pl.BlockSpec(memory_space=pltpu.VMEM)
     return pl.pallas_call(
         functools.partial(feed_kernel, units=units),
-        in_specs=[vmem, pl.BlockSpec(memory_space=pl.ANY)],
+        in_specs=[vmem, vmem],
         out_specs=vmem,
         out_shape=jax.ShapeDtypeStruct((rows, depth), BF16),
-        scratch_shapes=[
-            pltpu.VMEM((depth, width), BF16),
-            pltpu.VMEM((rows, 2 * units), F32),
-            pltpu.SemaphoreType.DMA((pieces,)),
-        ],
-        compiler_params=pltpu.CompilerParams(vmem_limit_bytes=60 * 2**20),
+        scratch_shapes=[pltpu.VMEM((rows, 2 * units), F32)],
+        compiler_params=pltpu.CompilerParams(vmem_limit_bytes=32 * 2**20),
         cost_estimate=pl.CostEstimate(
             flops=6 * rows * depth * units, bytes_accessed=10 * 2**20, transcendentals=0
         ),
@@ -327,17 +319,40 @@
     )(x, weights)
 
 
-def normalize(stream, gain):
+def stream_kernel(part_ref, resid_ref, gain_ref, _, stream_ref, copies_ref):
+    proj = part_ref[0].astype(F32)
+    for n in range(1, part_ref.shape[0]):
+        proj = proj + part_ref[n].astype(F32)
+    stream = (resid_ref[...].astype(F32) + proj).astype(BF16)
+    stream_ref[...] = stream
     values = stream.astype(F32)
-    return (
-        values * lax.rsqrt(jnp.mean(values * values, axis=-1, keepdims=True) + EPSILON) * gain
-    ).astype(BF16)
-
-
-def summed_over(x, axis):
+    normed = values * lax.rsqrt(jnp.mean(values * values, axis=-1, keepdims=True) + EPSILON)
+    normed = (normed * gain_ref[...]).astype(BF16)
+    for n in range(copies_ref.shape[0]):
+        copies_ref[n] = normed
+
+
+def stream_rows(parts, resid, gain, weights, copies):
+    vmem = pl.BlockSpec(memory_space=pltpu.VMEM)
+    return pl.pallas_call(
+        stream_kernel,
+        in_specs=[vmem, vmem, vmem, vmem],
+        out_specs=(vmem, vmem),
+        out_shape=(
+            jax.ShapeDtypeStruct(resid.shape, BF16),
+            jax.ShapeDtypeStruct((copies, *resid.shape), BF16),
+        ),
+        compiler_params=pltpu.CompilerParams(vmem_limit_bytes=8 * 2**20),
+        cost_estimate=pl.CostEstimate(
+            flops=2 * 10**10, bytes_accessed=2**20, transcendentals=0
+        ),
+        name="stream",
+    )(parts, resid, gain.reshape(1, -1), weights[0:8, 0:128])
+
+
+def scattered(x, axis):
     count = lax.axis_size(axis)
-    blocks = lax.all_to_all(x.reshape(count, -1, x.shape[1]), axis, 0, 0, tiled=True)
-    return jnp.sum(blocks.astype(F32), axis=0)
+    return lax.all_to_all(x.reshape(count, -1, x.shape[1]), axis, 0, 0, tiled=True)
 
 
 def body(
@@ -359,26 +374,31 @@
     spare = -(3 * units) % 128
     if spare:
         shard.append(jnp.zeros((gate_weight.shape[0], spare), BF16))
-    weights = lax.all_gather(jnp.concatenate(shard, axis=1), SP, axis=0, tiled=True)
-
-    copies, keys_values = prep(query, key, value, q_gain, k_gain, lax.axis_size("sp_1"))
-    queries = lax.all_to_all(copies, "sp_1", 0, 0, tiled=True)
+    shard = jnp.concatenate(shard, axis=1)
+    shard = lax.ppermute(shard, ("yb", "c"), [(0, 0), (1, 2), (2, 1), (3, 3)])
+    weights = lax.all_gather(shard, WEIGHTS, axis=0, tiled=True)
+
+    copies, keys_values = prep(query, key, value, q_gain, k_gain, lax.axis_size(ROW))
+    queries = lax.all_to_all(copies, ROW, 0, 0, tiled=True)
     keys_values = lax.all_gather(keys_values, "sp_0", axis=0, tiled=True)
     other_weight = lax.ppermute(out_weight, "c", [(0, 1), (1, 0)])
-    partial = lax.all_to_all(attend(queries, keys_values), "sp_1", 0, 0, tiled=True)
+    partial = lax.all_to_all(attend(queries, keys_values), ROW, 0, 0, tiled=True)
     attn = lax.all_gather(combine(partial), "c", axis=0)
-    proj = summed_over(project(attn, out_weight, other_weight), "x")
+    parts = scattered(project(attn, out_weight, other_weight), "x")
     share = rows // lax.axis_size(TP)
     my_resid = lax.dynamic_slice_in_dim(resid, lax.axis_index(TP) * share, share, 0)
-    my_stream = (my_resid.astype(F32) + proj).astype(BF16)
-    normed = lax.all_gather(normalize(my_stream, norm_gain), TP, axis=0, tiled=True)
-    down = summed_over(feed(normed, weights, units), TP)
+    my_stream, copies = stream_rows(
+        parts, my_resid, norm_gain, weights, lax.axis_size(FEED)
+    )
+    normed = lax.all_to_all(copies, FEED, 0, 0, tiled=True).reshape(-1, resid.shape[1])
+    down = jnp.sum(scattered(feed(normed, weights, units), FEED).astype(F32), axis=0)
     return (my_stream.astype(F32) + 0.5 * down).astype(BF16)
 
 
 def solution(mesh):
     torus = Mesh(
-        mesh.devices.reshape(8, 8, mesh.shape["tp"] // 2, 2), ("sp_0", "sp_1", "x", "c")
+        mesh.devices.reshape(8, 4, 2, mesh.shape["tp"] // 2, 2),
+        ("sp_0", "ya", "yb", "x", "c"),
     )
     return jax.shard_map(
         body,

time: 160 us -> 183 us (1.14)
  waiting for transfers between devices: 19.7 us -> 44 us
  Pallas kernels: 20.4 us -> 17.8 us
  starting transfers between devices: 26.3 us -> 28.5 us
    all_gather x1, waiting for transfers between devices: 0.01 us -> 17.3 us  [body(): weights = lax.all_gather(shard, WEIGHTS, axis=0, tiled=True)]
    all_gather x1 -> x0, blocking collectives: 16 us -> none  [body(): lax.all_gather(normalize(my_stream, norm_gain), TP, axis=0, tiled=True)]
    all_to_all x1 -> x2, blocking collectives: 17.3 us -> 31.9 us  [the longest x1 17.5 us: body(): lax.all_to_all(copies, FEED, 0, 0, tiled=True).reshape(-1, resid.shape[1])]
    ppermute x0 -> x1, starting transfers between devices: none -> 4.58 us  [body(): shard = lax.ppermute(shard, ('yb', 'c'), [(0, 0), (1, 2), (2, 1), (3, 3)])]
    pallas_call x1, Pallas kernels: 7.03 us -> 2.47 us  [feed(): pl.pallas_call(functools.partial(feed_kernel, units=units), in_specs=[vme...]
    all_to_all x3, waiting for transfers between devices: 19.6 us -> 23.9 us  [the longest x1 23.9 us: body(): lax.all_to_all(attend(queries, keys_values), ROW, 0, 0, tiled=True)]
    ppermute x0 -> x1, waiting for transfers between devices: none -> 2.72 us  [body(): shard = lax.ppermute(shard, ('yb', 'c'), [(0, 0), (1, 2), (2, 1), (3, 3)])]
  transfers between devices with their start and end apart: 5 -> 6, of which waited for: 2 -> 3; matrix products, arithmetic and copies ran while one was open for 1% -> 0% of each run, Pallas kernels for 8% -> 8%
where the time goes in v5:
time: 183 us; the launch traced here: 182 us
  blocking collectives  75 us (41%)
  waiting for transfers between devices  44 us (24%)
  starting transfers between devices  28.5 us (16%)
  Pallas kernels  17.8 us (10%)
  between operations  13.5 us (7%)
  local copies, waits for them, and re-layouts  2.38 us (1%)
    all_gather x1, blocking collectives, body(): keys_values = lax.all_gather(keys_values, 'sp_0', axis=0, tiled=True)  29.2 us
    all_to_all x1, waiting for transfers between devices, body(): lax.all_to_all(attend(queries, keys_values), ROW, 0, 0, tiled=True)  23.9 us
    all_to_all x1, blocking collectives, body(): lax.all_to_all(copies, FEED, 0, 0, tiled=True).reshape(-1, resid.shape[1])  17.5 us
    all_gather x1, waiting for transfers between devices, body(): weights = lax.all_gather(shard, WEIGHTS, axis=0, tiled=True)  17.3 us
    all_to_all x1, blocking collectives, scattered(): lax.all_to_all(x.reshape(count, -1, x.shape[1]), axis, 0, 0, tiled=True)  14.5 us
    all_gather x1, blocking collectives, body(): attn = lax.all_gather(combine(partial), 'c', axis=0)  13.9 us
    pallas_call x1, Pallas kernels, attend(): pl.pallas_call(functools.partial(attend_kernel, chunk=next((n for n in (5...  9.36 us
    all_to_all x1, starting transfers between devices, body(): queries = lax.all_to_all(copies, ROW, 0, 0, tiled=True)  6.84 us
  transfers between devices with their start and end apart: 6, of which 3 were waited for; matrix products, arithmetic and copies ran while one was open for 0% of the time, Pallas kernels for 8%

profile of v5, /device:TPU:1, one launch (start us, length us, event | category | flops | bytes accessed | tf_op | source)
XLA Modules:
  0.0 182.0 jit_solution(3218291271048574688)
XLA Ops:
  6.5 0.0 copy-start
  6.5 0.0 all-gather.3.cloned.1.call-start
  6.5 1.0 concatenate.3
  7.6 4.6 %collective-permute-start.1 = (bf16[32,2176]{1,0:T(8,128)(2,1)S(1)}, bf16[32,2176]{1,0:T(8,128)(2,1)S(1)}, u32[]{:S(2)}, u32[]{:S(2)}) collective-permute-start(bf16[32,2176]{1,0:T(8,128)(2,1)S(1)} %concatenate.3), channel_id=1, source_target_pairs={{0,0},{1,8},{8,1},{9,9},{2,2},{3,10},{10,3},{11,11},{4,4},{5,12},{... | collective-permute-start | bytes 417800 | tf_op jit(solution)/shard_map/ppermute | solution.py:378
  12.2 2.7 %collective-permute-done.1 = bf16[32,2176]{1,0:T(8,128)(2,1)S(1)} collective-permute-done((bf16[32,2176]{1,0:T(8,128)(2,1)S(1)}, bf16[32,2176]{1,0:T(8,128)(2,1)S(1)}, u32[]{:S(2)}, u32[]{:S(2)}) %collective-permute-start.1) | collective-permute-done | bytes 139296 | tf_op jit(solution)/shard_map/ppermute | solution.py:378
  14.9 0.0 copy-start.4
  14.9 0.7 copy-done.4
  15.6 0.0 all-gather.3.cloned.1.call-update
  15.6 2.8 %prep.1 = (bf16[8,192,256]{2,1,0:T(8,128)(2,1)}, bf16[192,256]{1,0:T(8,128)(2,1)}) custom-call(bf16[192,256]{1,0:T(8,128)(2,1)} %q_ref.1, bf16[192,128]{1,0:T(8,128)(2,1)} %k_ref.1, bf16[192,128]{1,0:T(8,128)(2,1)} %v_ref.1, f32[1,128]{1,0:T(1,128)} %bitcast.13, f32[1,128]{1,0:T(1,128)} %bitcast.14, f32[1,128]{1,0:T(1,128)} %constant.30.clone.inv_ref, ...), custom_call_target="tpu_custom_call" | custom-call | flops 4000000000 | bytes 2097152 | tf_op jit(solution)/shard_map/prep/pallas_call | solution.py:82
  18.4 0.0 copy-start.2
  18.4 0.0 copy-start.3
  18.4 6.8 %all-to-all-start = ((bf16[8,192,256]{2,1,0:T(8,128)(2,1)}), bf16[8,192,256]{2,1,0:T(8,128)(2,1)S(1)}, u32[]{:S(2)}, u32[]{:S(2)}) async-start(bf16[8,192,256]{2,1,0:T(8,128)(2,1)} %get-tuple-element.9), calls=%async_computation | async-start | bytes 1572864 | tf_op jit(solution)/shard_map/all_to_all | solution.py:382
  25.2 29.2 %all_gather.12.kv_ref = bf16[1536,256]{1,0:T(8,128)(2,1)S(1)} all-gather(bf16[192,256]{1,0:T(8,128)(2,1)} %get-tuple-element.10), channel_id=1, replica_groups=mesh['sp_0'=8,'ya'=4,'yb'=2,'x'=4,'c'=2] {'sp_0'}, dimensions={0}, use_global_device_ids=true | all-gather | bytes 884736 | tf_op jit(solution)/shard_map/all_gather | solution.py:383
  54.4 0.0 all-to-all-done.q_ref.next_ref
  54.4 9.4 %attend.1 = bf16[8,208,256]{2,1,0:T(8,128)(2,1)} custom-call(bf16[8,192,256]{2,1,0:T(8,128)(2,1)S(1)} %all-to-all-done.q_ref.next_ref, bf16[8,192,256]{2,1,0:T(8,128)(2,1)S(1)} %all-to-all-done.q_ref.next_ref, bf16[1536,256]{1,0:T(8,128)(2,1)S(1)} %all_gather.12.kv_ref), custom_call_target="tpu_custom_call" | custom-call | flops 2415919104 | bytes 4194304 | tf_op jit(solution)/shard_map/attend/pallas_call | solution.py:187
  63.8 6.6 %all-to-all-start.1 = ((bf16[8,208,256]{2,1,0:T(8,128)(2,1)}), bf16[8,208,256]{2,1,0:T(8,128)(2,1)S(1)}, u32[]{:S(2)}, u32[]{:S(2)}) async-start(bf16[8,208,256]{2,1,0:T(8,128)(2,1)} %attend.1), calls=%async_computation.1 | async-start | bytes 1703936 | tf_op jit(solution)/shard_map/all_to_all | solution.py:385
  70.4 0.0 copy-done.2
  70.4 6.5 %collective-permute-start = (bf16[256,2048]{1,0:T(8,128)(2,1)S(1)}, bf16[256,2048]{1,0:T(8,128)(2,1)}, u32[]{:S(2)}, u32[]{:S(2)}) collective-permute-start(bf16[256,2048]{1,0:T(8,128)(2,1)S(1)} %copy-done.2), channel_id=1, source_target_pairs={{0,1},{1,0},{2,3},{3,2},{4,5},{5,4},{6,7},{7,6},{8,9},{9,8},{10,11... | collective-permute-start | bytes 3145736 | tf_op jit(solution)/shard_map/ppermute | solution.py:384
  76.9 23.9 %all-to-all-done.1.part_ref = bf16[8,208,256]{2,1,0:T(8,128)(2,1)S(1)} async-done(((bf16[8,208,256]{2,1,0:T(8,128)(2,1)}), bf16[8,208,256]{2,1,0:T(8,128)(2,1)S(1)}, u32[]{:S(2)}, u32[]{:S(2)}) %all-to-all-start.1) | async-done | bytes 852000 | tf_op jit(solution)/shard_map/all_to_all | solution.py:385
  100.9 0.5 combine.1
  101.4 13.9 %all-gather = bf16[4,96,256]{2,1,0:T(8,128)(2,1)S(1)} all-gather(bf16[2,96,256]{2,1,0:T(8,128)(2,1)S(1)} %combine.1), channel_id=2, replica_groups=mesh['sp_0'=8,'ya'=4,'yb'=2,'x'=4,'c'=2] {'c'}, dimensions={0}, use_global_device_ids=true | all-gather | bytes 294912 | tf_op jit(solution)/shard_map/all_gather | solution.py:386
  115.3 0.0 collective-permute-done.other_ref
  115.3 2.4 %project.1 = bf16[96,2048]{1,0:T(8,128)(2,1)} custom-call(bf16[2,2,96,256]{3,2,1,0:T(8,128)(2,1)S(1)} %bitcast.10, bf16[256,2048]{1,0:T(8,128)(2,1)S(1)} %copy-done.2, bf16[256,2048]{1,0:T(8,128)(2,1)} %collective-permute-done.other_ref), custom_call_target="tpu_custom_call" | custom-call | flops 201326592 | bytes 3145728 | tf_op jit(solution)/shard_map/project/pallas_call | solution.py:276
  117.8 4.0 %all-to-all-start.2 = ((bf16[4,24,2048]{2,1,0:T(8,128)(2,1)}), bf16[4,24,2048]{2,1,0:T(8,128)(2,1)S(1)}, u32[]{:S(2)}, u32[]{:S(2)}) async-start(bf16[4,24,2048]{2,1,0:T(8,128)(2,1)} %bitcast.3), calls=%async_computation.2 | async-start | bytes 786432 | tf_op jit(solution)/shard_map/all_to_all | solution.py:355
  121.7 0.0 copy-done
  121.7 17.3 %all-gather.3.cloned.1.call-done.w_ref = bf16[2048,2176]{1,0:T(8,128)(2,1)} async-done(((bf16[32,2176]{1,0:T(8,128)(2,1)}), bf16[2048,2176]{1,0:T(8,128)(2,1)}) %all-gather.3.cloned.1.call-update) | async-done | bytes 8912912 | tf_op jit(solution)/shard_map/all_gather | solution.py:379
  139.1 0.7 slice.4._
  139.7 0.0 all-to-all-done.2.part_ref
  139.8 0.0 copy-done.3
  139.8 0.0 copy-start.1
  139.8 0.2 stream.1
  140.0 17.5 %all_to_all.25 = bf16[8,24,2048]{2,1,0:T(8,128)(2,1)S(1)} all-to-all(bf16[8,24,2048]{2,1,0:T(8,128)(2,1)S(1)} %get-tuple-element.12), channel_id=1, replica_groups=mesh['sp_0'=8,'ya'=4,'yb'=2,'x'=4,'c'=2] {'x','yb'}, dimensions={0} | all-to-all | bytes 1572864 | tf_op jit(solution)/shard_map/all_to_all | solution.py:393
  157.4 0.0 copy-done.1
  157.4 2.5 %feed.1 = bf16[192,2048]{1,0:T(8,128)(2,1)S(1)} custom-call(bf16[192,2048]{1,0:T(8,128)(2,1)S(1)} %bitcast.8, bf16[2048,2176]{1,0:T(8,128)(2,1)S(1)} %copy-done.1), custom_call_target="tpu_custom_call" | custom-call | flops 1660944384 | bytes 10485760 | tf_op jit(solution)/shard_map/feed/pallas_call | solution.py:308
  159.9 14.5 %all_to_all.26 = bf16[8,24,2048]{2,1,0:T(8,128)(2,1)S(1)} all-to-all(bf16[8,24,2048]{2,1,0:T(8,128)(2,1)S(1)} %bitcast.9), channel_id=1, replica_groups=mesh['sp_0'=8,'ya'=4,'yb'=2,'x'=4,'c'=2] {'x','yb'}, dimensions={0} | all-to-all | bytes 1572864 | tf_op jit(solution)/shard_map/all_to_all | solution.py:355
  174.3 0.1 convert_reduce_fusion
  174.5 0.7 add_convert_fusion
  (2 shorter events, 0.0 us)
Async XLA Ops:
  6.5 115.2 %copy-start = (bf16[192,2048]{1,0:T(8,128)(2,1)S(1)}, bf16[192,2048]{1,0:T(8,128)(2,1)}, u32[]{:S(2)}) copy-start(bf16[192,2048]{1,0:T(8,128)(2,1)} %param.15) | copy-start | bytes 2359300
  6.5 132.5 %all-gather.3.cloned.1.call-start = ((), (), s32[]{:S(2)}) async-start(), calls=%async_computation.5 | async-start | bytes 9052160 | tf_op jit(solution)/shard_map/all_gather | solution.py:379
  7.6 7.3 %collective-permute-start.1 = (bf16[32,2176]{1,0:T(8,128)(2,1)S(1)}, bf16[32,2176]{1,0:T(8,128)(2,1)S(1)}, u32[]{:S(2)}, u32[]{:S(2)}) collective-permute-start(bf16[32,2176]{1,0:T(8,128)(2,1)S(1)} %concatenate.3), channel_id=1, source_target_pairs={{0,0},{1,8},{8,1},{9,9},{2,2},{3,10},{10,3},{11,11},{4,4},{5,12},{... | collective-permute-start | bytes 417800 | tf_op jit(solution)/shard_map/ppermute | solution.py:378
  14.9 0.7 copy-start.4
  18.4 52.1 %copy-start.2 = (bf16[256,2048]{1,0:T(8,128)(2,1)S(1)}, bf16[256,2048]{1,0:T(8,128)(2,1)}, u32[]{:S(2)}) copy-start(bf16[256,2048]{1,0:T(8,128)(2,1)} %own_ref.1) | copy-start | bytes 3145732
  18.4 121.4 %copy-start.3 = (f32[2048]{0:T(1024)S(1)}, f32[2048]{0:T(1024)}, u32[]{:S(2)}) copy-start(f32[2048]{0:T(1024)} %param.22) | copy-start | bytes 24580
  18.4 36.0 %all-to-all-start = ((bf16[8,192,256]{2,1,0:T(8,128)(2,1)}), bf16[8,192,256]{2,1,0:T(8,128)(2,1)S(1)}, u32[]{:S(2)}, u32[]{:S(2)}) async-start(bf16[8,192,256]{2,1,0:T(8,128)(2,1)} %get-tuple-element.9), calls=%async_computation | async-start | bytes 1572864 | tf_op jit(solution)/shard_map/all_to_all | solution.py:382
  63.8 37.1 %all-to-all-start.1 = ((bf16[8,208,256]{2,1,0:T(8,128)(2,1)}), bf16[8,208,256]{2,1,0:T(8,128)(2,1)S(1)}, u32[]{:S(2)}, u32[]{:S(2)}) async-start(bf16[8,208,256]{2,1,0:T(8,128)(2,1)} %attend.1), calls=%async_computation.1 | async-start | bytes 1703936 | tf_op jit(solution)/shard_map/all_to_all | solution.py:385
  70.4 44.9 %collective-permute-start = (bf16[256,2048]{1,0:T(8,128)(2,1)S(1)}, bf16[256,2048]{1,0:T(8,128)(2,1)}, u32[]{:S(2)}, u32[]{:S(2)}) collective-permute-start(bf16[256,2048]{1,0:T(8,128)(2,1)S(1)} %copy-done.2), channel_id=1, source_target_pairs={{0,1},{1,0},{2,3},{3,2},{4,5},{5,4},{6,7},{7,6},{8,9},{9,8},{10,11... | collective-permute-start | bytes 3145736 | tf_op jit(solution)/shard_map/ppermute | solution.py:384
  117.8 22.0 %all-to-all-start.2 = ((bf16[4,24,2048]{2,1,0:T(8,128)(2,1)}), bf16[4,24,2048]{2,1,0:T(8,128)(2,1)S(1)}, u32[]{:S(2)}, u32[]{:S(2)}) async-start(bf16[4,24,2048]{2,1,0:T(8,128)(2,1)} %bitcast.3), calls=%async_computation.2 | async-start | bytes 786432 | tf_op jit(solution)/shard_map/all_to_all | solution.py:355
  139.8 17.7 %copy-start.1 = (bf16[2048,2176]{1,0:T(8,128)(2,1)S(1)}, bf16[2048,2176]{1,0:T(8,128)(2,1)}, u32[]{:S(2)}) copy-start(bf16[2048,2176]{1,0:T(8,128)(2,1)} %all-gather.3.cloned.1.call-done.w_ref) | copy-start | bytes 26738692
Sparse Core Ops, SparseCore 0:
  15.7 123.3 all-gather.2

commit v6 on v4

--- a/solution.py
+++ b/solution.py
@@ -32,7 +32,26 @@
     return inverse[None, :], sign[None, :], cosine, sine
 
 
-def prep_kernel(q_ref, k_ref, v_ref, qg_ref, kg_ref, inv_ref, sign_ref, cos_ref, sin_ref, qo_ref, kvo_ref):
+def prep_kernel(
+    q_ref,
+    k_ref,
+    v_ref,
+    gate_ref,
+    up_ref,
+    down_ref,
+    qg_ref,
+    kg_ref,
+    inv_ref,
+    sign_ref,
+    cos_ref,
+    sin_ref,
+    wo_ref,
+    qo_ref,
+    kvo_ref,
+):
+    units = gate_ref.shape[1]
+    for n, ref in enumerate((gate_ref, up_ref, down_ref)):
+        wo_ref[:, n * units : (n + 1) * units] = ref[...]
     rows, head_dim = k_ref.shape
     heads = q_ref.shape[1] // head_dim
     quarter = head_dim // 4
@@ -70,12 +89,13 @@
     kvo_ref[:, head_dim:] = v_ref[...]
 
 
-def prep(query, key, value, q_gain, k_gain, copies):
+def prep(query, key, value, gate, up, down, q_gain, k_gain, copies):
     rows, head_dim = key.shape
     inverse, sign, cosine, sine = rope_tables(head_dim)
     return pl.pallas_call(
         prep_kernel,
         out_shape=(
+            jax.ShapeDtypeStruct((gate.shape[0], 3 * gate.shape[1]), BF16),
             jax.ShapeDtypeStruct((copies, *query.shape), BF16),
             jax.ShapeDtypeStruct((rows, 2 * head_dim), BF16),
         ),
@@ -84,6 +104,9 @@
         query,
         key,
         value,
+        gate,
+        up,
+        down,
         q_gain.reshape(1, -1),
         k_gain.reshape(1, -1),
         jnp.asarray(inverse),
@@ -275,9 +298,9 @@
     )(attn, own, other)
 
 
-def feed_kernel(x_ref, w_hbm, o_ref, w_ref, acc_ref, sems, *, units):
+def feed_kernel(x_hbm, w_hbm, o_ref, x_ref, w_ref, acc_ref, sems, *, units):
     depth, width = w_ref.shape
-    pieces = sems.shape[0]
+    pieces = sems.shape[0] - 1
     block = depth // pieces
     both = 2 * units
     spare = width - 3 * units
@@ -286,6 +309,9 @@
         at = pl.ds(i * block, block)
         copies.append(pltpu.make_async_copy(w_hbm.at[at], w_ref.at[at], sems.at[i]))
         copies[-1].start()
+    rows_copy = pltpu.make_async_copy(x_hbm, x_ref, sems.at[pieces])
+    rows_copy.start()
+    rows_copy.wait()
     for i in range(pieces):
         at = pl.ds(i * block, block)
         copies[i].wait()
@@ -308,16 +334,16 @@
     rows, depth = x.shape
     width = weights.shape[1]
     pieces = 8
-    vmem = pl.BlockSpec(memory_space=pltpu.VMEM)
     return pl.pallas_call(
         functools.partial(feed_kernel, units=units),
-        in_specs=[vmem, pl.BlockSpec(memory_space=pl.ANY)],
-        out_specs=vmem,
+        in_specs=[pl.BlockSpec(memory_space=pl.ANY)] * 2,
+        out_specs=pl.BlockSpec(memory_space=pltpu.VMEM),
         out_shape=jax.ShapeDtypeStruct((rows, depth), BF16),
         scratch_shapes=[
+            pltpu.VMEM((rows, depth), BF16),
             pltpu.VMEM((depth, width), BF16),
             pltpu.VMEM((rows, 2 * units), F32),
-            pltpu.SemaphoreType.DMA((pieces,)),
+            pltpu.SemaphoreType.DMA((pieces + 1,)),
         ],
         compiler_params=pltpu.CompilerParams(vmem_limit_bytes=60 * 2**20),
         cost_estimate=pl.CostEstimate(
@@ -327,17 +353,35 @@
     )(x, weights)
 
 
-def normalize(stream, gain):
+def stream_kernel(part_ref, resid_ref, gain_ref, stream_ref, normed_ref):
+    proj = part_ref[0].astype(F32)
+    for n in range(1, part_ref.shape[0]):
+        proj = proj + part_ref[n].astype(F32)
+    stream = (resid_ref[...].astype(F32) + proj).astype(BF16)
+    stream_ref[...] = stream
     values = stream.astype(F32)
-    return (
-        values * lax.rsqrt(jnp.mean(values * values, axis=-1, keepdims=True) + EPSILON) * gain
-    ).astype(BF16)
-
-
-def summed_over(x, axis):
+    normed = values * lax.rsqrt(jnp.mean(values * values, axis=-1, keepdims=True) + EPSILON)
+    normed_ref[...] = (normed * gain_ref[...]).astype(BF16)
+
+
+def stream_rows(parts, resid, gain):
+    return pl.pallas_call(
+        stream_kernel,
+        out_shape=(
+            jax.ShapeDtypeStruct(resid.shape, BF16),
+            jax.ShapeDtypeStruct(resid.shape, BF16),
+        ),
+        compiler_params=pltpu.CompilerParams(vmem_limit_bytes=8 * 2**20),
+        cost_estimate=pl.CostEstimate(
+            flops=8 * resid.size, bytes_accessed=2**20, transcendentals=0
+        ),
+        name="stream",
+    )(parts, resid, gain.reshape(1, -1))
+
+
+def scattered(x, axis):
     count = lax.axis_size(axis)
-    blocks = lax.all_to_all(x.reshape(count, -1, x.shape[1]), axis, 0, 0, tiled=True)
-    return jnp.sum(blocks.astype(F32), axis=0)
+    return lax.all_to_all(x.reshape(count, -1, x.shape[1]), axis, 0, 0, tiled=True)
 
 
 def body(
@@ -355,24 +399,29 @@
 ):
     rows = query.shape[0]
     units = gate_weight.shape[1]
-    shard = [gate_weight, up_weight, down_weight.T]
-    spare = -(3 * units) % 128
-    if spare:
-        shard.append(jnp.zeros((gate_weight.shape[0], spare), BF16))
-    weights = lax.all_gather(jnp.concatenate(shard, axis=1), SP, axis=0, tiled=True)
-
-    copies, keys_values = prep(query, key, value, q_gain, k_gain, lax.axis_size("sp_1"))
+    shard, copies, keys_values = prep(
+        query,
+        key,
+        value,
+        gate_weight,
+        up_weight,
+        down_weight.T,
+        q_gain,
+        k_gain,
+        lax.axis_size("sp_1"),
+    )
+    weights = lax.all_gather(shard, SP, axis=0, tiled=True)
     queries = lax.all_to_all(copies, "sp_1", 0, 0, tiled=True)
     keys_values = lax.all_gather(keys_values, "sp_0", axis=0, tiled=True)
     other_weight = lax.ppermute(out_weight, "c", [(0, 1), (1, 0)])
     partial = lax.all_to_all(attend(queries, keys_values), "sp_1", 0, 0, tiled=True)
     attn = lax.all_gather(combine(partial), "c", axis=0)
-    proj = summed_over(project(attn, out_weight, other_weight), "x")
+    parts = scattered(project(attn, out_weight, other_weight), "x")
     share = rows // lax.axis_size(TP)
     my_resid = lax.dynamic_slice_in_dim(resid, lax.axis_index(TP) * share, share, 0)
-    my_stream = (my_resid.astype(F32) + proj).astype(BF16)
-    normed = lax.all_gather(normalize(my_stream, norm_gain), TP, axis=0, tiled=True)
-    down = summed_over(feed(normed, weights, units), TP)
+    my_stream, normed = stream_rows(parts, my_resid, norm_gain)
+    normed = lax.all_gather(normed, TP, axis=0, tiled=True)
+    down = jnp.sum(scattered(feed(normed, weights, units), TP).astype(F32), axis=0)
     return (my_stream.astype(F32) + 0.5 * down).astype(BF16)
 
 

time: 160 us -> 160 us (level)
  Pallas kernels: 20.4 us -> 23.8 us
  local copies, waits for them, and re-layouts: 1.71 us -> 0.02 us
    concatenate x1 -> x0, local copies, waits for them, and re-layouts: 1.7 us -> none  [body(): jnp.concatenate(shard, axis=1)]
    pallas_call x2 -> x3, Pallas kernels: 9.88 us -> 11.5 us  [the longest x1 8.31 us: feed(): pl.pallas_call(functools.partial(feed_kernel, units=units), in_specs=[pl....]
  transfers between devices with their start and end apart: 5 -> 5, of which waited for: 2 -> 2; matrix products, arithmetic and copies ran while one was open for 1% -> 0% of each run, Pallas kernels for 8% -> 8%
where the time goes in v6:
time: 160 us
  blocking collectives  76.6 us (48%)
  starting transfers between devices  26.3 us (16%)
  Pallas kernels  23.8 us (15%)
  waiting for transfers between devices  18.8 us (12%)
  between operations  13.4 us (8%)
    all_gather x1, blocking collectives, body(): keys_values = lax.all_gather(keys_values, 'sp_0', axis=0, tiled=True)  28.4 us
    all_to_all x1, blocking collectives, scattered(): lax.all_to_all(x.reshape(count, -1, x.shape[1]), axis, 0, 0, tiled=True)  17 us
    all_gather x1, blocking collectives, body(): normed = lax.all_gather(normed, TP, axis=0, tiled=True)  16 us
    all_gather x1, blocking collectives, body(): attn = lax.all_gather(combine(partial), 'c', axis=0)  15.1 us
    all_to_all x1, waiting for transfers between devices, body(): lax.all_to_all(attend(queries, keys_values), 'sp_1', 0, 0, tiled=True)  11.5 us
    pallas_call x1, Pallas kernels, attend(): pl.pallas_call(functools.partial(attend_kernel, chunk=next((n for n in (5...  9.38 us
    ppermute x1, starting transfers between devices, body(): other_weight = lax.ppermute(out_weight, 'c', [(0, 1), (1, 0)])  8.51 us
    pallas_call x1, Pallas kernels, feed(): pl.pallas_call(functools.partial(feed_kernel, units=units), in_specs=[pl....  8.31 us
  transfers between devices with their start and end apart: 5, of which 2 were waited for; matrix products, arithmetic and copies ran while one was open for 0% of the time, Pallas kernels for 8%

profile of v6, /device:TPU:1, one launch (start us, length us, event | category | flops | bytes accessed | tf_op | source)
XLA Modules:
  0.0 159.8 jit_solution(8144893494116138327)
XLA Ops:
  6.5 0.0 copy-start
  6.5 0.0 copy-start.1
  6.5 0.0 all-gather.3.cloned.1.call-start
  6.5 3.0 %prep.1 = (bf16[32,2112]{1,0:T(8,128)(2,1)}, bf16[8,192,256]{2,1,0:T(8,128)(2,1)}, bf16[192,256]{1,0:T(8,128)(2,1)}) custom-call(bf16[192,256]{1,0:T(8,128)(2,1)} %q_ref.1, bf16[192,128]{1,0:T(8,128)(2,1)} %k_ref.1, bf16[192,128]{1,0:T(8,128)(2,1)} %v_ref.1, bf16[32,704]{1,0:T(8,128)(2,1)} %gate_ref.1, bf16[32,704]{1,0:T(8,128)(2,1)} %up_ref.1, ...), custom_call_target="tpu_custom_call" | custom-call | tf_op jit(solution)/shard_map/prep/pallas_call | solution.py:95
  9.5 0.0 all-gather.3.cloned.1.call-update
  9.5 0.0 copy-start.2
  9.6 7.7 %all-to-all-start = ((bf16[8,192,256]{2,1,0:T(8,128)(2,1)}), bf16[8,192,256]{2,1,0:T(8,128)(2,1)S(1)}, u32[]{:S(2)}, u32[]{:S(2)}) async-start(bf16[8,192,256]{2,1,0:T(8,128)(2,1)} %get-tuple-element.10), calls=%async_computation | async-start | bytes 1572864 | tf_op jit(solution)/shard_map/all_to_all | solution.py:414
  17.2 28.4 %all_gather.15.kv_ref = bf16[1536,256]{1,0:T(8,128)(2,1)S(1)} all-gather(bf16[192,256]{1,0:T(8,128)(2,1)} %get-tuple-element.11), channel_id=1, replica_groups=mesh['sp_0'=8,'sp_1'=8,'x'=4,'c'=2] {'sp_0'}, dimensions={0}, use_global_device_ids=true | all-gather | bytes 884736 | tf_op jit(solution)/shard_map/all_gather | solution.py:415
  45.6 0.0 all-to-all-done.q_ref.next_ref
  45.6 9.4 %attend.1 = bf16[8,208,256]{2,1,0:T(8,128)(2,1)} custom-call(bf16[8,192,256]{2,1,0:T(8,128)(2,1)S(1)} %all-to-all-done.q_ref.next_ref, bf16[8,192,256]{2,1,0:T(8,128)(2,1)S(1)} %all-to-all-done.q_ref.next_ref, bf16[1536,256]{1,0:T(8,128)(2,1)S(1)} %all_gather.15.kv_ref), custom_call_target="tpu_custom_call" | custom-call | flops 2415919104 | bytes 4194304 | tf_op jit(solution)/shard_map/attend/pallas_call | solution.py:201
  55.0 6.6 %all-to-all-start.1 = ((bf16[8,208,256]{2,1,0:T(8,128)(2,1)}), bf16[8,208,256]{2,1,0:T(8,128)(2,1)S(1)}, u32[]{:S(2)}, u32[]{:S(2)}) async-start(bf16[8,208,256]{2,1,0:T(8,128)(2,1)} %attend.1), calls=%async_computation.1 | async-start | bytes 1703936 | tf_op jit(solution)/shard_map/all_to_all | solution.py:417
  61.6 0.0 copy-done.1
  61.6 8.5 %collective-permute-start = (bf16[256,2048]{1,0:T(8,128)(2,1)S(1)}, bf16[256,2048]{1,0:T(8,128)(2,1)}, u32[]{:S(2)}, u32[]{:S(2)}) collective-permute-start(bf16[256,2048]{1,0:T(8,128)(2,1)S(1)} %copy-done.1), channel_id=1, source_target_pairs={{0,1},{1,0},{2,3},{3,2},{4,5},{5,4},{6,7},{7,6},{8,9},{9,8},{10,11... | collective-permute-start | bytes 3145736 | tf_op jit(solution)/shard_map/ppermute | solution.py:416
  70.1 11.5 %all-to-all-done.1.part_ref = bf16[8,208,256]{2,1,0:T(8,128)(2,1)S(1)} async-done(((bf16[8,208,256]{2,1,0:T(8,128)(2,1)}), bf16[8,208,256]{2,1,0:T(8,128)(2,1)S(1)}, u32[]{:S(2)}, u32[]{:S(2)}) %all-to-all-start.1) | async-done | bytes 852000 | tf_op jit(solution)/shard_map/all_to_all | solution.py:417
  81.6 0.5 combine.1
  82.2 15.1 %all-gather = bf16[4,96,256]{2,1,0:T(8,128)(2,1)S(1)} all-gather(bf16[2,96,256]{2,1,0:T(8,128)(2,1)S(1)} %combine.1), channel_id=2, replica_groups=mesh['sp_0'=8,'sp_1'=8,'x'=4,'c'=2] {'c'}, dimensions={0}, use_global_device_ids=true | all-gather | bytes 294912 | tf_op jit(solution)/shard_map/all_gather | solution.py:418
  97.3 0.0 collective-permute-done.other_ref
  97.3 2.4 %project.1 = bf16[96,2048]{1,0:T(8,128)(2,1)} custom-call(bf16[2,2,96,256]{3,2,1,0:T(8,128)(2,1)S(1)} %bitcast.7, bf16[256,2048]{1,0:T(8,128)(2,1)S(1)} %copy-done.1, bf16[256,2048]{1,0:T(8,128)(2,1)} %collective-permute-done.other_ref), custom_call_target="tpu_custom_call" | custom-call | flops 201326592 | bytes 3145728 | tf_op jit(solution)/shard_map/project/pallas_call | solution.py:290
  99.7 3.5 %all-to-all-start.2 = ((bf16[4,24,2048]{2,1,0:T(8,128)(2,1)}), bf16[4,24,2048]{2,1,0:T(8,128)(2,1)S(1)}, u32[]{:S(2)}, u32[]{:S(2)}) async-start(bf16[4,24,2048]{2,1,0:T(8,128)(2,1)} %bitcast.4), calls=%async_computation.2 | async-start | bytes 786432 | tf_op jit(solution)/shard_map/all_to_all | solution.py:384
  103.3 0.0 copy-done
  103.3 7.3 %all-to-all-done.2.part_ref = bf16[4,24,2048]{2,1,0:T(8,128)(2,1)S(1)} async-done(((bf16[4,24,2048]{2,1,0:T(8,128)(2,1)}), bf16[4,24,2048]{2,1,0:T(8,128)(2,1)S(1)}, u32[]{:S(2)}, u32[]{:S(2)}) %all-to-all-start.2) | async-done | bytes 393248 | tf_op jit(solution)/shard_map/all_to_all | solution.py:384
  110.6 0.0 copy-done.2
  110.6 0.2 stream.1
  110.8 16.0 %all_gather.18.x_hbm = bf16[192,2048]{1,0:T(8,128)(2,1)} all-gather(bf16[24,2048]{1,0:T(8,128)(2,1)S(1)} %get-tuple-element.13), channel_id=1, replica_groups=mesh['sp_0'=8,'sp_1'=8,'x'=4,'c'=2] {'x','c'}, dimensions={0}, use_global_device_ids=true | all-gather | bytes 884736 | tf_op jit(solution)/shard_map/all_gather | solution.py:423
  126.8 0.0 all-gather.3.cloned.1.call-done.w_hbm
  126.8 8.3 %feed.1 = bf16[192,2048]{1,0:T(8,128)(2,1)} custom-call(bf16[192,2048]{1,0:T(8,128)(2,1)} %all_gather.18.x_hbm, bf16[2048,2112]{1,0:T(8,128)(2,1)} %all-gather.3.cloned.1.call-done.w_hbm), custom_call_target="tpu_custom_call" | custom-call | flops 1660944384 | bytes 10485760 | tf_op jit(solution)/shard_map/feed/pallas_call | solution.py:337
  135.1 17.0 %all_to_all.20 = bf16[8,24,2048]{2,1,0:T(8,128)(2,1)S(1)} all-to-all(bf16[8,24,2048]{2,1,0:T(8,128)(2,1)} %bitcast.9), channel_id=1, replica_groups=mesh['sp_0'=8,'sp_1'=8,'x'=4,'c'=2] {'x','c'}, dimensions={0} | all-to-all | bytes 1572864 | tf_op jit(solution)/shard_map/all_to_all | solution.py:384
  152.1 0.1 convert_reduce_fusion
  152.2 0.7 add_convert_fusion
  (1 shorter events, 0.0 us)
Async XLA Ops:
  6.5 96.8 %copy-start = (bf16[192,2048]{1,0:T(8,128)(2,1)S(1)}, bf16[192,2048]{1,0:T(8,128)(2,1)}, u32[]{:S(2)}) copy-start(bf16[192,2048]{1,0:T(8,128)(2,1)} %param.15) | copy-start | bytes 2359300
  6.5 55.1 %copy-start.1 = (bf16[256,2048]{1,0:T(8,128)(2,1)S(1)}, bf16[256,2048]{1,0:T(8,128)(2,1)}, u32[]{:S(2)}) copy-start(bf16[256,2048]{1,0:T(8,128)(2,1)} %own_ref.1) | copy-start | bytes 3145732
  6.5 120.3 %all-gather.3.cloned.1.call-start = ((), (), s32[]{:S(2)}) async-start(), calls=%async_computation.4 | async-start | bytes 9052160 | tf_op jit(solution)/shard_map/all_gather | solution.py:413
  9.5 101.0 %copy-start.2 = (f32[2048]{0:T(1024)S(1)}, f32[2048]{0:T(1024)}, u32[]{:S(2)}) copy-start(f32[2048]{0:T(1024)} %param.22) | copy-start | bytes 24580
  9.6 36.1 %all-to-all-start = ((bf16[8,192,256]{2,1,0:T(8,128)(2,1)}), bf16[8,192,256]{2,1,0:T(8,128)(2,1)S(1)}, u32[]{:S(2)}, u32[]{:S(2)}) async-start(bf16[8,192,256]{2,1,0:T(8,128)(2,1)} %get-tuple-element.10), calls=%async_computation | async-start | bytes 1572864 | tf_op jit(solution)/shard_map/all_to_all | solution.py:414
  55.0 26.6 %all-to-all-start.1 = ((bf16[8,208,256]{2,1,0:T(8,128)(2,1)}), bf16[8,208,256]{2,1,0:T(8,128)(2,1)S(1)}, u32[]{:S(2)}, u32[]{:S(2)}) async-start(bf16[8,208,256]{2,1,0:T(8,128)(2,1)} %attend.1), calls=%async_computation.1 | async-start | bytes 1703936 | tf_op jit(solution)/shard_map/all_to_all | solution.py:417
  61.6 35.7 %collective-permute-start = (bf16[256,2048]{1,0:T(8,128)(2,1)S(1)}, bf16[256,2048]{1,0:T(8,128)(2,1)}, u32[]{:S(2)}, u32[]{:S(2)}) collective-permute-start(bf16[256,2048]{1,0:T(8,128)(2,1)S(1)} %copy-done.1), channel_id=1, source_target_pairs={{0,1},{1,0},{2,3},{3,2},{4,5},{5,4},{6,7},{7,6},{8,9},{9,8},{10,11... | collective-permute-start | bytes 3145736 | tf_op jit(solution)/shard_map/ppermute | solution.py:416
  99.7 10.8 %all-to-all-start.2 = ((bf16[4,24,2048]{2,1,0:T(8,128)(2,1)}), bf16[4,24,2048]{2,1,0:T(8,128)(2,1)S(1)}, u32[]{:S(2)}, u32[]{:S(2)}) async-start(bf16[4,24,2048]{2,1,0:T(8,128)(2,1)} %bitcast.4), calls=%async_computation.2 | async-start | bytes 786432 | tf_op jit(solution)/shard_map/all_to_all | solution.py:384
Sparse Core Ops, SparseCore 0:
  10.3 116.2 all-gather.2

commit v7 on v6

--- a/solution.py
+++ b/solution.py
@@ -52,6 +52,9 @@
     units = gate_ref.shape[1]
     for n, ref in enumerate((gate_ref, up_ref, down_ref)):
         wo_ref[:, n * units : (n + 1) * units] = ref[...]
+    spare = wo_ref.shape[1] - 3 * units
+    if spare:
+        wo_ref[:, 3 * units :] = jnp.zeros((wo_ref.shape[0], spare), BF16)
     rows, head_dim = k_ref.shape
     heads = q_ref.shape[1] // head_dim
     quarter = head_dim // 4
@@ -95,7 +98,7 @@
     return pl.pallas_call(
         prep_kernel,
         out_shape=(
-            jax.ShapeDtypeStruct((gate.shape[0], 3 * gate.shape[1]), BF16),
+            jax.ShapeDtypeStruct((gate.shape[0], -(-3 * gate.shape[1] // 128) * 128), BF16),
             jax.ShapeDtypeStruct((copies, *query.shape), BF16),
             jax.ShapeDtypeStruct((rows, 2 * head_dim), BF16),
         ),
@@ -304,13 +307,13 @@
     block = depth // pieces
     both = 2 * units
     spare = width - 3 * units
+    rows_copy = pltpu.make_async_copy(x_hbm, x_ref, sems.at[pieces])
+    rows_copy.start()
     copies = []
     for i in range(pieces):
         at = pl.ds(i * block, block)
         copies.append(pltpu.make_async_copy(w_hbm.at[at], w_ref.at[at], sems.at[i]))
         copies[-1].start()
-    rows_copy = pltpu.make_async_copy(x_hbm, x_ref, sems.at[pieces])
-    rows_copy.start()
     rows_copy.wait()
     for i in range(pieces):
         at = pl.ds(i * block, block)
@@ -408,13 +411,13 @@
         down_weight.T,
         q_gain,
         k_gain,
-        lax.axis_size("sp_1"),
+        lax.axis_size("sp_0"),
     )
     weights = lax.all_gather(shard, SP, axis=0, tiled=True)
-    queries = lax.all_to_all(copies, "sp_1", 0, 0, tiled=True)
-    keys_values = lax.all_gather(keys_values, "sp_0", axis=0, tiled=True)
+    queries = lax.all_to_all(copies, "sp_0", 0, 0, tiled=True)
+    keys_values = lax.all_gather(keys_values, "sp_1", axis=0, tiled=True)
     other_weight = lax.ppermute(out_weight, "c", [(0, 1), (1, 0)])
-    partial = lax.all_to_all(attend(queries, keys_values), "sp_1", 0, 0, tiled=True)
+    partial = lax.all_to_all(attend(queries, keys_values), "sp_0", 0, 0, tiled=True)
     attn = lax.all_gather(combine(partial), "c", axis=0)
     parts = scattered(project(attn, out_weight, other_weight), "x")
     share = rows // lax.axis_size(TP)

time: 160 us -> 157 us (0.981)
  blocking collectives: 76.6 us -> 67 us
  waiting for transfers between devices: 18.8 us -> 23.9 us
  starting transfers between devices: 26.3 us -> 29.6 us
  Pallas kernels: 23.8 us -> 21.6 us
    all_gather x1, blocking collectives: 28.4 us -> 23.7 us  [body(): keys_values = lax.all_gather(keys_values, 'sp_1', axis=0, tiled=True)]
    all_gather x1, blocking collectives: 15.1 us -> 10.4 us  [body(): attn = lax.all_gather(combine(partial), 'c', axis=0)]
    all_to_all x2, starting transfers between devices: 14.3 us -> 18.3 us  [the longest x1 10.9 us: body(): queries = lax.all_to_all(copies, 'sp_0', 0, 0, tiled=True)]
    all_to_all x2, waiting for transfers between devices: 11.5 us -> 14.8 us  [the longest x1 14.8 us: body(): lax.all_to_all(attend(queries, keys_values), 'sp_0', 0, 0, tiled=True)]
    pallas_call x1, Pallas kernels: 8.31 us -> 6.16 us  [feed(): pl.pallas_call(functools.partial(feed_kernel, units=units), in_specs=[pl....]
    all_gather x1, waiting for transfers between devices: 0.01 us -> 1.74 us  [body(): weights = lax.all_gather(shard, SP, axis=0, tiled=True)]
  transfers between devices with their start and end apart: 5 -> 5, of which waited for: 2 -> 3; matrix products, arithmetic and copies ran while one was open for 0% -> 0% of each run, Pallas kernels for 8% -> 8%
where the time goes in v7:
time: 157 us; the launch traced here: 156 us
  blocking collectives  67 us (43%)
  starting transfers between devices  29.6 us (19%)
  waiting for transfers between devices  23.9 us (15%)
  Pallas kernels  21.6 us (14%)
  between operations  13.4 us (9%)
    all_gather x1, blocking collectives, body(): keys_values = lax.all_gather(keys_values, 'sp_1', axis=0, tiled=True)  23.7 us
    all_to_all x1, blocking collectives, scattered(): lax.all_to_all(x.reshape(count, -1, x.shape[1]), axis, 0, 0, tiled=True)  16.9 us
    all_gather x1, blocking collectives, body(): normed = lax.all_gather(normed, TP, axis=0, tiled=True)  16 us
    all_to_all x1, waiting for transfers between devices, body(): lax.all_to_all(attend(queries, keys_values), 'sp_0', 0, 0, tiled=True)  14.8 us
    all_to_all x1, starting transfers between devices, body(): queries = lax.all_to_all(copies, 'sp_0', 0, 0, tiled=True)  10.9 us
    all_gather x1, blocking collectives, body(): attn = lax.all_gather(combine(partial), 'c', axis=0)  10.4 us
    pallas_call x1, Pallas kernels, attend(): pl.pallas_call(functools.partial(attend_kernel, chunk=next((n for n in (5...  9.38 us
    all_to_all x1, starting transfers between devices, body(): lax.all_to_all(attend(queries, keys_values), 'sp_0', 0, 0, tiled=True)  7.39 us
  transfers between devices with their start and end apart: 5, of which 3 were waited for; matrix products, arithmetic and copies ran while one was open for 0% of the time, Pallas kernels for 8%

profile of v7, /device:TPU:1, one launch (start us, length us, event | category | flops | bytes accessed | tf_op | source)
XLA Modules:
  0.0 156.4 jit_solution(15786921938881120578)
XLA Ops:
  6.5 0.0 copy-start
  6.5 0.0 copy-start.1
  6.5 0.0 all-gather.3.cloned.1.call-start
  6.5 3.0 %prep.1 = (bf16[32,2176]{1,0:T(8,128)(2,1)}, bf16[8,192,256]{2,1,0:T(8,128)(2,1)}, bf16[192,256]{1,0:T(8,128)(2,1)}) custom-call(bf16[192,256]{1,0:T(8,128)(2,1)} %q_ref.1, bf16[192,128]{1,0:T(8,128)(2,1)} %k_ref.1, bf16[192,128]{1,0:T(8,128)(2,1)} %v_ref.1, bf16[32,704]{1,0:T(8,128)(2,1)} %gate_ref.1, bf16[32,704]{1,0:T(8,128)(2,1)} %up_ref.1, ...), custom_call_target="tpu_custom_call" | custom-call | tf_op jit(solution)/shard_map/prep/pallas_call | solution.py:98
  9.5 0.0 all-gather.3.cloned.1.call-update
  9.5 0.0 copy-start.2
  9.6 10.9 %all-to-all-start = ((bf16[8,192,256]{2,1,0:T(8,128)(2,1)}), bf16[8,192,256]{2,1,0:T(8,128)(2,1)S(1)}, u32[]{:S(2)}, u32[]{:S(2)}) async-start(bf16[8,192,256]{2,1,0:T(8,128)(2,1)} %get-tuple-element.10), calls=%async_computation | async-start | bytes 1572864 | tf_op jit(solution)/shard_map/all_to_all | solution.py:417
  20.4 23.7 %all_gather.15.kv_ref = bf16[1536,256]{1,0:T(8,128)(2,1)S(1)} all-gather(bf16[192,256]{1,0:T(8,128)(2,1)} %get-tuple-element.11), channel_id=1, replica_groups=mesh['sp_0'=8,'sp_1'=8,'x'=4,'c'=2] {'sp_1'}, dimensions={0}, use_global_device_ids=true | all-gather | bytes 884736 | tf_op jit(solution)/shard_map/all_gather | solution.py:418
  44.1 0.0 all-to-all-done.q_ref.next_ref
  44.1 9.4 %attend.1 = bf16[8,208,256]{2,1,0:T(8,128)(2,1)} custom-call(bf16[8,192,256]{2,1,0:T(8,128)(2,1)S(1)} %all-to-all-done.q_ref.next_ref, bf16[8,192,256]{2,1,0:T(8,128)(2,1)S(1)} %all-to-all-done.q_ref.next_ref, bf16[1536,256]{1,0:T(8,128)(2,1)S(1)} %all_gather.15.kv_ref), custom_call_target="tpu_custom_call" | custom-call | flops 2415919104 | bytes 4194304 | tf_op jit(solution)/shard_map/attend/pallas_call | solution.py:204
  53.5 7.4 %all-to-all-start.1 = ((bf16[8,208,256]{2,1,0:T(8,128)(2,1)}), bf16[8,208,256]{2,1,0:T(8,128)(2,1)S(1)}, u32[]{:S(2)}, u32[]{:S(2)}) async-start(bf16[8,208,256]{2,1,0:T(8,128)(2,1)} %attend.1), calls=%async_computation.1 | async-start | bytes 1703936 | tf_op jit(solution)/shard_map/all_to_all | solution.py:420
  60.9 0.0 copy-done.1
  60.9 7.0 %collective-permute-start = (bf16[256,2048]{1,0:T(8,128)(2,1)S(1)}, bf16[256,2048]{1,0:T(8,128)(2,1)}, u32[]{:S(2)}, u32[]{:S(2)}) collective-permute-start(bf16[256,2048]{1,0:T(8,128)(2,1)S(1)} %copy-done.1), channel_id=1, source_target_pairs={{0,1},{1,0},{2,3},{3,2},{4,5},{5,4},{6,7},{7,6},{8,9},{9,8},{10,11... | collective-permute-start | bytes 3145736 | tf_op jit(solution)/shard_map/ppermute | solution.py:419
  67.9 14.8 %all-to-all-done.1.part_ref = bf16[8,208,256]{2,1,0:T(8,128)(2,1)S(1)} async-done(((bf16[8,208,256]{2,1,0:T(8,128)(2,1)}), bf16[8,208,256]{2,1,0:T(8,128)(2,1)S(1)}, u32[]{:S(2)}, u32[]{:S(2)}) %all-to-all-start.1) | async-done | bytes 852000 | tf_op jit(solution)/shard_map/all_to_all | solution.py:420
  82.7 0.5 combine.1
  83.3 10.4 %all-gather = bf16[4,96,256]{2,1,0:T(8,128)(2,1)S(1)} all-gather(bf16[2,96,256]{2,1,0:T(8,128)(2,1)S(1)} %combine.1), channel_id=2, replica_groups=mesh['sp_0'=8,'sp_1'=8,'x'=4,'c'=2] {'c'}, dimensions={0}, use_global_device_ids=true | all-gather | bytes 294912 | tf_op jit(solution)/shard_map/all_gather | solution.py:421
  93.7 0.0 collective-permute-done.other_ref
  93.7 2.4 %project.1 = bf16[96,2048]{1,0:T(8,128)(2,1)} custom-call(bf16[2,2,96,256]{3,2,1,0:T(8,128)(2,1)S(1)} %bitcast.7, bf16[256,2048]{1,0:T(8,128)(2,1)S(1)} %copy-done.1, bf16[256,2048]{1,0:T(8,128)(2,1)} %collective-permute-done.other_ref), custom_call_target="tpu_custom_call" | custom-call | flops 201326592 | bytes 3145728 | tf_op jit(solution)/shard_map/project/pallas_call | solution.py:293
  96.2 4.3 %all-to-all-start.2 = ((bf16[4,24,2048]{2,1,0:T(8,128)(2,1)}), bf16[4,24,2048]{2,1,0:T(8,128)(2,1)S(1)}, u32[]{:S(2)}, u32[]{:S(2)}) async-start(bf16[4,24,2048]{2,1,0:T(8,128)(2,1)} %bitcast.4), calls=%async_computation.2 | async-start | bytes 786432 | tf_op jit(solution)/shard_map/all_to_all | solution.py:387
  100.4 0.0 copy-done
  100.5 7.3 %all-to-all-done.2.part_ref = bf16[4,24,2048]{2,1,0:T(8,128)(2,1)S(1)} async-done(((bf16[4,24,2048]{2,1,0:T(8,128)(2,1)}), bf16[4,24,2048]{2,1,0:T(8,128)(2,1)S(1)}, u32[]{:S(2)}, u32[]{:S(2)}) %all-to-all-start.2) | async-done | bytes 393248 | tf_op jit(solution)/shard_map/all_to_all | solution.py:387
  107.7 0.0 copy-done.2
  107.7 0.2 stream.1
  107.9 16.0 %all_gather.18.x_hbm = bf16[192,2048]{1,0:T(8,128)(2,1)} all-gather(bf16[24,2048]{1,0:T(8,128)(2,1)S(1)} %get-tuple-element.13), channel_id=1, replica_groups=mesh['sp_0'=8,'sp_1'=8,'x'=4,'c'=2] {'x','c'}, dimensions={0}, use_global_device_ids=true | all-gather | bytes 884736 | tf_op jit(solution)/shard_map/all_gather | solution.py:426
  124.0 1.7 %all-gather.3.cloned.1.call-done.w_hbm = bf16[2048,2176]{1,0:T(8,128)(2,1)} async-done(((bf16[32,2176]{1,0:T(8,128)(2,1)}), bf16[2048,2176]{1,0:T(8,128)(2,1)}) %all-gather.3.cloned.1.call-update) | async-done | bytes 8912912 | tf_op jit(solution)/shard_map/all_gather | solution.py:416
  125.7 6.2 %feed.1 = bf16[192,2048]{1,0:T(8,128)(2,1)} custom-call(bf16[192,2048]{1,0:T(8,128)(2,1)} %all_gather.18.x_hbm, bf16[2048,2176]{1,0:T(8,128)(2,1)} %all-gather.3.cloned.1.call-done.w_hbm), custom_call_target="tpu_custom_call" | custom-call | flops 1660944384 | bytes 10485760 | tf_op jit(solution)/shard_map/feed/pallas_call | solution.py:340
  131.9 16.9 %all_to_all.20 = bf16[8,24,2048]{2,1,0:T(8,128)(2,1)S(1)} all-to-all(bf16[8,24,2048]{2,1,0:T(8,128)(2,1)} %bitcast.9), channel_id=1, replica_groups=mesh['sp_0'=8,'sp_1'=8,'x'=4,'c'=2] {'x','c'}, dimensions={0} | all-to-all | bytes 1572864 | tf_op jit(solution)/shard_map/all_to_all | solution.py:387
  148.8 0.1 convert_reduce_fusion
  148.9 0.7 add_convert_fusion
  (1 shorter events, 0.0 us)
Async XLA Ops:
  6.5 93.9 %copy-start = (bf16[192,2048]{1,0:T(8,128)(2,1)S(1)}, bf16[192,2048]{1,0:T(8,128)(2,1)}, u32[]{:S(2)}) copy-start(bf16[192,2048]{1,0:T(8,128)(2,1)} %param.15) | copy-start | bytes 2359300
  6.5 54.3 %copy-start.1 = (bf16[256,2048]{1,0:T(8,128)(2,1)S(1)}, bf16[256,2048]{1,0:T(8,128)(2,1)}, u32[]{:S(2)}) copy-start(bf16[256,2048]{1,0:T(8,128)(2,1)} %own_ref.1) | copy-start | bytes 3145732
  6.5 119.2 %all-gather.3.cloned.1.call-start = ((), (), s32[]{:S(2)}) async-start(), calls=%async_computation.4 | async-start | bytes 9052160 | tf_op jit(solution)/shard_map/all_gather | solution.py:416
  9.5 98.2 %copy-start.2 = (f32[2048]{0:T(1024)S(1)}, f32[2048]{0:T(1024)}, u32[]{:S(2)}) copy-start(f32[2048]{0:T(1024)} %param.22) | copy-start | bytes 24580
  9.6 34.5 %all-to-all-start = ((bf16[8,192,256]{2,1,0:T(8,128)(2,1)}), bf16[8,192,256]{2,1,0:T(8,128)(2,1)S(1)}, u32[]{:S(2)}, u32[]{:S(2)}) async-start(bf16[8,192,256]{2,1,0:T(8,128)(2,1)} %get-tuple-element.10), calls=%async_computation | async-start | bytes 1572864 | tf_op jit(solution)/shard_map/all_to_all | solution.py:417
  53.5 29.3 %all-to-all-start.1 = ((bf16[8,208,256]{2,1,0:T(8,128)(2,1)}), bf16[8,208,256]{2,1,0:T(8,128)(2,1)S(1)}, u32[]{:S(2)}, u32[]{:S(2)}) async-start(bf16[8,208,256]{2,1,0:T(8,128)(2,1)} %attend.1), calls=%async_computation.1 | async-start | bytes 1703936 | tf_op jit(solution)/shard_map/all_to_all | solution.py:420
  60.9 32.8 %collective-permute-start = (bf16[256,2048]{1,0:T(8,128)(2,1)S(1)}, bf16[256,2048]{1,0:T(8,128)(2,1)}, u32[]{:S(2)}, u32[]{:S(2)}) collective-permute-start(bf16[256,2048]{1,0:T(8,128)(2,1)S(1)} %copy-done.1), channel_id=1, source_target_pairs={{0,1},{1,0},{2,3},{3,2},{4,5},{5,4},{6,7},{7,6},{8,9},{9,8},{10,11... | collective-permute-start | bytes 3145736 | tf_op jit(solution)/shard_map/ppermute | solution.py:419
  96.2 11.6 %all-to-all-start.2 = ((bf16[4,24,2048]{2,1,0:T(8,128)(2,1)}), bf16[4,24,2048]{2,1,0:T(8,128)(2,1)S(1)}, u32[]{:S(2)}, u32[]{:S(2)}) async-start(bf16[4,24,2048]{2,1,0:T(8,128)(2,1)} %bitcast.4), calls=%async_computation.2 | async-start | bytes 786432 | tf_op jit(solution)/shard_map/all_to_all | solution.py:387
Sparse Core Ops, SparseCore 0:
  10.3 115.3 all-gather.2

commit v8 on v7

--- a/solution.py
+++ b/solution.py
@@ -301,20 +301,17 @@
     )(attn, own, other)
 
 
-def feed_kernel(x_hbm, w_hbm, o_ref, x_ref, w_ref, acc_ref, sems, *, units):
+def feed_kernel(x_ref, w_hbm, o_ref, w_ref, acc_ref, sems, *, units):
     depth, width = w_ref.shape
-    pieces = sems.shape[0] - 1
+    pieces = sems.shape[0]
     block = depth // pieces
     both = 2 * units
     spare = width - 3 * units
-    rows_copy = pltpu.make_async_copy(x_hbm, x_ref, sems.at[pieces])
-    rows_copy.start()
     copies = []
     for i in range(pieces):
         at = pl.ds(i * block, block)
         copies.append(pltpu.make_async_copy(w_hbm.at[at], w_ref.at[at], sems.at[i]))
         copies[-1].start()
-    rows_copy.wait()
     for i in range(pieces):
         at = pl.ds(i * block, block)
         copies[i].wait()
@@ -337,18 +334,18 @@
     rows, depth = x.shape
     width = weights.shape[1]
     pieces = 8
+    vmem = pl.BlockSpec(memory_space=pltpu.VMEM)
     return pl.pallas_call(
         functools.partial(feed_kernel, units=units),
-        in_specs=[pl.BlockSpec(memory_space=pl.ANY)] * 2,
-        out_specs=pl.BlockSpec(memory_space=pltpu.VMEM),
+        in_specs=[vmem, pl.BlockSpec(memory_space=pl.ANY)],
+        out_specs=vmem,
         out_shape=jax.ShapeDtypeStruct((rows, depth), BF16),
         scratch_shapes=[
-            pltpu.VMEM((rows, depth), BF16),
             pltpu.VMEM((depth, width), BF16),
             pltpu.VMEM((rows, 2 * units), F32),
-            pltpu.SemaphoreType.DMA((pieces + 1,)),
+            pltpu.SemaphoreType.DMA((pieces,)),
         ],
-        compiler_params=pltpu.CompilerParams(vmem_limit_bytes=60 * 2**20),
+        compiler_params=pltpu.CompilerParams(vmem_limit_bytes=50 * 2**20),
         cost_estimate=pl.CostEstimate(
             flops=6 * rows * depth * units, bytes_accessed=10 * 2**20, transcendentals=0
         ),

time: 157 us -> 156 us (level)
  no operation moved by 1% of the time
where the time goes in v8:
time: 156 us; the launch traced here: 155 us
  blocking collectives  65.7 us (42%)
  starting transfers between devices  29.6 us (19%)
  waiting for transfers between devices  25 us (16%)
  Pallas kernels  20.5 us (13%)
  between operations  13.4 us (9%)
    all_gather x1, blocking collectives, body(): keys_values = lax.all_gather(keys_values, 'sp_1', axis=0, tiled=True)  23.7 us
    all_to_all x1, blocking collectives, scattered(): lax.all_to_all(x.reshape(count, -1, x.shape[1]), axis, 0, 0, tiled=True)  16.7 us
    all_gather x1, blocking collectives, body(): normed = lax.all_gather(normed, TP, axis=0, tiled=True)  14.9 us
    all_to_all x1, waiting for transfers between devices, body(): lax.all_to_all(attend(queries, keys_values), 'sp_0', 0, 0, tiled=True)  14.8 us
    all_to_all x1, starting transfers between devices, body(): queries = lax.all_to_all(copies, 'sp_0', 0, 0, tiled=True)  10.9 us
    all_gather x1, blocking collectives, body(): attn = lax.all_gather(combine(partial), 'c', axis=0)  10.4 us
    pallas_call x1, Pallas kernels, attend(): pl.pallas_call(functools.partial(attend_kernel, chunk=next((n for n in (5...  9.38 us
    all_to_all x1, starting transfers between devices, body(): lax.all_to_all(attend(queries, keys_values), 'sp_0', 0, 0, tiled=True)  7.39 us
  transfers between devices with their start and end apart: 5, of which 3 were waited for; matrix products, arithmetic and copies ran while one was open for 0% of the time, Pallas kernels for 8%

profile of v8, /device:TPU:1, one launch (start us, length us, event | category | flops | bytes accessed | tf_op | source)
XLA Modules:
  0.0 155.1 jit_solution(7446190397750387504)
XLA Ops:
  6.5 0.0 copy-start
  6.5 0.0 copy-start.1
  6.5 0.0 all-gather.3.cloned.1.call-start
  6.5 3.0 %prep.1 = (bf16[32,2176]{1,0:T(8,128)(2,1)}, bf16[8,192,256]{2,1,0:T(8,128)(2,1)}, bf16[192,256]{1,0:T(8,128)(2,1)}) custom-call(bf16[192,256]{1,0:T(8,128)(2,1)} %q_ref.1, bf16[192,128]{1,0:T(8,128)(2,1)} %k_ref.1, bf16[192,128]{1,0:T(8,128)(2,1)} %v_ref.1, bf16[32,704]{1,0:T(8,128)(2,1)} %gate_ref.1, bf16[32,704]{1,0:T(8,128)(2,1)} %up_ref.1, ...), custom_call_target="tpu_custom_call" | custom-call | tf_op jit(solution)/shard_map/prep/pallas_call | solution.py:98
  9.5 0.0 all-gather.3.cloned.1.call-update
  9.5 0.0 copy-start.2
  9.6 10.9 %all-to-all-start = ((bf16[8,192,256]{2,1,0:T(8,128)(2,1)}), bf16[8,192,256]{2,1,0:T(8,128)(2,1)S(1)}, u32[]{:S(2)}, u32[]{:S(2)}) async-start(bf16[8,192,256]{2,1,0:T(8,128)(2,1)} %get-tuple-element.10), calls=%async_computation | async-start | bytes 1572864 | tf_op jit(solution)/shard_map/all_to_all | solution.py:414
  20.4 23.7 %all_gather.15.kv_ref = bf16[1536,256]{1,0:T(8,128)(2,1)S(1)} all-gather(bf16[192,256]{1,0:T(8,128)(2,1)} %get-tuple-element.11), channel_id=1, replica_groups=mesh['sp_0'=8,'sp_1'=8,'x'=4,'c'=2] {'sp_1'}, dimensions={0}, use_global_device_ids=true | all-gather | bytes 884736 | tf_op jit(solution)/shard_map/all_gather | solution.py:415
  44.1 0.0 all-to-all-done.q_ref.next_ref
  44.1 9.4 %attend.1 = bf16[8,208,256]{2,1,0:T(8,128)(2,1)} custom-call(bf16[8,192,256]{2,1,0:T(8,128)(2,1)S(1)} %all-to-all-done.q_ref.next_ref, bf16[8,192,256]{2,1,0:T(8,128)(2,1)S(1)} %all-to-all-done.q_ref.next_ref, bf16[1536,256]{1,0:T(8,128)(2,1)S(1)} %all_gather.15.kv_ref), custom_call_target="tpu_custom_call" | custom-call | flops 2415919104 | bytes 4194304 | tf_op jit(solution)/shard_map/attend/pallas_call | solution.py:204
  53.5 7.4 %all-to-all-start.1 = ((bf16[8,208,256]{2,1,0:T(8,128)(2,1)}), bf16[8,208,256]{2,1,0:T(8,128)(2,1)S(1)}, u32[]{:S(2)}, u32[]{:S(2)}) async-start(bf16[8,208,256]{2,1,0:T(8,128)(2,1)} %attend.1), calls=%async_computation.1 | async-start | bytes 1703936 | tf_op jit(solution)/shard_map/all_to_all | solution.py:417
  60.9 0.0 copy-done.1
  60.9 7.0 %collective-permute-start = (bf16[256,2048]{1,0:T(8,128)(2,1)S(1)}, bf16[256,2048]{1,0:T(8,128)(2,1)}, u32[]{:S(2)}, u32[]{:S(2)}) collective-permute-start(bf16[256,2048]{1,0:T(8,128)(2,1)S(1)} %copy-done.1), channel_id=1, source_target_pairs={{0,1},{1,0},{2,3},{3,2},{4,5},{5,4},{6,7},{7,6},{8,9},{9,8},{10,11... | collective-permute-start | bytes 3145736 | tf_op jit(solution)/shard_map/ppermute | solution.py:416
  67.9 14.8 %all-to-all-done.1.part_ref = bf16[8,208,256]{2,1,0:T(8,128)(2,1)S(1)} async-done(((bf16[8,208,256]{2,1,0:T(8,128)(2,1)}), bf16[8,208,256]{2,1,0:T(8,128)(2,1)S(1)}, u32[]{:S(2)}, u32[]{:S(2)}) %all-to-all-start.1) | async-done | bytes 852000 | tf_op jit(solution)/shard_map/all_to_all | solution.py:417
  82.7 0.5 combine.1
  83.3 10.4 %all-gather = bf16[4,96,256]{2,1,0:T(8,128)(2,1)S(1)} all-gather(bf16[2,96,256]{2,1,0:T(8,128)(2,1)S(1)} %combine.1), channel_id=2, replica_groups=mesh['sp_0'=8,'sp_1'=8,'x'=4,'c'=2] {'c'}, dimensions={0}, use_global_device_ids=true | all-gather | bytes 294912 | tf_op jit(solution)/shard_map/all_gather | solution.py:418
  93.7 0.0 collective-permute-done.other_ref
  93.7 2.4 %project.1 = bf16[96,2048]{1,0:T(8,128)(2,1)} custom-call(bf16[2,2,96,256]{3,2,1,0:T(8,128)(2,1)S(1)} %bitcast.8, bf16[256,2048]{1,0:T(8,128)(2,1)S(1)} %copy-done.1, bf16[256,2048]{1,0:T(8,128)(2,1)} %collective-permute-done.other_ref), custom_call_target="tpu_custom_call" | custom-call | flops 201326592 | bytes 3145728 | tf_op jit(solution)/shard_map/project/pallas_call | solution.py:293
  96.2 4.3 %all-to-all-start.2 = ((bf16[4,24,2048]{2,1,0:T(8,128)(2,1)}), bf16[4,24,2048]{2,1,0:T(8,128)(2,1)S(1)}, u32[]{:S(2)}, u32[]{:S(2)}) async-start(bf16[4,24,2048]{2,1,0:T(8,128)(2,1)} %bitcast.4), calls=%async_computation.2 | async-start | bytes 786432 | tf_op jit(solution)/shard_map/all_to_all | solution.py:384
  100.4 0.0 copy-done
  100.5 7.3 %all-to-all-done.2.part_ref = bf16[4,24,2048]{2,1,0:T(8,128)(2,1)S(1)} async-done(((bf16[4,24,2048]{2,1,0:T(8,128)(2,1)}), bf16[4,24,2048]{2,1,0:T(8,128)(2,1)S(1)}, u32[]{:S(2)}, u32[]{:S(2)}) %all-to-all-start.2) | async-done | bytes 393248 | tf_op jit(solution)/shard_map/all_to_all | solution.py:384
  107.7 0.0 copy-done.2
  107.7 0.2 stream.1
  107.9 14.9 %all_gather.18.x_ref = bf16[192,2048]{1,0:T(8,128)(2,1)S(1)} all-gather(bf16[24,2048]{1,0:T(8,128)(2,1)S(1)} %get-tuple-element.13), channel_id=1, replica_groups=mesh['sp_0'=8,'sp_1'=8,'x'=4,'c'=2] {'x','c'}, dimensions={0}, use_global_device_ids=true | all-gather | bytes 884736 | tf_op jit(solution)/shard_map/all_gather | solution.py:423
  122.9 2.8 %all-gather.3.cloned.1.call-done.w_hbm = bf16[2048,2176]{1,0:T(8,128)(2,1)} async-done(((bf16[32,2176]{1,0:T(8,128)(2,1)}), bf16[2048,2176]{1,0:T(8,128)(2,1)}) %all-gather.3.cloned.1.call-update) | async-done | bytes 8912912 | tf_op jit(solution)/shard_map/all_gather | solution.py:413
  125.7 5.0 %feed.1 = bf16[192,2048]{1,0:T(8,128)(2,1)S(1)} custom-call(bf16[192,2048]{1,0:T(8,128)(2,1)S(1)} %all_gather.18.x_ref, bf16[2048,2176]{1,0:T(8,128)(2,1)} %all-gather.3.cloned.1.call-done.w_hbm), custom_call_target="tpu_custom_call" | custom-call | flops 1660944384 | bytes 10485760 | tf_op jit(solution)/shard_map/feed/pallas_call | solution.py:338
  130.7 16.7 %all_to_all.20 = bf16[8,24,2048]{2,1,0:T(8,128)(2,1)S(1)} all-to-all(bf16[8,24,2048]{2,1,0:T(8,128)(2,1)S(1)} %bitcast.7), channel_id=1, replica_groups=mesh['sp_0'=8,'sp_1'=8,'x'=4,'c'=2] {'x','c'}, dimensions={0} | all-to-all | bytes 1572864 | tf_op jit(solution)/shard_map/all_to_all | solution.py:384
  147.4 0.1 convert_reduce_fusion
  147.5 0.7 add_convert_fusion
  (1 shorter events, 0.0 us)
Async XLA Ops:
  6.5 93.9 %copy-start = (bf16[192,2048]{1,0:T(8,128)(2,1)S(1)}, bf16[192,2048]{1,0:T(8,128)(2,1)}, u32[]{:S(2)}) copy-start(bf16[192,2048]{1,0:T(8,128)(2,1)} %param.15) | copy-start | bytes 2359300
  6.5 54.3 %copy-start.1 = (bf16[256,2048]{1,0:T(8,128)(2,1)S(1)}, bf16[256,2048]{1,0:T(8,128)(2,1)}, u32[]{:S(2)}) copy-start(bf16[256,2048]{1,0:T(8,128)(2,1)} %own_ref.1) | copy-start | bytes 3145732
  6.5 119.2 %all-gather.3.cloned.1.call-start = ((), (), s32[]{:S(2)}) async-start(), calls=%async_computation.4 | async-start | bytes 9052160 | tf_op jit(solution)/shard_map/all_gather | solution.py:413
  9.5 98.2 %copy-start.2 = (f32[2048]{0:T(1024)S(1)}, f32[2048]{0:T(1024)}, u32[]{:S(2)}) copy-start(f32[2048]{0:T(1024)} %param.22) | copy-start | bytes 24580
  9.6 34.5 %all-to-all-start = ((bf16[8,192,256]{2,1,0:T(8,128)(2,1)}), bf16[8,192,256]{2,1,0:T(8,128)(2,1)S(1)}, u32[]{:S(2)}, u32[]{:S(2)}) async-start(bf16[8,192,256]{2,1,0:T(8,128)(2,1)} %get-tuple-element.10), calls=%async_computation | async-start | bytes 1572864 | tf_op jit(solution)/shard_map/all_to_all | solution.py:414
  53.5 29.3 %all-to-all-start.1 = ((bf16[8,208,256]{2,1,0:T(8,128)(2,1)}), bf16[8,208,256]{2,1,0:T(8,128)(2,1)S(1)}, u32[]{:S(2)}, u32[]{:S(2)}) async-start(bf16[8,208,256]{2,1,0:T(8,128)(2,1)} %attend.1), calls=%async_computation.1 | async-start | bytes 1703936 | tf_op jit(solution)/shard_map/all_to_all | solution.py:417
  60.9 32.8 %collective-permute-start = (bf16[256,2048]{1,0:T(8,128)(2,1)S(1)}, bf16[256,2048]{1,0:T(8,128)(2,1)}, u32[]{:S(2)}, u32[]{:S(2)}) collective-permute-start(bf16[256,2048]{1,0:T(8,128)(2,1)S(1)} %copy-done.1), channel_id=1, source_target_pairs={{0,1},{1,0},{2,3},{3,2},{4,5},{5,4},{6,7},{7,6},{8,9},{9,8},{10,11... | collective-permute-start | bytes 3145736 | tf_op jit(solution)/shard_map/ppermute | solution.py:416
  96.2 11.6 %all-to-all-start.2 = ((bf16[4,24,2048]{2,1,0:T(8,128)(2,1)}), bf16[4,24,2048]{2,1,0:T(8,128)(2,1)S(1)}, u32[]{:S(2)}, u32[]{:S(2)}) async-start(bf16[4,24,2048]{2,1,0:T(8,128)(2,1)} %bitcast.4), calls=%async_computation.2 | async-start | bytes 786432 | tf_op jit(solution)/shard_map/all_to_all | solution.py:384
Sparse Core Ops, SparseCore 0:
  10.3 115.3 all-gather.2

commit v9 on v8

--- a/solution.py
+++ b/solution.py
@@ -16,7 +16,7 @@
 BF16 = jnp.bfloat16
 F32 = jnp.float32
 ROPE_BASE = 10000.0
-STAT_ROWS = 16
+STAT_ROWS = 8
 LOG2E = 1.4426950408889634
 
 

time: 156 us -> 155 us (level)
  waiting for transfers between devices: 25 us -> 22.7 us
  blocking collectives: 65.7 us -> 67.6 us
    all_to_all x1, waiting for transfers between devices: 14.8 us -> 12.4 us  [body(): lax.all_to_all(attend(queries, keys_values), 'sp_0', 0, 0, tiled=True)]
    all_gather x1, blocking collectives: 10.4 us -> 12.2 us  [body(): attn = lax.all_gather(combine(partial), 'c', axis=0)]
where the time goes in v9:
time: 155 us; the launch traced here: 154 us
  blocking collectives  67.6 us (44%)
  starting transfers between devices  29.3 us (19%)
  waiting for transfers between devices  22.7 us (15%)
  Pallas kernels  20.7 us (13%)
  between operations  13.4 us (9%)
    all_gather x1, blocking collectives, body(): keys_values = lax.all_gather(keys_values, 'sp_1', axis=0, tiled=True)  23.7 us
    all_to_all x1, blocking collectives, scattered(): lax.all_to_all(x.reshape(count, -1, x.shape[1]), axis, 0, 0, tiled=True)  16.7 us
    all_gather x1, blocking collectives, body(): normed = lax.all_gather(normed, TP, axis=0, tiled=True)  14.9 us
    all_to_all x1, waiting for transfers between devices, body(): lax.all_to_all(attend(queries, keys_values), 'sp_0', 0, 0, tiled=True)  12.4 us
    all_gather x1, blocking collectives, body(): attn = lax.all_gather(combine(partial), 'c', axis=0)  12.2 us
    all_to_all x1, starting transfers between devices, body(): queries = lax.all_to_all(copies, 'sp_0', 0, 0, tiled=True)  10.9 us
    pallas_call x1, Pallas kernels, attend(): pl.pallas_call(functools.partial(attend_kernel, chunk=next((n for n in (5...  9.5 us
    all_to_all x1, starting transfers between devices, body(): lax.all_to_all(attend(queries, keys_values), 'sp_0', 0, 0, tiled=True)  7.32 us
  transfers between devices with their start and end apart: 5, of which 3 were waited for; matrix products, arithmetic and copies ran while one was open for 0% of the time, Pallas kernels for 8%

profile of v9, /device:TPU:1, one launch (start us, length us, event | category | flops | bytes accessed | tf_op | source)
XLA Modules:
  0.0 154.5 jit_solution(3194366121412027286)
XLA Ops:
  6.5 0.0 copy-start
  6.5 0.0 copy-start.1
  6.5 0.0 all-gather.3.cloned.1.call-start
  6.5 3.0 %prep.1 = (bf16[32,2176]{1,0:T(8,128)(2,1)}, bf16[8,192,256]{2,1,0:T(8,128)(2,1)}, bf16[192,256]{1,0:T(8,128)(2,1)}) custom-call(bf16[192,256]{1,0:T(8,128)(2,1)} %q_ref.1, bf16[192,128]{1,0:T(8,128)(2,1)} %k_ref.1, bf16[192,128]{1,0:T(8,128)(2,1)} %v_ref.1, bf16[32,704]{1,0:T(8,128)(2,1)} %gate_ref.1, bf16[32,704]{1,0:T(8,128)(2,1)} %up_ref.1, ...), custom_call_target="tpu_custom_call" | custom-call | tf_op jit(solution)/shard_map/prep/pallas_call | solution.py:98
  9.5 0.0 all-gather.3.cloned.1.call-update
  9.5 0.0 copy-start.2
  9.6 10.9 %all-to-all-start = ((bf16[8,192,256]{2,1,0:T(8,128)(2,1)}), bf16[8,192,256]{2,1,0:T(8,128)(2,1)S(1)}, u32[]{:S(2)}, u32[]{:S(2)}) async-start(bf16[8,192,256]{2,1,0:T(8,128)(2,1)} %get-tuple-element.10), calls=%async_computation | async-start | bytes 1572864 | tf_op jit(solution)/shard_map/all_to_all | solution.py:414
  20.4 23.7 %all_gather.15.kv_ref = bf16[1536,256]{1,0:T(8,128)(2,1)S(1)} all-gather(bf16[192,256]{1,0:T(8,128)(2,1)} %get-tuple-element.11), channel_id=1, replica_groups=mesh['sp_0'=8,'sp_1'=8,'x'=4,'c'=2] {'sp_1'}, dimensions={0}, use_global_device_ids=true | all-gather | bytes 884736 | tf_op jit(solution)/shard_map/all_gather | solution.py:415
  44.1 0.0 all-to-all-done.q_ref.next_ref
  44.1 9.5 %attend.1 = bf16[8,200,256]{2,1,0:T(8,128)(2,1)} custom-call(bf16[8,192,256]{2,1,0:T(8,128)(2,1)S(1)} %all-to-all-done.q_ref.next_ref, bf16[8,192,256]{2,1,0:T(8,128)(2,1)S(1)} %all-to-all-done.q_ref.next_ref, bf16[1536,256]{1,0:T(8,128)(2,1)S(1)} %all_gather.15.kv_ref), custom_call_target="tpu_custom_call" | custom-call | flops 2415919104 | bytes 4194304 | tf_op jit(solution)/shard_map/attend/pallas_call | solution.py:204
  53.6 7.3 %all-to-all-start.1 = ((bf16[8,200,256]{2,1,0:T(8,128)(2,1)}), bf16[8,200,256]{2,1,0:T(8,128)(2,1)S(1)}, u32[]{:S(2)}, u32[]{:S(2)}) async-start(bf16[8,200,256]{2,1,0:T(8,128)(2,1)} %attend.1), calls=%async_computation.1 | async-start | bytes 1638400 | tf_op jit(solution)/shard_map/all_to_all | solution.py:417
  60.9 0.0 copy-done.1
  60.9 7.2 %collective-permute-start = (bf16[256,2048]{1,0:T(8,128)(2,1)S(1)}, bf16[256,2048]{1,0:T(8,128)(2,1)}, u32[]{:S(2)}, u32[]{:S(2)}) collective-permute-start(bf16[256,2048]{1,0:T(8,128)(2,1)S(1)} %copy-done.1), channel_id=1, source_target_pairs={{0,1},{1,0},{2,3},{3,2},{4,5},{5,4},{6,7},{7,6},{8,9},{9,8},{10,11... | collective-permute-start | bytes 3145736 | tf_op jit(solution)/shard_map/ppermute | solution.py:416
  68.2 12.4 %all-to-all-done.1.part_ref = bf16[8,200,256]{2,1,0:T(8,128)(2,1)S(1)} async-done(((bf16[8,200,256]{2,1,0:T(8,128)(2,1)}), bf16[8,200,256]{2,1,0:T(8,128)(2,1)S(1)}, u32[]{:S(2)}, u32[]{:S(2)}) %all-to-all-start.1) | async-done | bytes 819232 | tf_op jit(solution)/shard_map/all_to_all | solution.py:417
  80.6 0.5 combine.1
  81.1 12.2 %all-gather = bf16[4,96,256]{2,1,0:T(8,128)(2,1)S(1)} all-gather(bf16[2,96,256]{2,1,0:T(8,128)(2,1)S(1)} %combine.1), channel_id=2, replica_groups=mesh['sp_0'=8,'sp_1'=8,'x'=4,'c'=2] {'c'}, dimensions={0}, use_global_device_ids=true | all-gather | bytes 294912 | tf_op jit(solution)/shard_map/all_gather | solution.py:418
  93.3 0.0 collective-permute-done.other_ref
  93.3 2.5 %project.1 = bf16[96,2048]{1,0:T(8,128)(2,1)} custom-call(bf16[2,2,96,256]{3,2,1,0:T(8,128)(2,1)S(1)} %bitcast.8, bf16[256,2048]{1,0:T(8,128)(2,1)S(1)} %copy-done.1, bf16[256,2048]{1,0:T(8,128)(2,1)} %collective-permute-done.other_ref), custom_call_target="tpu_custom_call" | custom-call | flops 201326592 | bytes 3145728 | tf_op jit(solution)/shard_map/project/pallas_call | solution.py:293
  95.8 3.9 %all-to-all-start.2 = ((bf16[4,24,2048]{2,1,0:T(8,128)(2,1)}), bf16[4,24,2048]{2,1,0:T(8,128)(2,1)S(1)}, u32[]{:S(2)}, u32[]{:S(2)}) async-start(bf16[4,24,2048]{2,1,0:T(8,128)(2,1)} %bitcast.4), calls=%async_computation.2 | async-start | bytes 786432 | tf_op jit(solution)/shard_map/all_to_all | solution.py:384
  99.7 0.0 copy-done
  99.7 7.3 %all-to-all-done.2.part_ref = bf16[4,24,2048]{2,1,0:T(8,128)(2,1)S(1)} async-done(((bf16[4,24,2048]{2,1,0:T(8,128)(2,1)}), bf16[4,24,2048]{2,1,0:T(8,128)(2,1)S(1)}, u32[]{:S(2)}, u32[]{:S(2)}) %all-to-all-start.2) | async-done | bytes 393248 | tf_op jit(solution)/shard_map/all_to_all | solution.py:384
  107.0 0.0 copy-done.2
  107.0 0.2 stream.1
  107.2 14.9 %all_gather.18.x_ref = bf16[192,2048]{1,0:T(8,128)(2,1)S(1)} all-gather(bf16[24,2048]{1,0:T(8,128)(2,1)S(1)} %get-tuple-element.13), channel_id=1, replica_groups=mesh['sp_0'=8,'sp_1'=8,'x'=4,'c'=2] {'x','c'}, dimensions={0}, use_global_device_ids=true | all-gather | bytes 884736 | tf_op jit(solution)/shard_map/all_gather | solution.py:423
  122.1 2.9 %all-gather.3.cloned.1.call-done.w_hbm = bf16[2048,2176]{1,0:T(8,128)(2,1)} async-done(((bf16[32,2176]{1,0:T(8,128)(2,1)}), bf16[2048,2176]{1,0:T(8,128)(2,1)}) %all-gather.3.cloned.1.call-update) | async-done | bytes 8912912 | tf_op jit(solution)/shard_map/all_gather | solution.py:413
  125.0 5.0 %feed.1 = bf16[192,2048]{1,0:T(8,128)(2,1)S(1)} custom-call(bf16[192,2048]{1,0:T(8,128)(2,1)S(1)} %all_gather.18.x_ref, bf16[2048,2176]{1,0:T(8,128)(2,1)} %all-gather.3.cloned.1.call-done.w_hbm), custom_call_target="tpu_custom_call" | custom-call | flops 1660944384 | bytes 10485760 | tf_op jit(solution)/shard_map/feed/pallas_call | solution.py:338
  130.1 16.7 %all_to_all.20 = bf16[8,24,2048]{2,1,0:T(8,128)(2,1)S(1)} all-to-all(bf16[8,24,2048]{2,1,0:T(8,128)(2,1)S(1)} %bitcast.7), channel_id=1, replica_groups=mesh['sp_0'=8,'sp_1'=8,'x'=4,'c'=2] {'x','c'}, dimensions={0} | all-to-all | bytes 1572864 | tf_op jit(solution)/shard_map/all_to_all | solution.py:384
  146.8 0.1 convert_reduce_fusion
  146.9 0.7 add_convert_fusion
  (1 shorter events, 0.0 us)
Async XLA Ops:
  6.5 93.1 %copy-start = (bf16[192,2048]{1,0:T(8,128)(2,1)S(1)}, bf16[192,2048]{1,0:T(8,128)(2,1)}, u32[]{:S(2)}) copy-start(bf16[192,2048]{1,0:T(8,128)(2,1)} %param.15) | copy-start | bytes 2359300
  6.5 54.4 %copy-start.1 = (bf16[256,2048]{1,0:T(8,128)(2,1)S(1)}, bf16[256,2048]{1,0:T(8,128)(2,1)}, u32[]{:S(2)}) copy-start(bf16[256,2048]{1,0:T(8,128)(2,1)} %own_ref.1) | copy-start | bytes 3145732
  6.5 118.5 %all-gather.3.cloned.1.call-start = ((), (), s32[]{:S(2)}) async-start(), calls=%async_computation.4 | async-start | bytes 9052160 | tf_op jit(solution)/shard_map/all_gather | solution.py:413
  9.5 97.4 %copy-start.2 = (f32[2048]{0:T(1024)S(1)}, f32[2048]{0:T(1024)}, u32[]{:S(2)}) copy-start(f32[2048]{0:T(1024)} %param.22) | copy-start | bytes 24580
  9.6 34.5 %all-to-all-start = ((bf16[8,192,256]{2,1,0:T(8,128)(2,1)}), bf16[8,192,256]{2,1,0:T(8,128)(2,1)S(1)}, u32[]{:S(2)}, u32[]{:S(2)}) async-start(bf16[8,192,256]{2,1,0:T(8,128)(2,1)} %get-tuple-element.10), calls=%async_computation | async-start | bytes 1572864 | tf_op jit(solution)/shard_map/all_to_all | solution.py:414
  53.6 27.0 %all-to-all-start.1 = ((bf16[8,200,256]{2,1,0:T(8,128)(2,1)}), bf16[8,200,256]{2,1,0:T(8,128)(2,1)S(1)}, u32[]{:S(2)}, u32[]{:S(2)}) async-start(bf16[8,200,256]{2,1,0:T(8,128)(2,1)} %attend.1), calls=%async_computation.1 | async-start | bytes 1638400 | tf_op jit(solution)/shard_map/all_to_all | solution.py:417
  60.9 32.4 %collective-permute-start = (bf16[256,2048]{1,0:T(8,128)(2,1)S(1)}, bf16[256,2048]{1,0:T(8,128)(2,1)}, u32[]{:S(2)}, u32[]{:S(2)}) collective-permute-start(bf16[256,2048]{1,0:T(8,128)(2,1)S(1)} %copy-done.1), channel_id=1, source_target_pairs={{0,1},{1,0},{2,3},{3,2},{4,5},{5,4},{6,7},{7,6},{8,9},{9,8},{10,11... | collective-permute-start | bytes 3145736 | tf_op jit(solution)/shard_map/ppermute | solution.py:416
  95.8 11.2 %all-to-all-start.2 = ((bf16[4,24,2048]{2,1,0:T(8,128)(2,1)}), bf16[4,24,2048]{2,1,0:T(8,128)(2,1)S(1)}, u32[]{:S(2)}, u32[]{:S(2)}) async-start(bf16[4,24,2048]{2,1,0:T(8,128)(2,1)} %bitcast.4), calls=%async_computation.2 | async-start | bytes 786432 | tf_op jit(solution)/shard_map/all_to_all | solution.py:384
Sparse Core Ops, SparseCore 0:
  10.3 114.6 all-gather.2
